TPU v7x, 32 devices: a whole 2x2x4 slice. The times are simulated.
32 devices in a mesh: ep: 32 (over z, y, x, core).
Axes of the slice: x: 2, y: 2, z: 4, core: 2. Of those that a mesh axis runs over, the one named last changes fastest.
Arguments:
- hidden_in: bfloat16 [512, 2048], P('ep'), may hold values from -6 to 6
- lengths: int32 [512], P('ep'), may hold values from 1 to 1024
- attn_gain: float32 [2048], replicated, may hold values from 0.1 to 1.9
- query_weight: bfloat16 [2048, 512], replicated, may hold values from -0.125 to 0.125
- key_weight: bfloat16 [2048, 128], replicated, may hold values from -0.125 to 0.125
- value_weight: bfloat16 [2048, 128], replicated, may hold values from -0.125 to 0.125
- score_bias: float32 [8], replicated, may hold values from -7.5 to -3.5
- out_weight: bfloat16 [512, 2048], replicated, may hold values from -0.25 to 0.25
- key_cache: bfloat16 [512, 1024, 128], P('ep'), may hold values from -6 to 6
- value_cache: bfloat16 [512, 1024, 128], P('ep'), may hold values from -10 to 10
- ffn_gain: float32 [2048], replicated, may hold values from 0.1 to 1.9
- routes: int32 [512, 4], P('ep'), may hold values from 0 to 31, all different within a row; in each aligned block of 16 rows (0 to 15, 16 to 31, ...) at most 2 rows name the same one
- route_weights: float32 [512, 4], P('ep'), may hold values from 0.25 to 1
- expert_gate: bfloat16 [32, 2048, 512], P('ep'), may hold values from -0.125 to 0.125
- expert_up: bfloat16 [32, 2048, 512], P('ep'), may hold values from -0.125 to 0.125
- expert_down: bfloat16 [32, 512, 2048], P('ep'), may hold values from -0.25 to 0.25
- dense_gate: bfloat16 [2048, 2048], P(None, 'ep'), may hold values from -0.125 to 0.125
- dense_up: bfloat16 [2048, 2048], P(None, 'ep'), may hold values from -0.125 to 0.125
- dense_down: bfloat16 [2048, 2048], P(None, 'ep'), may hold values from -0.125 to 0.125
- branch_gate: float32 [2048], replicated, may hold values from -0.125 to 0.125
Outputs:
- hidden_out: bfloat16 [512, 2048], P('ep')
- new_keys: bfloat16 [512, 128], P('ep')
- new_values: bfloat16 [512, 128], P('ep')
Inputs may be any that keep to these rules, and one draw needn't show every extreme that they name: `routes`: in each device's 16 rows no expert is named twice.
All inputs are finite; a program needn't handle non-finite values.
Results may differ from a plain program's by a relative error of at most 0.0061.
Values may be sent and summed in bfloat16 or wider, within the bound.
No kernel may reach another device: no remote copies, remote signals or barrier semaphores. Data moves between devices by JAX's collectives and lax.ppermute only.
A program may use at most 128 MiB of HBM per device.

v0:
```python
import jax
import jax.numpy as jnp
from jax import lax
from jax.sharding import PartitionSpec as P

HEADS = 8
KV_HEADS = 2
HEAD = 64
TOP = 4


norm_eps = 1e-06


def rms_norm(values_in, gain):
    as_float = values_in.astype(jnp.float32)
    scaled = as_float * lax.rsqrt(jnp.mean(as_float * as_float, axis=-1, keepdims=True) + norm_eps)
    return (scaled * gain).astype(jnp.bfloat16)


def later_sums(log_keep):
    cache_len = log_keep.shape[-1]
    span = 128
    block_count = cache_len // span
    lead_shape = log_keep.shape[:-1]
    blocked = log_keep.reshape(lead_shape + (block_count, span))
    span_pos = jnp.arange(span, dtype=jnp.int32)
    inner_tri = (span_pos[:, None] > span_pos[None, :]).astype(jnp.float32)
    inside = jnp.einsum("nkgbj,js->nkgbs", blocked, inner_tri, precision=lax.Precision.HIGHEST)
    totals = jnp.sum(blocked, axis=-1)
    block_pos = jnp.arange(block_count, dtype=jnp.int32)
    outer_tri = (block_pos[:, None] > block_pos[None, :]).astype(jnp.float32)
    beyond = jnp.einsum("nkgc,cb->nkgb", totals, outer_tri, precision=lax.Precision.HIGHEST)
    return (inside + beyond[..., None]).reshape(log_keep.shape)


def stick_attend(query_blk, key_blk, value_blk, seq_lens, score_bias):
    seq_count = query_blk.shape[0]
    cache_len = key_blk.shape[1]
    per_group = HEADS // KV_HEADS
    query_r = query_blk.reshape(seq_count, KV_HEADS, per_group, HEAD)
    key_r = key_blk.reshape(seq_count, cache_len, KV_HEADS, HEAD)
    value_r = value_blk.reshape(seq_count, cache_len, KV_HEADS, HEAD)
    head_bias = score_bias.reshape(KV_HEADS, per_group)[None, :, :, None]
    scores = jnp.einsum(
        "nkgd,nskd->nkgs", query_r, key_r, preferred_element_type=jnp.float32
    ) * HEAD ** (-0.5)
    scores = scores + head_bias
    live_mask = (jnp.arange(cache_len, dtype=jnp.int32)[None, :] < seq_lens[:, None])[
        :, None, None, :
    ]
    log_keep = jnp.where(live_mask, jax.nn.log_sigmoid(-scores), 0.0)
    after_sum = later_sums(log_keep)
    weights = jnp.where(live_mask, jnp.exp(jax.nn.log_sigmoid(scores) + after_sum), 0.0).astype(
        jnp.bfloat16
    )
    mixed = jnp.einsum("nkgs,nskd->nkgd", weights, value_r, preferred_element_type=jnp.float32)
    return mixed.astype(jnp.bfloat16).reshape(seq_count, HEADS * HEAD)


def dense_hidden_of(tok_rows, gate_w, up_w):
    gate_pre = jnp.dot(tok_rows, gate_w, preferred_element_type=jnp.float32)
    up_pre = jnp.dot(tok_rows, up_w, preferred_element_type=jnp.float32)
    return (jax.nn.silu(gate_pre) * up_pre).astype(jnp.bfloat16)


def down_product(hidden_rows, down_w):
    return lax.dot_general(
        hidden_rows, down_w, (((1,), (1,)), ((), ())), preferred_element_type=jnp.float32
    )


def per_device(
    hidden_in,
    lengths,
    attn_gain,
    query_weight,
    key_weight,
    value_weight,
    score_bias,
    out_weight,
    key_cache,
    value_cache,
    ffn_gain,
    routes,
    route_weights,
    expert_gate,
    expert_up,
    expert_down,
    dense_gate,
    dense_up,
    dense_down,
    branch_gate,
):
    seq_count = hidden_in.shape[0]
    row_width = hidden_in.shape[1]
    normed = rms_norm(hidden_in, attn_gain)
    queries = jnp.dot(normed, query_weight, preferred_element_type=jnp.float32).astype(jnp.bfloat16)
    new_keys = jnp.dot(normed, key_weight, preferred_element_type=jnp.float32).astype(jnp.bfloat16)
    new_values = jnp.dot(normed, value_weight, preferred_element_type=jnp.float32).astype(
        jnp.bfloat16
    )
    attended = stick_attend(queries, key_cache, value_cache, lengths, score_bias)
    middle = hidden_in.astype(jnp.float32) + jnp.dot(
        attended, out_weight, preferred_element_type=jnp.float32
    )
    ffn_in = rms_norm(middle, ffn_gain)
    devices = lax.axis_size("ep")
    local_experts = expert_gate.shape[0]
    experts_all = local_experts * devices
    capacity = max(1, seq_count * TOP // experts_all)
    flat_ids = routes.reshape(-1)
    pick_count = flat_ids.shape[0]
    pick_pos = jnp.arange(pick_count, dtype=jnp.int32)
    same_expert = (flat_ids[:, None] == flat_ids[None, :]) & (pick_pos[None, :] < pick_pos[:, None])
    slot_rank = jnp.sum(same_expert.astype(jnp.int32), axis=1)
    slot_index = flat_ids * capacity + slot_rank
    pick_rows = jnp.repeat(ffn_in, TOP, axis=0)
    outgoing = (
        jnp.zeros((experts_all * capacity, row_width), jnp.bfloat16).at[slot_index].set(pick_rows)
    )
    outgoing = outgoing.reshape(devices, local_experts * capacity, row_width)
    arrived = lax.all_to_all(outgoing, "ep", split_axis=0, concat_axis=0, tiled=True)
    flat_in = arrived.reshape(-1, row_width)
    gate_pre = jnp.dot(flat_in, expert_gate[0], preferred_element_type=jnp.float32)
    up_pre = jnp.dot(flat_in, expert_up[0], preferred_element_type=jnp.float32)
    hidden_act = (jax.nn.silu(gate_pre) * up_pre).astype(jnp.bfloat16)
    expert_rows = jnp.dot(hidden_act, expert_down[0], preferred_element_type=jnp.float32).astype(
        jnp.bfloat16
    )
    returned = lax.all_to_all(
        expert_rows.reshape(arrived.shape), "ep", split_axis=0, concat_axis=0, tiled=True
    )
    returned = returned.reshape(experts_all * capacity, row_width)
    picked = returned[slot_index].reshape(seq_count, TOP, row_width).astype(jnp.float32)
    expert_sum = jnp.sum(picked * route_weights[:, :, None], axis=1)

    def hidden_rows(piece, start):
        return dense_hidden_of(piece, dense_gate, dense_up)

    unit_hidden = hidden_rows(lax.all_gather(ffn_in, "ep", axis=0, tiled=True), jnp.int32(0))
    token_hidden = lax.all_to_all(unit_hidden, "ep", split_axis=0, concat_axis=1, tiled=True)
    full_down = lax.all_gather(dense_down, "ep", axis=1, tiled=True)
    dense_out = down_product(token_hidden, full_down)
    gate_value = jax.nn.sigmoid(
        jnp.dot(ffn_in.astype(jnp.float32), branch_gate, precision=lax.Precision.HIGHEST)
    )
    hidden_out = (middle + expert_sum + gate_value[:, None] * dense_out).astype(jnp.bfloat16)
    return (hidden_out, new_keys, new_values)


def solution(mesh):
    return jax.shard_map(
        per_device,
        mesh=mesh,
        in_specs=(
            P("ep", None),
            P("ep"),
            P(),
            P(),
            P(),
            P(),
            P(),
            P(),
            P("ep", None, None),
            P("ep", None, None),
            P(),
            P("ep", None),
            P("ep", None),
            P("ep", None, None),
            P("ep", None, None),
            P("ep", None, None),
            P(None, "ep"),
            P(None, "ep"),
            P(None, "ep"),
            P(),
        ),
        out_specs=(P("ep", None), P("ep", None), P("ep", None)),
        check_vma=False,
    )
```

profile of v0, /device:TPU:0, one launch (start us, length us, event | category | flops | bytes accessed | tf_op | source)
XLA Modules:
  0.0 187.4 jit_solution(7200954543116276917)
XLA Ops:
  7.2 1.1 fusion.31
  8.4 2.1 %convolution_convert_fusion.2 = bf16[16,512]{1,0:T(8,128)(2,1)S(1)} fusion(bf16[2048,512]{1,0:T(8,128)(2,1)} %param.23, bf16[16,2048]{1,0:T(8,128)(2,1)} %param.20, f32[2048]{0:T(1024)} %param.22, f32[16]{0:T(128)S(1)} %add_rsqrt_fusion.1), kind=kOutput, calls=%fused_computation.22 | convolution fusion | flops 33693696 | bytes 2187328 | tf_op jit(solution)/shard_map/dot_general | solution.py:98
  10.6 6.4 %copy.46 = bf16[16,1024,128]{1,2,0:T(8,128)(2,1)} copy(bf16[16,1024,128]{2,1,0:T(8,128)(2,1)} %param.28) | data formatting | bytes 8388608 | tf_op args[8]
  17.1 4.0 %fusion.27 = (f32[16,2,4,1024]{3,2,1,0:T(4,128)S(1)}, f32[16,2,4,1024]{3,2,1,0:T(4,128)}) fusion(pred[16,1024]{1,0:T(8,128)(4,1)S(1)} %iota_compare_fusion.1, f32[2,4]{1,0:T(2,128)S(1)} %add.87, bf16[16,2,4,64]{3,2,1,0:T(4,128)(2,1)S(1)} %reshape.115, bf16[16,1024,2,64]{1,3,2,0:T(8,128)(2,1)} %bitcast.67), kind=kOutput, calls=%fused_computation.36 | convolution fusion | flops 18087936 | bytes 5275680 | tf_op jit(solution)/shard_map/nkgd,nskd->nkgs/dot_general | solution.py:45
  22.7 6.5 %copy.49 = bf16[16,1024,128]{1,2,0:T(8,128)(2,1)} copy(bf16[16,1024,128]{2,1,0:T(8,128)(2,1)} %param.29) | data formatting | bytes 8388608 | tf_op args[9]
  29.1 3.4 %convolution_convert_fusion.1 = bf16[16,2,4,64]{3,2,1,0:T(4,128)(2,1)S(1)} fusion(bf16[16,1024,2,64]{1,3,2,0:T(8,128)(2,1)} %bitcast.68, f32[16,2,4,1024]{3,2,1,0:T(4,128)S(1)} %reshape.118, f32[16,2,4,1024]{3,2,1,0:T(4,128)S(1)} %copy-done.14, pred[16,1024]{1,0:T(8,128)(4,1)S(1)} %iota_compare_fusion.1), kind=kOutput, calls=%fused_computation.21 | convolution fusion | flops 18227200 | bytes 5275648 | tf_op jit(solution)/shard_map/nkgs,nskd->nkgd/dot_general | solution.py:57
  32.7 2.1 %multiply_reduce_fusion.1 = (f32[16]{0:T(128)S(1)}, f32[16,2048]{1,0:T(8,128)S(1)}) fusion(bf16[16,512]{1,0:T(8,128)(2,1)S(1)} %reshape.120, bf16[512,2048]{1,0:T(8,128)(2,1)} %param.27, bf16[16,2048]{1,0:T(8,128)(2,1)S(1)} %copy-done.2), kind=kOutput, calls=%fused_computation.51 | convolution fusion | flops 33685488 | bytes 2310208 | tf_op jit(solution)/shard_map/dot_general | solution.py:104
  36.3 0.9 broadcast_in_dim.20
  37.9 1.1 scatter_custom_fusion
  38.9 0.9 reshape.122
  39.8 7.3 %all-to-all-start = ((bf16[32,2,2048]{2,1,0:T(2,128)(2,1)}), bf16[32,2,2048]{2,1,0:T(2,128)(2,1)S(1)}, u32[]{:S(2)}, u32[]{:S(2)}) async-start(bf16[32,2,2048]{2,1,0:T(2,128)(2,1)} %reshape.122), calls=%async_computation | async-start | bytes 524288 | tf_op jit(solution)/shard_map/all_to_all | solution.py:123
  47.3 11.6 %all-to-all-done = bf16[32,2,2048]{2,1,0:T(2,128)(2,1)S(1)} async-done(((bf16[32,2,2048]{2,1,0:T(2,128)(2,1)}), bf16[32,2,2048]{2,1,0:T(2,128)(2,1)S(1)}, u32[]{:S(2)}, u32[]{:S(2)}) %all-to-all-start) | async-done | bytes 262176 | tf_op jit(solution)/shard_map/all_to_all | solution.py:123
  59.0 2.1 %fusion.5 = f32[64,512]{1,0:T(8,128)S(1)} fusion(bf16[64,2048]{1,0:T(8,128)(2,1)S(1)} %reshape.123, bf16[1,2048,512]{2,1,0:T(8,128)(2,1)} %param.33), kind=kOutput, calls=%fused_computation.10 | convolution fusion | flops 134217728 | bytes 2490368 | tf_op jit(solution)/shard_map/dot_general | solution.py:125
  61.1 2.6 %convolution_convert_fusion = bf16[64,2048]{1,0:T(8,128)(2,1)S(1)} fusion(bf16[1,512,2048]{2,1,0:T(8,128)(2,1)S(1)} %copy-done, bf16[64,2048]{1,0:T(8,128)(2,1)S(1)} %reshape.123, bf16[1,2048,512]{2,1,0:T(8,128)(2,1)} %param.34, f32[64,512]{1,0:T(8,128)S(1)} %fusion.5), kind=kOutput, calls=%fused_computation.2 | convolution fusion | flops 268763136 | bytes 4849664 | tf_op jit(solution)/shard_map/dot_general | solution.py:128
  63.7 0.9 reshape.124
  64.6 2.6 %all-to-all-start.1 = ((bf16[32,2,2048]{2,1,0:T(2,128)(2,1)}), bf16[32,2,2048]{2,1,0:T(2,128)(2,1)S(1)}, u32[]{:S(2)}, u32[]{:S(2)}) async-start(bf16[32,2,2048]{2,1,0:T(2,128)(2,1)} %reshape.124), calls=%async_computation.1 | async-start | bytes 524288 | tf_op jit(solution)/shard_map/all_to_all | solution.py:131
  68.1 1.9 %convolution_convert_fusion.4 = bf16[16,128]{1,0:T(8,128)(2,1)} fusion(bf16[2048,128]{1,0:T(8,128)(2,1)} %param.24, bf16[16,2048]{1,0:T(8,128)(2,1)S(1)} %copy-done.2, f32[2048]{0:T(1024)S(1)} %copy-done.6, f32[16]{0:T(128)S(1)} %add_rsqrt_fusion.1), kind=kOutput, calls=%fused_computation.24 | convolution fusion | flops 8521728 | bytes 602176 | tf_op jit(solution)/shard_map/dot_general | solution.py:99
  70.1 9.1 %all-to-all-done.1 = bf16[32,2,2048]{2,1,0:T(2,128)(2,1)S(1)} async-done(((bf16[32,2,2048]{2,1,0:T(2,128)(2,1)}), bf16[32,2,2048]{2,1,0:T(2,128)(2,1)S(1)}, u32[]{:S(2)}, u32[]{:S(2)}) %all-to-all-start.1) | async-done | bytes 262176 | tf_op jit(solution)/shard_map/all_to_all | solution.py:131
  80.2 16.4 %all-gather.3.cloned.1.call-done = bf16[512,2048]{1,0:T(8,128)(2,1)} async-done(((bf16[16,2048]{1,0:T(8,128)(2,1)}), bf16[512,2048]{1,0:T(8,128)(2,1)}) %all-gather.3.cloned.1.call-update) | async-done | bytes 2097168 | tf_op jit(solution)/shard_map/all_gather | solution.py:141
  96.6 2.5 %fusion.55 = f32[512,64]{0,1:T(8,128)S(1)} fusion(bf16[512,2048]{1,0:T(8,128)(2,1)} %all-gather.3.cloned.1.call-done, bf16[2048,64]{0,1:T(8,128)(2,1)S(1)} %copy-done.5), kind=kOutput, calls=%fused_computation.74 | convolution fusion | flops 134217728 | bytes 2490368 | tf_op jit(solution)/shard_map/dot_general | solution.py:62
  100.8 3.5 %all-to-all-start.2 = ((bf16[32,2,512]{2,1,0:T(2,128)(2,1)}), bf16[32,2,512]{2,1,0:T(2,128)(2,1)S(1)}, u32[]{:S(2)}, u32[]{:S(2)}) async-start(bf16[32,2,512]{2,1,0:T(2,128)(2,1)} %reshape.149), calls=%async_computation.2 | async-start | bytes 131072 | tf_op jit(solution)/shard_map/all_to_all | solution.py:142
  104.6 7.1 %all-to-all-done.2 = bf16[32,2,512]{2,1,0:T(2,128)(2,1)S(1)} async-done(((bf16[32,2,512]{2,1,0:T(2,128)(2,1)}), bf16[32,2,512]{2,1,0:T(2,128)(2,1)S(1)}, u32[]{:S(2)}, u32[]{:S(2)}) %all-to-all-start.2) | async-done | bytes 65568 | tf_op jit(solution)/shard_map/all_to_all | solution.py:142
  112.1 63.3 %all-gather.5.cloned.1.call-done = bf16[2048,2048]{0,1:T(8,128)(2,1)} async-done(((bf16[2048,64]{0,1:T(8,128)(2,1)}), bf16[2048,2048]{0,1:T(8,128)(2,1)}) %all-gather.5.cloned.1.call-update) | async-done | bytes 8388624 | tf_op jit(solution)/shard_map/all_gather | solution.py:143
  175.4 5.2 %fusion.1 = bf16[16,2048]{1,0:T(8,128)(2,1)} fusion(bf16[16,2048]{1,0:T(8,128)(2,1)S(1)} %all_to_all.25, bf16[2048,2048]{0,1:T(8,128)(2,1)} %all-gather.5.cloned.1.call-done, f32[16,2048]{1,0:T(8,128)S(1)} %get-tuple-element.6, f32[16,2048]{1,0:T(8,128)S(1)} %multiply_reduce_fusion, f32[16]{0:T(128)S(1)} %fusion.20), kind=kOutput, calls=%fused_computation.6 | convolution fusion | flops 134348800 | bytes 8781888 | tf_op jit(solution)/shard_map/dot_general | solution.py:68
  (70 shorter events, 8.6 us)
Async XLA Ops:
  7.2 53.9 %copy-start = (bf16[1,512,2048]{2,1,0:T(8,128)(2,1)S(1)}, bf16[1,512,2048]{2,1,0:T(8,128)(2,1)}, u32[]{:S(2)}) copy-start(bf16[1,512,2048]{2,1,0:T(8,128)(2,1)} %param.35) | copy-start | bytes 6291460
  7.2 3.3 %copy-start.10 = (s32[16]{0:T(128)S(1)}, s32[16]{0:T(128)}, u32[]{:S(2)}) copy-start(s32[16]{0:T(128)} %param.21) | copy-start | bytes 196
  7.2 89.4 %all-gather.3.cloned.1.call-start = ((), (), s32[]{:S(2)}) async-start(), calls=%async_computation.3 | async-start | bytes 2162688 | tf_op jit(solution)/shard_map/all_gather | solution.py:141
  10.6 6.4 %copy-start.13 = (f32[8]{0:T(128)S(1)}, f32[8]{0:T(128)}, u32[]{:S(2)}) copy-start(f32[8]{0:T(128)} %param.26) | copy-start | bytes 100
  22.7 6.5 %copy-start.14 = (f32[16,2,4,1024]{3,2,1,0:T(4,128)S(1)}, f32[16,2,4,1024]{3,2,1,0:T(4,128)}, u32[]{:S(2)}) copy-start(f32[16,2,4,1024]{3,2,1,0:T(4,128)} %get-tuple-element.4) | copy-start | bytes 1572868
  29.1 3.5 %copy-start.2 = (bf16[16,2048]{1,0:T(8,128)(2,1)S(1)}, bf16[16,2048]{1,0:T(8,128)(2,1)}, u32[]{:S(2)}) copy-start(bf16[16,2048]{1,0:T(8,128)(2,1)} %param.20) | copy-start | bytes 196612
  32.6 2.2 %copy-start.7 = (f32[2048]{0:T(1024)S(1)}, f32[2048]{0:T(1024)}, u32[]{:S(2)}) copy-start(f32[2048]{0:T(1024)} %param.30) | copy-start | bytes 24580
  32.6 4.8 %copy-start.8 = (s32[16,4]{0,1:T(4,128)S(1)}, s32[16,4]{0,1:T(4,128)}, u32[]{:S(2)}) copy-start(s32[16,4]{0,1:T(4,128)} %param.31) | copy-start | bytes 772
  32.7 14.5 %copy-start.12 = (f32[2048]{0:T(1024)S(1)}, f32[2048]{0:T(1024)}, u32[]{:S(2)}) copy-start(f32[2048]{0:T(1024)} %param.39) | copy-start | bytes 24580
  35.5 11.7 %copy-start.3 = (bf16[16,2048]{1,0:T(8,128)(2,1)S(1)}, bf16[16,2048]{1,0:T(8,128)(2,1)}, u32[]{:S(2)}) copy-start(bf16[16,2048]{1,0:T(8,128)(2,1)} %multiply_convert_fusion) | copy-start | bytes 196612
  35.5 139.8 %all-gather.5.cloned.1.call-start = ((), (), s32[]{:S(2)}) async-start(), calls=%async_computation.4 | async-start | bytes 8650752 | tf_op jit(solution)/shard_map/all_gather | solution.py:143
  39.8 19.1 %all-to-all-start = ((bf16[32,2,2048]{2,1,0:T(2,128)(2,1)}), bf16[32,2,2048]{2,1,0:T(2,128)(2,1)S(1)}, u32[]{:S(2)}, u32[]{:S(2)}) async-start(bf16[32,2,2048]{2,1,0:T(2,128)(2,1)} %reshape.122), calls=%async_computation | async-start | bytes 524288 | tf_op jit(solution)/shard_map/all_to_all | solution.py:123
  61.1 6.1 %copy-start.9 = (f32[16,4]{0,1:T(4,128)S(1)}, f32[16,4]{0,1:T(4,128)}, u32[]{:S(2)}) copy-start(f32[16,4]{0,1:T(4,128)} %param.32) | copy-start | bytes 772
  61.1 6.2 %copy-start.4 = (bf16[2048,128]{1,0:T(8,128)(2,1)S(1)}, bf16[2048,128]{1,0:T(8,128)(2,1)}, u32[]{:S(2)}) copy-start(bf16[2048,128]{1,0:T(8,128)(2,1)} %param.25) | copy-start | bytes 1572868
  61.1 6.2 %copy-start.6 = (f32[2048]{0:T(1024)S(1)}, f32[2048]{0:T(1024)}, u32[]{:S(2)}) copy-start(f32[2048]{0:T(1024)} %param.22) | copy-start | bytes 24580
  64.6 14.6 %all-to-all-start.1 = ((bf16[32,2,2048]{2,1,0:T(2,128)(2,1)}), bf16[32,2,2048]{2,1,0:T(2,128)(2,1)S(1)}, u32[]{:S(2)}, u32[]{:S(2)}) async-start(bf16[32,2,2048]{2,1,0:T(2,128)(2,1)} %reshape.124), calls=%async_computation.1 | async-start | bytes 524288 | tf_op jit(solution)/shard_map/all_to_all | solution.py:131
  68.1 28.5 %copy-start.5 = (bf16[2048,64]{0,1:T(8,128)(2,1)S(1)}, bf16[2048,64]{0,1:T(8,128)(2,1)}, u32[]{:S(2)}) copy-start(bf16[2048,64]{0,1:T(8,128)(2,1)} %param.36) | copy-start | bytes 786436
  80.0 19.1 %copy-start.11 = (bf16[2048,64]{0,1:T(8,128)(2,1)S(1)}, bf16[2048,64]{0,1:T(8,128)(2,1)}, u32[]{:S(2)}) copy-start(bf16[2048,64]{0,1:T(8,128)(2,1)} %param.37) | copy-start | bytes 786436
  96.6 2.5 %copy-start.1 = (bf16[512,2048]{1,0:T(8,128)(2,1)S(1)}, bf16[512,2048]{1,0:T(8,128)(2,1)}, u32[]{:S(2)}) copy-start(bf16[512,2048]{1,0:T(8,128)(2,1)} %all-gather.3.cloned.1.call-done) | copy-start | bytes 6291460
  100.8 11.0 %all-to-all-start.2 = ((bf16[32,2,512]{2,1,0:T(2,128)(2,1)}), bf16[32,2,512]{2,1,0:T(2,128)(2,1)S(1)}, u32[]{:S(2)}, u32[]{:S(2)}) async-start(bf16[32,2,512]{2,1,0:T(2,128)(2,1)} %reshape.149), calls=%async_computation.2 | async-start | bytes 131072 | tf_op jit(solution)/shard_map/all_to_all | solution.py:142
Sparse Core Ops, SparseCore 0:
  35.7 60.8 all-gather.2
  99.5 75.8 all-gather.4
where the time goes:
time: 188 us; the launch traced here: 187 us
  waiting for transfers between devices  108 us (57%)
  matrix products  28.3 us (15%)
  local copies, waits for them, and re-layouts  20.4 us (11%)
  between operations  14.4 us (8%)
  starting transfers between devices  13.4 us (7%)
  other arithmetic  2.76 us (1%)
    all_gather x1, waiting for transfers between devices, per_device(): full_down = lax.all_gather(dense_down, 'ep', axis=1, tiled=True)  63.3 us
    all_gather x1, waiting for transfers between devices, per_device(): lax.all_gather(ffn_in, 'ep', axis=0, tiled=True)  16.4 us
    unnamed x36, local copies, waits for them, and re-layouts  14 us
    all_to_all x1, waiting for transfers between devices, per_device(): lax.all_to_all(outgoing, 'ep', split_axis=0, concat_axis=0, tiled=True)  11.6 us
    all_to_all x1, waiting for transfers between devices, per_device(): lax.all_to_all(expert_rows.reshape(arrived.shape), 'ep', split_axis=0, co...  9.12 us
    all_to_all x1, starting transfers between devices, per_device(): lax.all_to_all(outgoing, 'ep', split_axis=0, concat_axis=0, tiled=True)  7.33 us
    all_to_all x1, waiting for transfers between devices, per_device(): lax.all_to_all(unit_hidden, 'ep', split_axis=0, concat_axis=1, tiled=True)  7.12 us
    dot_general x1, matrix products, down_product(): lax.dot_general(hidden_rows, down_w, (((1,), (1,)), ((), ())), preferred_...  5.21 us
  transfers between devices with their start and end apart: 5, of which 5 were waited for; matrix products, arithmetic and copies ran while one was open for 10% of the time, Pallas kernels for 0%

commit v1 on v0

v1 whole, which is shorter than its diff:
```python
import jax
import jax.numpy as jnp
from jax import lax
from jax.experimental import pallas as pl
from jax.experimental.pallas import tpu as pltpu
from jax.sharding import PartitionSpec as P

HEADS = 8
KV_HEADS = 2
HEAD = 64
TOP = 4
GROUP = HEADS // KV_HEADS
KV_WIDTH = KV_HEADS * HEAD
CHUNK = 256

norm_eps = 1e-06
bf16 = jnp.bfloat16
f32 = jnp.float32


def iota(shape, dim):
    return lax.broadcasted_iota(jnp.int32, shape, dim)


def matmul(left, right):
    return jnp.dot(left, right, preferred_element_type=f32)


def matmul_bt(left, right):
    return lax.dot_general(left, right, (((1,), (1,)), ((), ())), preferred_element_type=f32)


def matmul_at(left, right):
    return lax.dot_general(left, right, (((0,), (0,)), ((), ())), preferred_element_type=f32)


def rms_rows(values, gain):
    scale = lax.rsqrt(jnp.mean(values * values, axis=-1, keepdims=True) + norm_eps)
    return (values * scale * gain).astype(bf16)


def three_parts(values):
    high = values.astype(bf16)
    rest = values - high.astype(f32)
    middle = rest.astype(bf16)
    low = (rest - middle.astype(f32)).astype(bf16)
    return high, middle, low


def attend_kernel(
    capacity,
    lengths,
    score_bias,
    hidden,
    attn_gain,
    ffn_gain,
    branch_gate,
    routes_t,
    route_weights_t,
    query_hbm,
    key_hbm,
    value_hbm,
    keys_hbm,
    values_hbm,
    out_hbm,
    new_keys,
    new_values,
    middle,
    ffn_in,
    outgoing,
    combine,
    gate_value,
    query_w,
    key_w,
    value_w,
    keys,
    values,
    out_w,
    blocked,
    weights_t,
    weight_sems,
    key_sems,
    value_sems,
    out_sem,
):
    seqs = hidden.shape[0]
    cache_len = keys.shape[1]
    lanes = seqs * HEADS
    chunks = cache_len // CHUNK
    pairs = seqs // 2

    first = [
        pltpu.make_async_copy(query_hbm, query_w, weight_sems.at[0]),
        pltpu.make_async_copy(key_hbm, key_w, weight_sems.at[1]),
        pltpu.make_async_copy(value_hbm, value_w, weight_sems.at[2]),
    ]
    key_copies = [
        pltpu.make_async_copy(
            keys_hbm.at[:, pl.ds(c * CHUNK, CHUNK), :],
            keys.at[:, pl.ds(c * CHUNK, CHUNK), :],
            key_sems.at[c],
        )
        for c in range(chunks)
    ]
    value_copies = [
        pltpu.make_async_copy(
            values_hbm.at[pl.ds(p * 2, 2)], values.at[pl.ds(p * 2, 2)], value_sems.at[p]
        )
        for p in range(pairs)
    ]
    out_copy = pltpu.make_async_copy(out_hbm, out_w, out_sem)
    for copy in first:
        copy.start()
    for copy in reversed(key_copies):
        copy.start()
    for copy in value_copies:
        copy.start()
    out_copy.start()

    hidden_f = hidden[...].astype(f32)
    normed = rms_rows(hidden_f, attn_gain[...])

    lane = iota((1, lanes), 1)
    lane_len = jnp.zeros((1, lanes), jnp.int32)
    for n in range(seqs):
        lane_len = jnp.where(lane // HEADS == n, lengths[n], lane_len)
    lane_bias = jnp.zeros((1, lanes), f32)
    for h in range(HEADS):
        lane_bias = jnp.where(lane % HEADS == h, score_bias[h], lane_bias)

    spread = (iota((lanes, seqs), 0) // HEADS == iota((lanes, seqs), 1)).astype(bf16)
    gather = (iota((seqs, lanes), 1) // HEADS == iota((seqs, lanes), 0)).astype(bf16)
    wide = (lanes, HEADS * HEAD)
    own_head = iota(wide, 1) // HEAD == iota(wide, 0) % HEADS
    fold_shape = (HEADS * HEAD, KV_WIDTH)
    fold = (
        (iota(fold_shape, 0) // (HEAD * GROUP) == iota(fold_shape, 1) // HEAD)
        & (iota(fold_shape, 0) % HEAD == iota(fold_shape, 1) % HEAD)
    ).astype(bf16)
    later = (iota((CHUNK, CHUNK), 1) > iota((CHUNK, CHUNK), 0)).astype(bf16)

    for copy in first:
        copy.wait()
    queries = matmul(normed, query_w[...]).astype(bf16)
    new_keys[...] = matmul(normed, key_w[...]).astype(bf16)
    new_values[...] = matmul(normed, value_w[...]).astype(bf16)

    spread_q = jnp.where(own_head, matmul(spread, queries), 0.0).astype(bf16)
    by_head = jnp.transpose(matmul(spread_q, fold))
    square = (KV_WIDTH, lanes)
    for n in range(seqs):
        own_lane = iota(square, 1) // HEADS == n
        blocked[n * KV_WIDTH : (n + 1) * KV_WIDTH, :] = jnp.where(own_lane, by_head, 0.0).astype(
            bf16
        )

    carry = jnp.zeros((1, lanes), f32)
    for c in reversed(range(chunks)):
        key_copies[c].wait()
        rows = slice(c * CHUNK, (c + 1) * CHUNK)
        key_rows = jnp.concatenate([keys[n, rows, :] for n in range(seqs)], axis=1)
        scores = matmul(key_rows, blocked[...]) * HEAD ** (-0.5) + lane_bias
        live = iota((CHUNK, lanes), 0) + c * CHUNK < lane_len
        soft = jnp.log1p(jnp.exp(-jnp.abs(scores)))
        log_keep = jnp.where(live, jnp.minimum(-scores, 0.0) - soft, 0.0)
        log_take = jnp.minimum(scores, 0.0) - soft
        sums = matmul(later, jnp.concatenate(three_parts(log_keep), axis=1))
        after = sums[:, :lanes] + sums[:, lanes : 2 * lanes] + sums[:, 2 * lanes :] + carry
        carry = carry + jnp.sum(log_keep, axis=0, keepdims=True)
        taken = jnp.where(live, jnp.exp(log_take + after), 0.0)
        weights_t[:, rows] = jnp.transpose(taken).astype(bf16)

    pieces = []
    for p in range(pairs):
        value_copies[p].wait()
        value_rows = jnp.concatenate([values[2 * p], values[2 * p + 1]], axis=1)
        mixed = matmul(weights_t[2 * p * HEADS : 2 * (p + 1) * HEADS, :], value_rows)
        pieces.append(mixed[:HEADS, :KV_WIDTH])
        pieces.append(mixed[HEADS:, KV_WIDTH:])
    mixed = jnp.concatenate(pieces, axis=0)
    own_group = (iota(mixed.shape, 0) % HEADS) // GROUP == iota(mixed.shape, 1) // HEAD
    mixed = jnp.where(own_group, mixed, 0.0).astype(bf16)
    unfolded = jnp.where(own_head, matmul_bt(mixed, fold), 0.0).astype(bf16)
    attended = matmul(gather, unfolded).astype(bf16)

    out_copy.wait()
    middle_f = hidden_f + matmul(attended, out_w[...])
    middle[...] = middle_f
    ffn = rms_rows(middle_f, ffn_gain[...])
    ffn_in[...] = ffn
    gate_sum = jnp.sum(ffn.astype(f32) * branch_gate[...], axis=-1, keepdims=True)
    gate_value[...] = jnp.broadcast_to(jax.nn.sigmoid(gate_sum), gate_value.shape)

    slots = (outgoing.shape[0], seqs)
    expert = iota(slots, 0) // capacity
    named = jnp.zeros(slots, f32)
    weighted = jnp.zeros(slots, f32)
    for k in range(TOP):
        hit = expert == routes_t[k : k + 1, :]
        named = named + jnp.where(hit, 1.0, 0.0)
        weighted = weighted + jnp.where(hit, route_weights_t[k : k + 1, :], 0.0)
    earlier = (iota((seqs, seqs), 0) < iota((seqs, seqs), 1)).astype(bf16)
    rank = matmul(named.astype(bf16), earlier)
    mine = rank == (iota(slots, 0) % capacity).astype(f32)
    combine[...] = jnp.where(mine, weighted, 0.0)
    outgoing[...] = matmul(jnp.where(mine, named, 0.0).astype(bf16), ffn).astype(bf16)


def attend(capacity, slots, args):
    hidden = args[2]
    keys = args[11]
    seqs, width = hidden.shape
    cache_len = keys.shape[1]
    pairs = seqs // 2
    shapes = (
        jax.ShapeDtypeStruct((seqs, KV_WIDTH), bf16),
        jax.ShapeDtypeStruct((seqs, KV_WIDTH), bf16),
        jax.ShapeDtypeStruct((seqs, width), f32),
        jax.ShapeDtypeStruct((seqs, width), bf16),
        jax.ShapeDtypeStruct((slots, width), bf16),
        jax.ShapeDtypeStruct((slots, seqs), f32),
        jax.ShapeDtypeStruct((seqs, 128), f32),
    )
    smem = pl.BlockSpec(memory_space=pltpu.SMEM)
    vmem = pl.BlockSpec(memory_space=pltpu.VMEM)
    hbm = pl.BlockSpec(memory_space=pl.ANY)
    big = args[8:]
    return pl.pallas_call(
        lambda *refs: attend_kernel(capacity, *refs),
        out_shape=shapes,
        in_specs=[smem] * 2 + [vmem] * 6 + [hbm] * 6,
        out_specs=[vmem] * 7,
        scratch_shapes=[pltpu.VMEM(a.shape, a.dtype) for a in big]
        + [
            pltpu.VMEM((seqs * KV_WIDTH, seqs * HEADS), bf16),
            pltpu.VMEM((seqs * HEADS, cache_len), bf16),
            pltpu.SemaphoreType.DMA((3,)),
            pltpu.SemaphoreType.DMA((cache_len // CHUNK,)),
            pltpu.SemaphoreType.DMA((pairs,)),
            pltpu.SemaphoreType.DMA,
        ],
        compiler_params=pltpu.CompilerParams(vmem_limit_bytes=40 << 20),
        name="attend",
    )(*args)


def per_device(
    hidden_in,
    lengths,
    attn_gain,
    query_weight,
    key_weight,
    value_weight,
    score_bias,
    out_weight,
    key_cache,
    value_cache,
    ffn_gain,
    routes,
    route_weights,
    expert_gate,
    expert_up,
    expert_down,
    dense_gate,
    dense_up,
    dense_down,
    branch_gate,
):
    seqs, width = hidden_in.shape
    devices = lax.axis_size("ep")
    local_experts = expert_gate.shape[0]
    experts_all = local_experts * devices
    capacity = max(1, seqs * TOP // experts_all)
    slots = experts_all * capacity
    layers = 1
    while 2 * (2 * layers) ** 2 <= devices and devices % (4 * layers) == 0:
        layers = 2 * layers
    plane = devices // layers
    units = dense_gate.shape[1]

    def swap(values, bits):
        return lax.ppermute(values, "ep", [(i, i ^ bits) for i in range(devices)])

    def climb(values, steps):
        return lax.ppermute(
            values, "ep", [(i, (i + steps * plane) % devices) for i in range(devices)]
        )

    own_dense = jnp.concatenate([dense_gate.T, dense_up.T, dense_down.T], axis=0)
    dense_parts = [own_dense]
    for other in range(2, plane, 2):
        dense_parts.append(swap(own_dense, other))

    new_keys, new_values, middle, ffn_in, outgoing, combine, gate_value = attend(
        capacity,
        slots,
        (
            lengths,
            score_bias,
            hidden_in,
            attn_gain.reshape(1, width),
            ffn_gain.reshape(1, width),
            branch_gate.reshape(1, width),
            routes.T,
            route_weights.T,
            query_weight,
            key_weight,
            value_weight,
            key_cache,
            value_cache,
            out_weight,
        ),
    )

    outgoing = outgoing.reshape(devices, local_experts * capacity, width)
    arrived = lax.all_to_all(outgoing, "ep", split_axis=0, concat_axis=0, tiled=True)
    chain = [ffn_in] + [climb(ffn_in, k) for k in range(1, layers)]
    chain = jnp.concatenate(chain, axis=0)
    chain = jnp.concatenate([chain, swap(chain, 1)], axis=0)

    flat_in = arrived.reshape(-1, width)
    gate_pre = matmul(flat_in, expert_gate[0])
    up_pre = matmul(flat_in, expert_up[0])
    hidden_act = (jax.nn.silu(gate_pre) * up_pre).astype(bf16)
    expert_rows = matmul(hidden_act, expert_down[0]).astype(bf16)
    returned = lax.all_to_all(
        expert_rows.reshape(arrived.shape), "ep", split_axis=0, concat_axis=0, tiled=True
    ).reshape(slots, width)

    gates = jnp.concatenate([part[:units] for part in dense_parts], axis=0)
    ups = jnp.concatenate([part[units : 2 * units] for part in dense_parts], axis=0)
    downs = jnp.concatenate([part[2 * units :] for part in dense_parts], axis=0)
    dense_hidden = (
        jax.nn.silu(matmul_bt(chain, gates)) * matmul_bt(chain, ups)
    ).astype(bf16)
    partial = matmul(dense_hidden, downs)
    half = layers * seqs
    summed = partial[:half] + swap(partial[half:].astype(bf16), 1).astype(f32)
    dense_out = summed[:seqs]
    for k in range(1, layers):
        piece = summed[k * seqs : (k + 1) * seqs].astype(bf16)
        dense_out = dense_out + climb(piece, -k).astype(f32)

    expert_sum = lax.dot_general(
        combine,
        returned.astype(f32),
        (((0,), (0,)), ((), ())),
        precision=lax.Precision.HIGHEST,
        preferred_element_type=f32,
    )
    hidden_out = (middle + expert_sum + gate_value[:, :1] * dense_out).astype(bf16)
    return (hidden_out, new_keys, new_values)


def solution(mesh):
    return jax.shard_map(
        per_device,
        mesh=mesh,
        in_specs=(
            P("ep", None),
            P("ep"),
            P(),
            P(),
            P(),
            P(),
            P(),
            P(),
            P("ep", None, None),
            P("ep", None, None),
            P(),
            P("ep", None),
            P("ep", None),
            P("ep", None, None),
            P("ep", None, None),
            P("ep", None, None),
            P(None, "ep"),
            P(None, "ep"),
            P(None, "ep"),
            P(),
        ),
        out_specs=(P("ep", None), P("ep", None), P("ep", None)),
        check_vma=False,
    )
```

time: 188 us -> 86.3 us (0.46)
  waiting for transfers between devices: 108 us -> 11.3 us
  matrix products: 28.3 us -> 9.81 us
  between operations: 14.4 us -> 0.82 us
  starting transfers between devices: 13.4 us -> 22.7 us
  Pallas kernels: 0 us -> 9.07 us
  local copies, waits for them, and re-layouts: 20.4 us -> 27.5 us
    all_gather x2 -> x0, waiting for transfers between devices: 79.6 us -> none  [the longest x1 63.3 us: per_device(): full_down = lax.all_gather(dense_down, 'ep', axis=1, tiled=True)]
    dot_general x14 -> x5, matrix products: 28.3 us -> 9.81 us  [the longest x3 7.94 us: matmul(): return jnp.dot(left, right, preferred_element_type=f32)]
    ppermute x0 -> x11, starting transfers between devices: none -> 17.5 us  [the longest x6 11.3 us: climb(): lax.ppermute(values, 'ep', [(i, (i + steps * plane) % devices) for i in r...]
    all_to_all x1, waiting for transfers between devices: 9.12 us -> 0.01 us  [per_device(): lax.all_to_all(expert_rows.reshape(arrived.shape), 'ep', split_axis=0, co...]
    pallas_call x0 -> x1, Pallas kernels: none -> 9.07 us  [attend(): pl.pallas_call(lambda *refs: attend_kernel(capacity, *refs), out_shape=sh...]
    all_to_all x1 -> x0, waiting for transfers between devices: 7.12 us -> none  [per_device(): lax.all_to_all(unit_hidden, 'ep', split_axis=0, concat_axis=1, tiled=True)]
    slice x0 -> x6, local copies, waits for them, and re-layouts: none -> 7.11 us  [the longest x3 5.91 us: per_device(): part[units:2 * units]]
    all_to_all x1, waiting for transfers between devices: 11.6 us -> 5.61 us  [per_device(): lax.all_to_all(outgoing, 'ep', split_axis=0, concat_axis=0, tiled=True)]
  transfers between devices with their start and end apart: 5 -> 13, of which waited for: 5 -> 6; matrix products, arithmetic and copies ran while one was open for 10% -> 26% of each run, Pallas kernels for 0% -> 11%
where the time goes in v1:
time: 86.3 us; the launch traced here: 85.3 us
  local copies, waits for them, and re-layouts  27.5 us (32%)
  starting transfers between devices  22.7 us (26%)
  waiting for transfers between devices  11.3 us (13%)
  matrix products  9.81 us (11%)
  Pallas kernels  9.07 us (11%)
  other arithmetic  4.06 us (5%)
    unnamed x40, local copies, waits for them, and re-layouts  17.8 us
    ppermute x6, starting transfers between devices, climb(): lax.ppermute(values, 'ep', [(i, (i + steps * plane) % devices) for i in r...  11.3 us
    pallas_call x1, Pallas kernels, attend(): pl.pallas_call(lambda *refs: attend_kernel(capacity, *refs), out_shape=sh...  9.07 us
    dot_general x3, matrix products, matmul(): return jnp.dot(left, right, preferred_element_type=f32)  7.94 us
    ppermute x5, starting transfers between devices, swap(): return lax.ppermute(values, 'ep', [(i, i ^ bits) for i in range(devices)])  6.21 us
    slice x3, local copies, waits for them, and re-layouts, per_device(): part[units:2 * units]  5.91 us
    all_to_all x1, waiting for transfers between devices, per_device(): lax.all_to_all(outgoing, 'ep', split_axis=0, concat_axis=0, tiled=True)  5.61 us
    ppermute x6, waiting for transfers between devices, climb(): lax.ppermute(values, 'ep', [(i, (i + steps * plane) % devices) for i in r...  3.68 us
  transfers between devices with their start and end apart: 13, of which 6 were waited for; matrix products, arithmetic and copies ran while one was open for 26% of the time, Pallas kernels for 11%

profile of v1, /device:TPU:0, one launch (start us, length us, event | category | flops | bytes accessed | tf_op | source)
XLA Modules:
  0.0 85.3 jit_solution(12652583606138717254)
XLA Ops:
  0.6 2.2 %pad_maximum_fusion = bf16[192,2048]{1,0:T(8,128)(2,1)} fusion(bf16[64,2048]{1,0:T(8,128)(2,1)} %bitcast.36, bf16[64,2048]{1,0:T(8,128)(2,1)} %bitcast.38, bf16[64,2048]{1,0:T(8,128)(2,1)} %bitcast.34), kind=kLoop, calls=%fused_computation.33 | loop fusion | flops 2359296 | bytes 1572864 | tf_op jit(solution)/shard_map/concatenate | solution.py:289
  2.9 3.9 %collective-permute-start.6 = (bf16[192,2048]{1,0:T(8,128)(2,1)}, bf16[192,2048]{1,0:T(8,128)(2,1)}, u32[]{:S(2)}, u32[]{:S(2)}) collective-permute-start(bf16[192,2048]{1,0:T(8,128)(2,1)} %pad_maximum_fusion), channel_id=1, source_target_pairs={{0,6},{1,7},{2,4},{3,5},{4,2},{5,3},{6,0},{7,1},{8,14},{9,15},{10,... | collective-permute-start | bytes 2359304 | tf_op jit(solution)/shard_map/ppermute | solution.py:282
  7.3 2.2 %copy-done.1 = bf16[16,1024,128]{2,1,0:T(8,128)(2,1)S(1)} copy-done((bf16[16,1024,128]{2,1,0:T(8,128)(2,1)S(1)}, bf16[16,1024,128]{2,1,0:T(8,128)(2,1)}, u32[]{:S(2)}) %copy-start.1) | copy-done | bytes 4194328
  9.5 2.2 %copy-done.2 = bf16[16,1024,128]{2,1,0:T(8,128)(2,1)S(1)} copy-done((bf16[16,1024,128]{2,1,0:T(8,128)(2,1)S(1)}, bf16[16,1024,128]{2,1,0:T(8,128)(2,1)}, u32[]{:S(2)}) %copy-start.2) | copy-done | bytes 4194328
  11.7 1.6 %copy-done.3 = bf16[2048,512]{1,0:T(8,128)(2,1)S(1)} copy-done((bf16[2048,512]{1,0:T(8,128)(2,1)S(1)}, bf16[2048,512]{1,0:T(8,128)(2,1)}, u32[]{:S(2)}) %copy-start.3) | copy-done | bytes 2097176
  13.3 1.6 %copy-done.4 = bf16[512,2048]{1,0:T(8,128)(2,1)S(1)} copy-done((bf16[512,2048]{1,0:T(8,128)(2,1)S(1)}, bf16[512,2048]{1,0:T(8,128)(2,1)}, u32[]{:S(2)}) %copy-start.4) | copy-done | bytes 2097176
  22.5 9.1 %attend.1 = (bf16[16,128]{1,0:T(8,128)(2,1)}, bf16[16,128]{1,0:T(8,128)(2,1)}, f32[16,2048]{1,0:T(8,128)S(1)}, bf16[16,2048]{1,0:T(8,128)(2,1)S(1)}, bf16[64,204...) custom-call(s32[16]{0:T(128)S(1)} %copy-done.13, f32[8]{0:T(128)S(1)} %copy-done.14, ...), custom_call_target="tpu_custom_call" | custom-call | tf_op jit(solution)/shard_map/attend/pallas_call | solution.py:228
  31.6 1.6 %collective-permute-start = (bf16[16,2048]{1,0:T(8,128)(2,1)S(1)}, bf16[16,2048]{1,0:T(8,128)(2,1)S(1)}, u32[]{:S(2)}, u32[]{:S(2)}) collective-permute-start(bf16[16,2048]{1,0:T(8,128)(2,1)S(1)} %get-tuple-element.14), channel_id=1, source_target_pairs={{0,8},{1,9},{2,10},{3,11},{4,12},{5,13},{6,14},{7,15},{8,16},{9,17... | collective-permute-start | bytes 196616 | tf_op jit(solution)/shard_map/ppermute | solution.py:285
  33.3 2.6 %collective-permute-start.1 = (bf16[16,2048]{1,0:T(8,128)(2,1)S(1)}, bf16[16,2048]{1,0:T(8,128)(2,1)S(1)}, u32[]{:S(2)}, u32[]{:S(2)}) collective-permute-start(bf16[16,2048]{1,0:T(8,128)(2,1)S(1)} %get-tuple-element.14), channel_id=1, source_target_pairs={{0,16},{1,17},{2,18},{3,19},{4,20},{5,21},{6,22},{7,23},{8,24},{9,... | collective-permute-start | bytes 196616 | tf_op jit(solution)/shard_map/ppermute | solution.py:285
  35.9 1.3 %collective-permute-start.2 = (bf16[16,2048]{1,0:T(8,128)(2,1)S(1)}, bf16[16,2048]{1,0:T(8,128)(2,1)S(1)}, u32[]{:S(2)}, u32[]{:S(2)}) collective-permute-start(bf16[16,2048]{1,0:T(8,128)(2,1)S(1)} %get-tuple-element.14), channel_id=1, source_target_pairs={{0,24},{1,25},{2,26},{3,27},{4,28},{5,29},{6,30},{7,31},{8,0},{9,1... | collective-permute-start | bytes 196616 | tf_op jit(solution)/shard_map/ppermute | solution.py:285
  38.1 2.6 %all-to-all-start = ((bf16[32,2,2048]{2,1,0:T(2,128)(2,1)}), bf16[32,2,2048]{2,1,0:T(2,128)(2,1)S(1)}, u32[]{:S(2)}, u32[]{:S(2)}) async-start(bf16[32,2,2048]{2,1,0:T(2,128)(2,1)} %reshape.30), calls=%async_computation | async-start | bytes 524288 | tf_op jit(solution)/shard_map/all_to_all | solution.py:316
  41.3 1.6 %collective-permute-start.4 = (bf16[192,2048]{1,0:T(8,128)(2,1)}, bf16[192,2048]{1,0:T(8,128)(2,1)}, u32[]{:S(2)}, u32[]{:S(2)}) collective-permute-start(bf16[192,2048]{1,0:T(8,128)(2,1)} %pad_maximum_fusion), channel_id=1, source_target_pairs={{0,2},{1,3},{2,0},{3,1},{4,6},{5,7},{6,4},{7,5},{8,10},{9,11},{10,... | collective-permute-start | bytes 2359304 | tf_op jit(solution)/shard_map/ppermute | solution.py:282
  45.6 5.6 %all-to-all-done = bf16[32,2,2048]{2,1,0:T(2,128)(2,1)S(1)} async-done(((bf16[32,2,2048]{2,1,0:T(2,128)(2,1)}), bf16[32,2,2048]{2,1,0:T(2,128)(2,1)S(1)}, u32[]{:S(2)}, u32[]{:S(2)}) %all-to-all-start) | async-done | bytes 262176 | tf_op jit(solution)/shard_map/all_to_all | solution.py:316
  51.4 2.1 %fusion.3 = f32[64,512]{1,0:T(8,128)S(1)} fusion(bf16[64,2048]{1,0:T(8,128)(2,1)S(1)} %reshape.31, bf16[1,2048,512]{2,1,0:T(8,128)(2,1)} %param.33), kind=kOutput, calls=%fused_computation.5 | convolution fusion | flops 134217728 | bytes 2490368 | tf_op jit(solution)/shard_map/dot_general | solution.py:26
  53.4 2.5 %convolution_convert_fusion = bf16[64,2048]{1,0:T(8,128)(2,1)S(1)} fusion(bf16[1,512,2048]{2,1,0:T(8,128)(2,1)S(1)} %copy-done, bf16[64,2048]{1,0:T(8,128)(2,1)S(1)} %reshape.31, bf16[1,2048,512]{2,1,0:T(8,128)(2,1)} %param.34, f32[64,512]{1,0:T(8,128)S(1)} %fusion.3), kind=kOutput, calls=%fused_computation | convolution fusion | flops 268763136 | bytes 4849664 | tf_op jit(solution)/shard_map/dot_general | solution.py:26
  56.8 2.6 %all-to-all-start.1 = ((bf16[32,2,2048]{2,1,0:T(2,128)(2,1)}), bf16[32,2,2048]{2,1,0:T(2,128)(2,1)S(1)}, u32[]{:S(2)}, u32[]{:S(2)}) async-start(bf16[32,2,2048]{2,1,0:T(2,128)(2,1)} %reshape.32), calls=%async_computation.1 | async-start | bytes 524288 | tf_op jit(solution)/shard_map/all_to_all | solution.py:326
  59.4 1.9 %fusion.61 = (bf16[64,2048]{1,0:T(8,128)(2,1)S(1)}, bf16[64,2048]{1,0:T(8,128)(2,1)}, bf16[64,2048]{1,0:T(8,128)(2,1)S(1)}) fusion(bf16[192,2048]{1,0:T(8,128)(2,1)} %collective-permute-done.6), kind=kLoop, calls=%fused_computation.64 | loop fusion | bytes 1572864 | tf_op jit(solution)/shard_map/slice | solution.py:331
  61.4 2.0 %fusion.60 = (bf16[64,2048]{1,0:T(8,128)(2,1)}, bf16[64,2048]{1,0:T(8,128)(2,1)}, bf16[64,2048]{1,0:T(8,128)(2,1)S(1)}) fusion(bf16[192,2048]{1,0:T(8,128)(2,1)} %collective-permute-done.5), kind=kLoop, calls=%fused_computation.63 | loop fusion | bytes 1572864 | tf_op jit(solution)/shard_map/slice | solution.py:331
  64.1 2.0 %fusion.59 = (bf16[64,2048]{1,0:T(8,128)(2,1)}, bf16[64,2048]{1,0:T(8,128)(2,1)}, bf16[64,2048]{1,0:T(8,128)(2,1)S(1)}) fusion(bf16[192,2048]{1,0:T(8,128)(2,1)} %collective-permute-done.4), kind=kLoop, calls=%fused_computation.62 | loop fusion | bytes 1572864 | tf_op jit(solution)/shard_map/slice | solution.py:331
  66.1 1.6 %fusion.13 = f32[128,256]{1,0:T(8,128)S(1)} fusion(bf16[128,2048]{1,0:T(8,128)(2,1)} %constant_dynamic-update-slice_fusion, bf16[64,2048]{1,0:T(8,128)(2,1)S(1)} %get-tuple-element.27, bf16[64,2048]{1,0:T(8,128)(2,1)S(1)} %get-tuple-element.24, bf16[64,2048]{1,0:T(8,128)(2,1)S(1)} %get-tuple-element.21, bf16[64,2048]{1,0:T(8,128)(2,1)S(1)} %bitcast.35), kind=kOutput, calls=%fused_computation.9 | convolution fusion | flops 138412032 | bytes 1703936 | tf_op jit(solution)/shard_map/dot_general | solution.py:30
  67.7 3.4 %fusion.29 = f32[128,2048]{1,0:T(8,128)} fusion(bf16[64,2048]{1,0:T(8,128)(2,1)} %get-tuple-element.26, bf16[64,2048]{1,0:T(8,128)(2,1)} %get-tuple-element.23, bf16[64,2048]{1,0:T(8,128)(2,1)} %get-tuple-element.20, bf16[64,2048]{1,0:T(8,128)(2,1)S(1)} %bitcast.37, f32[128,256]{1,0:T(8,128)S(1)} %fusion.13, ...), kind=kOutput, calls=%fused_computation.25 | convolution fusion | flops 277020672 | bytes 3801088 | tf_op jit(solution)/shard_map/dot_general | solution.py:26
  74.9 1.6 %collective-permute-start.10 = (bf16[16,2048]{1,0:T(8,128)(2,1)S(1)}, bf16[16,2048]{1,0:T(8,128)(2,1)S(1)}, u32[]{:S(2)}, u32[]{:S(2)}) collective-permute-start(bf16[16,2048]{1,0:T(8,128)(2,1)S(1)} %get-tuple-element.29), channel_id=1, source_target_pairs={{0,8},{1,9},{2,10},{3,11},{4,12},{5,13},{6,14},{7,15},{8,16},{9,17... | collective-permute-start | bytes 196616 | tf_op jit(solution)/shard_map/ppermute | solution.py:285
  76.5 3.0 %collective-permute-start.9 = (bf16[16,2048]{1,0:T(8,128)(2,1)S(1)}, bf16[16,2048]{1,0:T(8,128)(2,1)S(1)}, u32[]{:S(2)}, u32[]{:S(2)}) collective-permute-start(bf16[16,2048]{1,0:T(8,128)(2,1)S(1)} %get-tuple-element.30), channel_id=1, source_target_pairs={{0,16},{1,17},{2,18},{3,19},{4,20},{5,21},{6,22},{7,23},{8,24},{9,... | collective-permute-start | bytes 196616 | tf_op jit(solution)/shard_map/ppermute | solution.py:285
  81.7 2.5 %collective-permute-done.9 = bf16[16,2048]{1,0:T(8,128)(2,1)S(1)} collective-permute-done((bf16[16,2048]{1,0:T(8,128)(2,1)S(1)}, bf16[16,2048]{1,0:T(8,128)(2,1)S(1)}, u32[]{:S(2)}, u32[]{:S(2)}) %collective-permute-start.9) | collective-permute-done | bytes 65568 | tf_op jit(solution)/shard_map/ppermute | solution.py:285
  (63 shorter events, 21.2 us)
Async XLA Ops:
  0.6 52.8 %copy-start = (bf16[1,512,2048]{2,1,0:T(8,128)(2,1)S(1)}, bf16[1,512,2048]{2,1,0:T(8,128)(2,1)}, u32[]{:S(2)}) copy-start(bf16[1,512,2048]{2,1,0:T(8,128)(2,1)} %param.35) | copy-start | bytes 6291460
  2.9 56.6 %collective-permute-start.6 = (bf16[192,2048]{1,0:T(8,128)(2,1)}, bf16[192,2048]{1,0:T(8,128)(2,1)}, u32[]{:S(2)}, u32[]{:S(2)}) collective-permute-start(bf16[192,2048]{1,0:T(8,128)(2,1)} %pad_maximum_fusion), channel_id=1, source_target_pairs={{0,6},{1,7},{2,4},{3,5},{4,2},{5,3},{6,0},{7,1},{8,14},{9,15},{10,... | collective-permute-start | bytes 2359304 | tf_op jit(solution)/shard_map/ppermute | solution.py:282
  6.8 54.6 %collective-permute-start.5 = (bf16[192,2048]{1,0:T(8,128)(2,1)}, bf16[192,2048]{1,0:T(8,128)(2,1)}, u32[]{:S(2)}, u32[]{:S(2)}) collective-permute-start(bf16[192,2048]{1,0:T(8,128)(2,1)} %pad_maximum_fusion), channel_id=1, source_target_pairs={{0,4},{1,5},{2,6},{3,7},{4,0},{5,1},{6,2},{7,3},{8,12},{9,13},{10,... | collective-permute-start | bytes 2359304 | tf_op jit(solution)/shard_map/ppermute | solution.py:282
  7.3 2.2 %copy-start.1 = (bf16[16,1024,128]{2,1,0:T(8,128)(2,1)S(1)}, bf16[16,1024,128]{2,1,0:T(8,128)(2,1)}, u32[]{:S(2)}) copy-start(bf16[16,1024,128]{2,1,0:T(8,128)(2,1)} %refs_11_.1) | copy-start | bytes 12582916
  9.5 2.2 %copy-start.2 = (bf16[16,1024,128]{2,1,0:T(8,128)(2,1)S(1)}, bf16[16,1024,128]{2,1,0:T(8,128)(2,1)}, u32[]{:S(2)}) copy-start(bf16[16,1024,128]{2,1,0:T(8,128)(2,1)} %refs_12_.1) | copy-start | bytes 12582916
  11.7 1.6 %copy-start.3 = (bf16[2048,512]{1,0:T(8,128)(2,1)S(1)}, bf16[2048,512]{1,0:T(8,128)(2,1)}, u32[]{:S(2)}) copy-start(bf16[2048,512]{1,0:T(8,128)(2,1)} %refs_8_.1) | copy-start | bytes 6291460
  13.3 1.6 %copy-start.4 = (bf16[512,2048]{1,0:T(8,128)(2,1)S(1)}, bf16[512,2048]{1,0:T(8,128)(2,1)}, u32[]{:S(2)}) copy-start(bf16[512,2048]{1,0:T(8,128)(2,1)} %refs_13_.1) | copy-start | bytes 6291460
  14.9 1.0 %copy-start.5 = (bf16[2048,128]{1,0:T(8,128)(2,1)S(1)}, bf16[2048,128]{1,0:T(8,128)(2,1)}, u32[]{:S(2)}) copy-start(bf16[2048,128]{1,0:T(8,128)(2,1)} %refs_9_.1) | copy-start | bytes 1572868
  15.9 1.0 %copy-start.6 = (bf16[2048,128]{1,0:T(8,128)(2,1)S(1)}, bf16[2048,128]{1,0:T(8,128)(2,1)}, u32[]{:S(2)}) copy-start(bf16[2048,128]{1,0:T(8,128)(2,1)} %refs_10_.1) | copy-start | bytes 1572868
  16.9 0.8 copy-start.7
  31.6 9.7 %collective-permute-start = (bf16[16,2048]{1,0:T(8,128)(2,1)S(1)}, bf16[16,2048]{1,0:T(8,128)(2,1)S(1)}, u32[]{:S(2)}, u32[]{:S(2)}) collective-permute-start(bf16[16,2048]{1,0:T(8,128)(2,1)S(1)} %get-tuple-element.14), channel_id=1, source_target_pairs={{0,8},{1,9},{2,10},{3,11},{4,12},{5,13},{6,14},{7,15},{8,16},{9,17... | collective-permute-start | bytes 196616 | tf_op jit(solution)/shard_map/ppermute | solution.py:285
  33.3 9.7 %collective-permute-start.1 = (bf16[16,2048]{1,0:T(8,128)(2,1)S(1)}, bf16[16,2048]{1,0:T(8,128)(2,1)S(1)}, u32[]{:S(2)}, u32[]{:S(2)}) collective-permute-start(bf16[16,2048]{1,0:T(8,128)(2,1)S(1)} %get-tuple-element.14), channel_id=1, source_target_pairs={{0,16},{1,17},{2,18},{3,19},{4,20},{5,21},{6,22},{7,23},{8,24},{9,... | collective-permute-start | bytes 196616 | tf_op jit(solution)/shard_map/ppermute | solution.py:285
  35.9 7.1 %collective-permute-start.2 = (bf16[16,2048]{1,0:T(8,128)(2,1)S(1)}, bf16[16,2048]{1,0:T(8,128)(2,1)S(1)}, u32[]{:S(2)}, u32[]{:S(2)}) collective-permute-start(bf16[16,2048]{1,0:T(8,128)(2,1)S(1)} %get-tuple-element.14), channel_id=1, source_target_pairs={{0,24},{1,25},{2,26},{3,27},{4,28},{5,29},{6,30},{7,31},{8,0},{9,1... | collective-permute-start | bytes 196616 | tf_op jit(solution)/shard_map/ppermute | solution.py:285
  38.1 13.2 %all-to-all-start = ((bf16[32,2,2048]{2,1,0:T(2,128)(2,1)}), bf16[32,2,2048]{2,1,0:T(2,128)(2,1)S(1)}, u32[]{:S(2)}, u32[]{:S(2)}) async-start(bf16[32,2,2048]{2,1,0:T(2,128)(2,1)} %reshape.30), calls=%async_computation | async-start | bytes 524288 | tf_op jit(solution)/shard_map/all_to_all | solution.py:316
  41.3 22.8 %collective-permute-start.4 = (bf16[192,2048]{1,0:T(8,128)(2,1)}, bf16[192,2048]{1,0:T(8,128)(2,1)}, u32[]{:S(2)}, u32[]{:S(2)}) collective-permute-start(bf16[192,2048]{1,0:T(8,128)(2,1)} %pad_maximum_fusion), channel_id=1, source_target_pairs={{0,2},{1,3},{2,0},{3,1},{4,6},{5,7},{6,4},{7,5},{8,10},{9,11},{10,... | collective-permute-start | bytes 2359304 | tf_op jit(solution)/shard_map/ppermute | solution.py:282
  43.0 1.9 %collective-permute-start.3 = (bf16[64,2048]{1,0:T(8,128)(2,1)S(1)}, bf16[64,2048]{1,0:T(8,128)(2,1)S(1)}, u32[]{:S(2)}, u32[]{:S(2)}) collective-permute-start(bf16[64,2048]{1,0:T(8,128)(2,1)S(1)} %pad_maximum_fusion.1), channel_id=1, source_target_pairs={{0,1},{1,0},{2,3},{3,2},{4,5},{5,4},{6,7},{7,6},{8,9},{9,8},{10,11... | collective-permute-start | bytes 786440 | tf_op jit(solution)/shard_map/ppermute | solution.py:282
  56.8 15.5 %all-to-all-start.1 = ((bf16[32,2,2048]{2,1,0:T(2,128)(2,1)}), bf16[32,2,2048]{2,1,0:T(2,128)(2,1)S(1)}, u32[]{:S(2)}, u32[]{:S(2)}) async-start(bf16[32,2,2048]{2,1,0:T(2,128)(2,1)} %reshape.32), calls=%async_computation.1 | async-start | bytes 524288 | tf_op jit(solution)/shard_map/all_to_all | solution.py:326
  59.4 6.6 %copy-start.15 = (bf16[2048,64]{0,1:T(8,128)(2,1)S(1)}, bf16[2048,64]{0,1:T(8,128)(2,1)}, u32[]{:S(2)}) copy-start(bf16[2048,64]{0,1:T(8,128)(2,1)} %param.36) | copy-start | bytes 786436
  66.1 1.6 %copy-start.16 = (bf16[2048,64]{0,1:T(8,128)(2,1)S(1)}, bf16[2048,64]{0,1:T(8,128)(2,1)}, u32[]{:S(2)}) copy-start(bf16[2048,64]{0,1:T(8,128)(2,1)} %param.38) | copy-start | bytes 786436
  66.1 1.6 %copy-start.17 = (bf16[2048,64]{0,1:T(8,128)(2,1)S(1)}, bf16[2048,64]{0,1:T(8,128)(2,1)}, u32[]{:S(2)}) copy-start(bf16[2048,64]{0,1:T(8,128)(2,1)} %param.37) | copy-start | bytes 786436
  72.1 1.6 %collective-permute-start.7 = (bf16[64,2048]{1,0:T(8,128)(2,1)S(1)}, bf16[64,2048]{1,0:T(8,128)(2,1)S(1)}, u32[]{:S(2)}, u32[]{:S(2)}) collective-permute-start(bf16[64,2048]{1,0:T(8,128)(2,1)S(1)} %slice.97), channel_id=1, source_target_pairs={{0,1},{1,0},{2,3},{3,2},{4,5},{5,4},{6,7},{7,6},{8,9},{9,8},{10,11... | collective-permute-start | bytes 786440 | tf_op jit(solution)/shard_map/ppermute | solution.py:282
  74.9 6.8 %collective-permute-start.10 = (bf16[16,2048]{1,0:T(8,128)(2,1)S(1)}, bf16[16,2048]{1,0:T(8,128)(2,1)S(1)}, u32[]{:S(2)}, u32[]{:S(2)}) collective-permute-start(bf16[16,2048]{1,0:T(8,128)(2,1)S(1)} %get-tuple-element.29), channel_id=1, source_target_pairs={{0,8},{1,9},{2,10},{3,11},{4,12},{5,13},{6,14},{7,15},{8,16},{9,17... | collective-permute-start | bytes 196616 | tf_op jit(solution)/shard_map/ppermute | solution.py:285
  76.5 7.7 %collective-permute-start.9 = (bf16[16,2048]{1,0:T(8,128)(2,1)S(1)}, bf16[16,2048]{1,0:T(8,128)(2,1)S(1)}, u32[]{:S(2)}, u32[]{:S(2)}) collective-permute-start(bf16[16,2048]{1,0:T(8,128)(2,1)S(1)} %get-tuple-element.30), channel_id=1, source_target_pairs={{0,16},{1,17},{2,18},{3,19},{4,20},{5,21},{6,22},{7,23},{8,24},{9,... | collective-permute-start | bytes 196616 | tf_op jit(solution)/shard_map/ppermute | solution.py:285
  79.5 5.1 %collective-permute-start.8 = (bf16[16,2048]{1,0:T(8,128)(2,1)S(1)}, bf16[16,2048]{1,0:T(8,128)(2,1)S(1)}, u32[]{:S(2)}, u32[]{:S(2)}) collective-permute-start(bf16[16,2048]{1,0:T(8,128)(2,1)S(1)} %get-tuple-element.28), channel_id=1, source_target_pairs={{0,24},{1,25},{2,26},{3,27},{4,28},{5,29},{6,30},{7,31},{8,0},{9,1... | collective-permute-start | bytes 196616 | tf_op jit(solution)/shard_map/ppermute | solution.py:285
  (7 other events, 4.8 us)

commit v2 on v1

--- a/solution.py
+++ b/solution.py
@@ -13,6 +13,7 @@
 KV_WIDTH = KV_HEADS * HEAD
 CHUNK = 256
 
+
 norm_eps = 1e-06
 bf16 = jnp.bfloat16
 f32 = jnp.float32
@@ -48,40 +49,51 @@
 
 
 def attend_kernel(
-    capacity,
+    lengths_hbm,
+    bias_hbm,
+    hidden_hbm,
+    attn_gain_hbm,
+    ffn_gain_hbm,
+    branch_hbm,
+    dispatch,
+    query_hbm,
+    key_hbm,
+    value_hbm,
+    keys_hbm,
+    values_hbm,
+    out_hbm,
+    expert_gate_hbm,
+    new_keys,
+    new_values,
+    middle_hbm,
+    ffn_hbm,
+    outgoing_hbm,
+    gate_value,
+    expert_gate,
     lengths,
     score_bias,
     hidden,
     attn_gain,
     ffn_gain,
     branch_gate,
-    routes_t,
-    route_weights_t,
-    query_hbm,
-    key_hbm,
-    value_hbm,
-    keys_hbm,
-    values_hbm,
-    out_hbm,
-    new_keys,
-    new_values,
-    middle,
-    ffn_in,
-    outgoing,
-    combine,
-    gate_value,
     query_w,
     key_w,
     value_w,
     keys,
     values,
     out_w,
+    middle,
+    ffn_in,
+    outgoing,
     blocked,
     weights_t,
+    small_sems,
     weight_sems,
     key_sems,
     value_sems,
     out_sem,
+    expert_sem,
+    send_sems,
 ):
     seqs = hidden.shape[0]
     cache_len = keys.shape[1]
@@ -89,6 +101,20 @@
     chunks = cache_len // CHUNK
     pairs = seqs // 2
 
+    small = [
+        pltpu.make_async_copy(source, target, small_sems.at[i])
+        for i, (source, target) in enumerate(
+            (
+                (hidden_hbm, hidden),
+                (attn_gain_hbm, attn_gain),
+                (lengths_hbm, lengths),
+                (bias_hbm, score_bias),
+                (ffn_gain_hbm, ffn_gain),
+                (branch_hbm, branch_gate),
+            )
+        )
+    ]
+    expert_copy = pltpu.make_async_copy(expert_gate_hbm, expert_gate, expert_sem)
     first = [
         pltpu.make_async_copy(query_hbm, query_w, weight_sems.at[0]),
         pltpu.make_async_copy(key_hbm, key_w, weight_sems.at[1]),
@@ -109,6 +135,8 @@
         for p in range(pairs)
     ]
     out_copy = pltpu.make_async_copy(out_hbm, out_w, out_sem)
+    for copy in small:
+        copy.start()
     for copy in first:
         copy.start()
     for copy in reversed(key_copies):
@@ -117,6 +145,8 @@
         copy.start()
     out_copy.start()
 
+    for copy in small:
+        copy.wait()
     hidden_f = hidden[...].astype(f32)
     normed = rms_rows(hidden_f, attn_gain[...])
 
@@ -170,6 +200,7 @@
         taken = jnp.where(live, jnp.exp(log_take + after), 0.0)
         weights_t[:, rows] = jnp.transpose(taken).astype(bf16)
 
+    expert_copy.start()
     pieces = []
     for p in range(pairs):
         value_copies[p].wait()
@@ -186,62 +217,340 @@
     out_copy.wait()
     middle_f = hidden_f + matmul(attended, out_w[...])
     middle[...] = middle_f
+    send_middle = pltpu.make_async_copy(middle, middle_hbm, send_sems.at[2])
+    send_middle.start()
     ffn = rms_rows(middle_f, ffn_gain[...])
     ffn_in[...] = ffn
+    send_ffn = pltpu.make_async_copy(ffn_in, ffn_hbm, send_sems.at[0])
+    send_ffn.start()
+    cut = outgoing.shape[1]
+    stacked = jnp.concatenate(
+        [ffn[:, j * cut : (j + 1) * cut] for j in range(ffn.shape[1] // cut)], axis=0
+    )
+    outgoing[...] = matmul(dispatch[...], stacked).astype(bf16)
+    send_out = pltpu.make_async_copy(outgoing, outgoing_hbm, send_sems.at[1])
+    send_out.start()
     gate_sum = jnp.sum(ffn.astype(f32) * branch_gate[...], axis=-1, keepdims=True)
     gate_value[...] = jnp.broadcast_to(jax.nn.sigmoid(gate_sum), gate_value.shape)
-
-    slots = (outgoing.shape[0], seqs)
-    expert = iota(slots, 0) // capacity
-    named = jnp.zeros(slots, f32)
-    weighted = jnp.zeros(slots, f32)
-    for k in range(TOP):
-        hit = expert == routes_t[k : k + 1, :]
-        named = named + jnp.where(hit, 1.0, 0.0)
-        weighted = weighted + jnp.where(hit, route_weights_t[k : k + 1, :], 0.0)
-    earlier = (iota((seqs, seqs), 0) < iota((seqs, seqs), 1)).astype(bf16)
-    rank = matmul(named.astype(bf16), earlier)
-    mine = rank == (iota(slots, 0) % capacity).astype(f32)
-    combine[...] = jnp.where(mine, weighted, 0.0)
-    outgoing[...] = matmul(jnp.where(mine, named, 0.0).astype(bf16), ffn).astype(bf16)
-
-
-def attend(capacity, slots, args):
+    expert_copy.wait()
+    send_middle.wait()
+    send_ffn.wait()
+    send_out.wait()
+
+
+SMEM = pl.BlockSpec(memory_space=pltpu.SMEM)
+VMEM = pl.BlockSpec(memory_space=pltpu.VMEM)
+HBM = pl.BlockSpec(memory_space=pltpu.HBM)
+
+
+def in_hbm(values):
+    return pltpu.with_memory_space_constraint(values, pltpu.HBM)
+
+
+def call(kernel, out_shape, args, in_specs, out_specs, scratch=(), limit=16):
+    return pl.pallas_call(
+        kernel,
+        out_shape=out_shape,
+        in_specs=in_specs,
+        out_specs=out_specs,
+        scratch_shapes=list(scratch),
+        compiler_params=pltpu.CompilerParams(vmem_limit_bytes=limit << 20),
+    )(*args)
+
+
+def shaped(shape, dtype):
+    return jax.ShapeDtypeStruct(shape, dtype)
+
+
+def attend(args, out_rows, out_cut):
     hidden = args[2]
-    keys = args[11]
+    keys = args[10]
     seqs, width = hidden.shape
     cache_len = keys.shape[1]
-    pairs = seqs // 2
-    shapes = (
-        jax.ShapeDtypeStruct((seqs, KV_WIDTH), bf16),
-        jax.ShapeDtypeStruct((seqs, KV_WIDTH), bf16),
-        jax.ShapeDtypeStruct((seqs, width), f32),
-        jax.ShapeDtypeStruct((seqs, width), bf16),
-        jax.ShapeDtypeStruct((slots, width), bf16),
-        jax.ShapeDtypeStruct((slots, seqs), f32),
-        jax.ShapeDtypeStruct((seqs, 128), f32),
-    )
-    smem = pl.BlockSpec(memory_space=pltpu.SMEM)
-    vmem = pl.BlockSpec(memory_space=pltpu.VMEM)
-    hbm = pl.BlockSpec(memory_space=pl.ANY)
-    big = args[8:]
-    return pl.pallas_call(
-        lambda *refs: attend_kernel(capacity, *refs),
-        out_shape=shapes,
-        in_specs=[smem] * 2 + [vmem] * 6 + [hbm] * 6,
-        out_specs=[vmem] * 7,
-        scratch_shapes=[pltpu.VMEM(a.shape, a.dtype) for a in big]
+    return call(
+        attend_kernel,
+        (
+            shaped((seqs, KV_WIDTH), bf16),
+            shaped((seqs, KV_WIDTH), bf16),
+            pltpu.HBM((seqs, width), f32),
+            pltpu.HBM((seqs, width), bf16),
+            pltpu.HBM((out_rows, out_cut), bf16),
+            shaped((seqs, 128), f32),
+        )
+        + tuple(pltpu.VMEM(a.shape, a.dtype) for a in args[13:]),
+        tuple(arg if i == 6 else in_hbm(arg) for i, arg in enumerate(args)),
+        [HBM] * 6 + [VMEM] + [HBM] * 7,
+        [VMEM] * 2 + [HBM] * 3 + [VMEM] * 2,
+        [
+            pltpu.SMEM(args[0].shape, jnp.int32),
+            pltpu.SMEM(args[1].shape, f32),
+        ]
+        + [pltpu.VMEM(a.shape, a.dtype) for a in args[2:6]]
+        + [pltpu.VMEM(a.shape, a.dtype) for a in args[7:13]]
         + [
+            pltpu.VMEM((seqs, width), f32),
+            pltpu.VMEM((seqs, width), bf16),
+            pltpu.VMEM((out_rows, out_cut), bf16),
             pltpu.VMEM((seqs * KV_WIDTH, seqs * HEADS), bf16),
             pltpu.VMEM((seqs * HEADS, cache_len), bf16),
+            pltpu.SemaphoreType.DMA((6,)),
             pltpu.SemaphoreType.DMA((3,)),
             pltpu.SemaphoreType.DMA((cache_len // CHUNK,)),
-            pltpu.SemaphoreType.DMA((pairs,)),
+            pltpu.SemaphoreType.DMA((seqs // 2,)),
             pltpu.SemaphoreType.DMA,
+            pltpu.SemaphoreType.DMA,
+            pltpu.SemaphoreType.DMA((3,)),
         ],
-        compiler_params=pltpu.CompilerParams(vmem_limit_bytes=40 << 20),
-        name="attend",
-    )(*args)
+        32,
+    )
+
+
+def prepare(gate_t, up_t, down_t, routes_t, route_weights_t, capacity, cuts, experts):
+    units, width = gate_t.shape
+    seqs = routes_t.shape[1]
+    rows = experts * capacity * cuts
+    lanes = cuts * seqs
+    half = units // 2
+
+    def kernel(
+        gate,
+        up,
+        down,
+        picks_hbm,
+        pick_weights_hbm,
+        low,
+        high,
+        dispatch,
+        combine_hbm,
+        combine,
+        picks,
+        pick_weights,
+        sems,
+    ):
+        small = [
+            pltpu.make_async_copy(picks_hbm, picks, sems.at[4]),
+            pltpu.make_async_copy(pick_weights_hbm, pick_weights, sems.at[5]),
+        ]
+        for copy in small:
+            copy.start()
+        copies = [
+            pltpu.make_async_copy(gate, low.at[pl.ds(0, units)], sems.at[0]),
+            pltpu.make_async_copy(
+                up.at[pl.ds(0, half)], low.at[pl.ds(units, half)], sems.at[1]
+            ),
+            pltpu.make_async_copy(
+                up.at[pl.ds(half, half)], high.at[pl.ds(0, half)], sems.at[2]
+            ),
+            pltpu.make_async_copy(down, high.at[pl.ds(half, units)], sems.at[3]),
+        ]
+        for copy in copies:
+            copy.start()
+        for copy in small:
+            copy.wait()
+        shape = (rows, seqs)
+        expert = iota(shape, 0) // (capacity * cuts)
+        named = jnp.zeros(shape, f32)
+        weighted = jnp.zeros(shape, f32)
+        for k in range(TOP):
+            hit = expert == picks[k : k + 1, :]
+            named = named + jnp.where(hit, 1.0, 0.0)
+            weighted = weighted + jnp.where(hit, pick_weights[k : k + 1, :], 0.0)
+        earlier = (iota((seqs, seqs), 0) < iota((seqs, seqs), 1)).astype(bf16)
+        rank = matmul(named.astype(bf16), earlier)
+        mine = rank == (iota(shape, 0) % capacity).astype(f32)
+        repeat = (iota((seqs, lanes), 1) % seqs == iota((seqs, lanes), 0)).astype(bf16)
+        own_cut = (iota((rows, lanes), 0) // capacity) % cuts == iota((rows, lanes), 1) // seqs
+
+        def spread(values):
+            return jnp.where(own_cut, matmul(values, repeat), 0.0).astype(bf16)
+
+        dispatch[...] = spread(jnp.where(mine, named, 0.0).astype(bf16))
+        parts = three_parts(jnp.where(mine, weighted, 0.0))
+        for part in range(3):
+            combine[:, part * lanes : (part + 1) * lanes] = spread(parts[part])
+        send = pltpu.make_async_copy(combine, combine_hbm, sems.at[6])
+        send.start()
+        send.wait()
+        for copy in copies:
+            copy.wait()
+
+    return call(
+        kernel,
+        (
+            shaped((units + half, width), bf16),
+            shaped((units + half, width), bf16),
+            shaped((rows, lanes), bf16),
+            pltpu.HBM((rows, 3 * lanes), bf16),
+        ),
+        (gate_t, up_t, down_t, routes_t, route_weights_t),
+        [HBM] * 5,
+        [HBM] * 2 + [VMEM] + [HBM],
+        [
+            pltpu.VMEM((rows, 3 * lanes), bf16),
+            pltpu.VMEM(routes_t.shape, jnp.int32),
+            pltpu.VMEM(route_weights_t.shape, f32),
+            pltpu.SemaphoreType.DMA((7,)),
+        ],
+        32,
+    )
+
+
+def run_experts(arrived, gate_w, up_w, down_w, capacity):
+    devices, chunk, cut = arrived.shape
+    cuts = chunk // capacity
+    block = min(devices, 256 // chunk)
+    block_rows = block * chunk
+    block_slots = block * capacity
+
+    def kernel(rows, gate, up_hbm, down_hbm, out, up, down, sems):
+        up_copy = pltpu.make_async_copy(up_hbm, up, sems.at[0])
+        down_copy = pltpu.make_async_copy(down_hbm, down, sems.at[1])
+        up_copy.start()
+        down_copy.start()
+        square = (block_rows, block_rows)
+
+        def target(index):
+            slot = index % block_slots
+            return (
+                slot // capacity * chunk + index // block_slots * capacity + slot % capacity
+            )
+
+        to_cuts = (target(iota(square, 0)) == iota(square, 1)).astype(bf16)
+        to_chunks = (target(iota(square, 1)) == iota(square, 0)).astype(bf16)
+        tokens = []
+        for b in range(devices // block):
+            part = rows[b * block : (b + 1) * block].reshape(block_rows, cut)
+            sorted_rows = matmul(to_cuts, part).astype(bf16)
+            tokens.append(
+                jnp.concatenate(
+                    [
+                        sorted_rows[j * block_slots : (j + 1) * block_slots]
+                        for j in range(cuts)
+                    ],
+                    axis=1,
+                )
+            )
+        tokens = jnp.concatenate(tokens, axis=0)
+        hidden = jax.nn.silu(matmul(tokens, gate[...]))
+        up_copy.wait()
+        hidden = hidden * matmul(tokens, up[...])
+        down_copy.wait()
+        result = matmul(hidden.astype(bf16), down[...]).astype(bf16)
+        for b in range(devices // block):
+            part = result[b * block_slots : (b + 1) * block_slots]
+            part = jnp.concatenate(
+                [part[:, j * cut : (j + 1) * cut] for j in range(cuts)], axis=0
+            )
+            out[b * block : (b + 1) * block] = (
+                matmul(to_chunks, part).astype(bf16).reshape(block, chunk, cut)
+            )
+
+    return call(
+        kernel,
+        shaped(arrived.shape, bf16),
+        (arrived, gate_w, in_hbm(up_w), in_hbm(down_w)),
+        [VMEM] * 2 + [HBM] * 2,
+        VMEM,
+        [
+            pltpu.VMEM(up_w.shape, up_w.dtype),
+            pltpu.VMEM(down_w.shape, down_w.dtype),
+            pltpu.SemaphoreType.DMA((2,)),
+        ],
+        32,
+    )
+
+
+def run_dense(tokens, lows, highs):
+    seqs, width = tokens[0].shape
+    count = len(lows)
+    held = lows[0].shape[0]
+    half = held // 3
+    units = 2 * half
+    total = len(tokens)
+    kept = total // 2 * seqs
+
+    def kernel(*refs):
+        token_refs = refs[:total]
+        sources = refs[total : total + 2 * count]
+        keep, give = refs[total + 2 * count : total + 2 * count + 2]
+        weights, sems = refs[total + 2 * count + 2 :]
+        copies = [
+            pltpu.make_async_copy(source, weights.at[i], sems.at[i])
+            for i, source in enumerate(sources)
+        ]
+        for copy in copies:
+            copy.start()
+        rows = jnp.concatenate([ref[...] for ref in token_refs], axis=0)
+        for copy in copies:
+            copy.wait()
+        gates = [weights[j, :units] for j in range(count)]
+        ups = []
+        for j in range(count):
+            ups += [weights[j, units:], weights[count + j, :half]]
+        downs = [weights[count + j, half:] for j in range(count)]
+        hidden = jax.nn.silu(matmul_bt(rows, jnp.concatenate(gates, axis=0)))
+        hidden = hidden * matmul_bt(rows, jnp.concatenate(ups, axis=0))
+        partial = matmul(hidden.astype(bf16), jnp.concatenate(downs, axis=0))
+        keep[...] = partial[:kept]
+        give[...] = partial[kept:].astype(bf16)
+
+    return call(
+        kernel,
+        (shaped((kept, width), f32), shaped((total * seqs - kept, width), bf16)),
+        (*tokens, *lows, *highs),
+        [VMEM] * total + [HBM] * (2 * count),
+        [VMEM] * 2,
+        [pltpu.VMEM((2 * count, held, width), bf16), pltpu.SemaphoreType.DMA((2 * count,))],
+        32,
+    )
+
+
+def merge(kept, taken, seqs):
+    layers = kept.shape[0] // seqs
+    width = kept.shape[1]
+
+    def kernel(left, right, own, *rest):
+        own[...] = left[:seqs] + right[:seqs].astype(f32)
+        for k in range(1, layers):
+            rows = slice(k * seqs, (k + 1) * seqs)
+            rest[k - 1][...] = (left[rows] + right[rows].astype(f32)).astype(bf16)
+
+    return call(
+        kernel,
+        (shaped((seqs, width), f32),) + (shaped((seqs, width), bf16),) * (layers - 1),
+        (kept, taken),
+        [VMEM] * 2,
+        [VMEM] * layers,
+    )
+
+
+def finish(middle, gate_value, combine, returned, dense_parts):
+    seqs, width = middle.shape
+    devices, chunk, cut = returned.shape
+    lanes = combine.shape[1] // 3
+
+    def kernel(base, gate, mix, rows, *refs):
+        out = refs[-1]
+        picked = rows[...].reshape(devices * chunk, cut)
+        mixed = matmul_at(mix[...], picked)
+        mixed = mixed[:lanes] + mixed[lanes : 2 * lanes] + mixed[2 * lanes :]
+        dense = refs[0][...]
+        for ref in refs[1:-1]:
+            dense = dense + ref[...].astype(f32)
+        expert_sum = jnp.concatenate(
+            [mixed[j * seqs : (j + 1) * seqs] for j in range(width // cut)], axis=1
+        )
+        out[...] = (base[...] + expert_sum + gate[:, :1] * dense).astype(bf16)
+
+    return call(
+        kernel,
+        shaped((seqs, width), bf16),
+        (middle, gate_value, combine, returned, *dense_parts),
+        [VMEM] * (4 + len(dense_parts)),
+        VMEM,
+        (),
+        32,
+    )
 
 
 def per_device(
@@ -268,15 +577,12 @@
 ):
     seqs, width = hidden_in.shape
     devices = lax.axis_size("ep")
-    local_experts = expert_gate.shape[0]
-    experts_all = local_experts * devices
+    experts_all = expert_gate.shape[0] * devices
     capacity = max(1, seqs * TOP // experts_all)
-    slots = experts_all * capacity
-    layers = 1
-    while 2 * (2 * layers) ** 2 <= devices and devices % (4 * layers) == 0:
-        layers = 2 * layers
+    cuts = max(1, 16 // capacity)
+    chunk = capacity * cuts
+    layers = layer_count(devices)
     plane = devices // layers
-    units = dense_gate.shape[1]
 
     def swap(values, bits):
         return lax.ppermute(values, "ep", [(i, i ^ bits) for i in range(devices)])
@@ -286,14 +592,40 @@
             values, "ep", [(i, (i + steps * plane) % devices) for i in range(devices)]
         )
 
-    own_dense = jnp.concatenate([dense_gate.T, dense_up.T, dense_down.T], axis=0)
-    dense_parts = [own_dense]
+    low, high, dispatch, combine = prepare(
+        in_hbm(dense_gate.T),
+        in_hbm(dense_up.T),
+        in_hbm(dense_down.T),
+        in_hbm(routes.T),
+        in_hbm(route_weights.T),
+        capacity,
+        cuts,
+        experts_all,
+    )
+    lows = [low]
+    highs = [high]
+    bits = 2
+    while bits < plane:
+        more_lows = [swap(low, bits)]
+        more_highs = [swap(high, bits)]
+        bits = 2 * bits
+        lows += more_lows
+        highs += more_highs
+    bits = 2
+    direct = {1 << (k + 1): k + 1 for k in range(len(lows) - 1)}
     for other in range(2, plane, 2):
-        dense_parts.append(swap(own_dense, other))
-
-    new_keys, new_values, middle, ffn_in, outgoing, combine, gate_value = attend(
-        capacity,
-        slots,
+        if other in direct:
+            continue
+        first = other & -other
+        last = other ^ first
+        if last in direct:
+            lows.append(swap(lows[direct[first]], last))
+            highs.append(swap(highs[direct[last]], first))
+        else:
+            lows.append(swap(low, other))
+            highs.append(swap(high, other))
+
+    new_keys, new_values, middle, ffn_in, outgoing, gate_value, gate_w = attend(
         (
             lengths,
             score_bias,
@@ -301,55 +633,49 @@
             attn_gain.reshape(1, width),
             ffn_gain.reshape(1, width),
             branch_gate.reshape(1, width),
-            routes.T,
-            route_weights.T,
+            dispatch,
             query_weight,
             key_weight,
             value_weight,
             key_cache,
             value_cache,
             out_weight,
+            expert_gate[0],
         ),
-    )
-
-    outgoing = outgoing.reshape(devices, local_experts * capacity, width)
-    arrived = lax.all_to_all(outgoing, "ep", split_axis=0, concat_axis=0, tiled=True)
-    chain = [ffn_in] + [climb(ffn_in, k) for k in range(1, layers)]
-    chain = jnp.concatenate(chain, axis=0)
-    chain = jnp.concatenate([chain, swap(chain, 1)], axis=0)
-
-    flat_in = arrived.reshape(-1, width)
-    gate_pre = matmul(flat_in, expert_gate[0])
-    up_pre = matmul(flat_in, expert_up[0])
-    hidden_act = (jax.nn.silu(gate_pre) * up_pre).astype(bf16)
-    expert_rows = matmul(hidden_act, expert_down[0]).astype(bf16)
+        devices * chunk,
+        width // cuts,
+    )
+    arrived = lax.all_to_all(
+        outgoing.reshape(devices, chunk, width // cuts),
+        "ep",
+        split_axis=0,
+        concat_axis=0,
+        tiled=True,
+    )
+    chain = [ffn_in]
+    for k in range(1, layers):
+        chain.append(climb(ffn_in, k))
+    for k in range(layers):
+        chain.append(swap(chain[k], 1))
+    expert_rows = run_experts(arrived, gate_w, expert_up[0], expert_down[0], capacity)
     returned = lax.all_to_all(
-        expert_rows.reshape(arrived.shape), "ep", split_axis=0, concat_axis=0, tiled=True
-    ).reshape(slots, width)
-
-    gates = jnp.concatenate([part[:units] for part in dense_parts], axis=0)
-    ups = jnp.concatenate([part[units : 2 * units] for part in dense_parts], axis=0)
-    downs = jnp.concatenate([part[2 * units :] for part in dense_parts], axis=0)
-    dense_hidden = (
-        jax.nn.silu(matmul_bt(chain, gates)) * matmul_bt(chain, ups)
-    ).astype(bf16)
-    partial = matmul(dense_hidden, downs)
-    half = layers * seqs
-    summed = partial[:half] + swap(partial[half:].astype(bf16), 1).astype(f32)
-    dense_out = summed[:seqs]
+        expert_rows, "ep", split_axis=0, concat_axis=0, tiled=True
+    )
+    kept, given = run_dense(chain, lows, highs)
+    taken = swap(given, 1)
+    own, *rest = merge(kept, taken, seqs)
+    parts = [own]
     for k in range(1, layers):
-        piece = summed[k * seqs : (k + 1) * seqs].astype(bf16)
-        dense_out = dense_out + climb(piece, -k).astype(f32)
-
-    expert_sum = lax.dot_general(
-        combine,
-        returned.astype(f32),
-        (((0,), (0,)), ((), ())),
-        precision=lax.Precision.HIGHEST,
-        preferred_element_type=f32,
-    )
-    hidden_out = (middle + expert_sum + gate_value[:, :1] * dense_out).astype(bf16)
+        parts.append(climb(rest[k - 1], -k))
+    hidden_out = finish(middle, gate_value, combine, returned, parts)
     return (hidden_out, new_keys, new_values)
+
+
+def layer_count(devices):
+    layers = 1
+    while 2 * (2 * layers) ** 2 <= devices and devices % (4 * layers) == 0:
+        layers = 2 * layers
+    return layers
 
 
 def solution(mesh):

time: 86.3 us -> 77.5 us (0.90)
  local copies, waits for them, and re-layouts: 27.5 us -> 3.99 us
  Pallas kernels: 9.07 us -> 23.5 us
  matrix products: 9.81 us -> 0 us
  waiting for transfers between devices: 11.3 us -> 20.3 us
  starting transfers between devices: 22.7 us -> 28.5 us
  other arithmetic: 4.06 us -> 0 us
    pallas_call x1 -> x6, Pallas kernels: 9.07 us -> 23.5 us  [call(): pl.pallas_call(kernel, out_shape=out_shape, in_specs=in_specs, out_specs=...]
    unnamed x40 -> x18, local copies, waits for them, and re-layouts: 17.8 us -> 3.99 us
    ppermute x6, waiting for transfers between devices: 3.68 us -> 15.1 us  [climb(): lax.ppermute(values, 'ep', [(i, (i + steps * plane) % devices) for i in r...]
    dot_general x5 -> x0, matrix products: 9.81 us -> none  [the longest x3 7.94 us: matmul(): return jnp.dot(left, right, preferred_element_type=f32)]
    slice x6 -> x0, local copies, waits for them, and re-layouts: 7.11 us -> none  [the longest x3 5.91 us: per_device(): part[units:2 * units]]
    all_to_all x2, waiting for transfers between devices: 5.62 us -> 0.01 us  [the longest x1 0.01 us: per_device(): lax.all_to_all(expert_rows, 'ep', split_axis=0, concat_axis=0, tiled=True)]
    ppermute x5 -> x11, starting transfers between devices: 6.21 us -> 10.6 us  [swap(): return lax.ppermute(values, 'ep', [(i, i ^ bits) for i in range(devices)])]
    all_to_all x2, starting transfers between devices: 5.17 us -> 8.44 us  [the longest x1 4.47 us: per_device(): lax.all_to_all(expert_rows, 'ep', split_axis=0, concat_axis=0, tiled=True)]
  transfers between devices with their start and end apart: 13 -> 19, of which waited for: 6 -> 8; matrix products, arithmetic and copies ran while one was open for 26% -> 0% of each run, Pallas kernels for 11% -> 27%
where the time goes in v2:
time: 77.5 us; the launch traced here: 77 us
  starting transfers between devices  28.5 us (37%)
  Pallas kernels  23.5 us (30%)
  waiting for transfers between devices  20.3 us (26%)
  local copies, waits for them, and re-layouts  3.99 us (5%)
    pallas_call x6, Pallas kernels, call(): pl.pallas_call(kernel, out_shape=out_shape, in_specs=in_specs, out_specs=...  23.5 us
    ppermute x6, waiting for transfers between devices, climb(): lax.ppermute(values, 'ep', [(i, (i + steps * plane) % devices) for i in r...  15.1 us
    ppermute x11, starting transfers between devices, swap(): return lax.ppermute(values, 'ep', [(i, i ^ bits) for i in range(devices)])  10.6 us
    ppermute x6, starting transfers between devices, climb(): lax.ppermute(values, 'ep', [(i, (i + steps * plane) % devices) for i in r...  9.41 us
    ppermute x11, waiting for transfers between devices, swap(): return lax.ppermute(values, 'ep', [(i, i ^ bits) for i in range(devices)])  5.19 us
    all_to_all x1, starting transfers between devices, per_device(): lax.all_to_all(expert_rows, 'ep', split_axis=0, concat_axis=0, tiled=True)  4.47 us
    unnamed x18, local copies, waits for them, and re-layouts  3.99 us
    all_to_all x1, starting transfers between devices, per_device(): lax.all_to_all(outgoing.reshape(devices, chunk, width // cuts), 'ep', spl...  3.97 us
  transfers between devices with their start and end apart: 19, of which 8 were waited for; matrix products, arithmetic and copies ran while one was open for 0% of the time, Pallas kernels for 27%

profile of v2, /device:TPU:0, one launch (start us, length us, event | category | flops | bytes accessed | tf_op | source)
XLA Modules:
  0.0 77.0 jit_solution(1880723318274051203)
XLA Ops:
  0.6 2.1 %shard_map.211 = (bf16[96,2048]{1,0:T(8,128)(2,1)S(1)}, bf16[96,2048]{1,0:T(8,128)(2,1)S(1)}, bf16[512,128]{1,0:T(8,128)(2,1)S(1)}, bf16[512,384]{1,0:T(8,128)(2,1)}) custom-call(bf16[64,2048]{1,0:T(8,128)(2,1)} %bitcast.15, bf16[64,2048]{1,0:T(8,128)(2,1)} %bitcast.16, bf16[64,2048]{1,0:T(8,128)(2,1)} %bitcast.17, s32[4,16]{1,0:T(4,128)} %bitcast.22, ...), custom_call_target="tpu_custom_call" | custom-call | tf_op jit(solution)/shard_map/pallas_call | solution.py:251
  2.8 3.0 %collective-permute-start.7 = (bf16[96,2048]{1,0:T(8,128)(2,1)S(1)}, bf16[96,2048]{1,0:T(8,128)(2,1)S(1)}, u32[]{:S(2)}, u32[]{:S(2)}) collective-permute-start(bf16[96,2048]{1,0:T(8,128)(2,1)S(1)} %get-tuple-element.27.refs_8_), channel_id=1, source_target_pairs={{0,2},{1,3},{2,0},{3,1},{4,6},{5,7},{6,4},{7,5},{8,10},{9,11},{10,... | collective-permute-start | bytes 1179656 | tf_op jit(solution)/shard_map/ppermute | solution.py:588
  5.8 1.5 %collective-permute-start.11 = (bf16[96,2048]{1,0:T(8,128)(2,1)S(1)}, bf16[96,2048]{1,0:T(8,128)(2,1)}, u32[]{:S(2)}, u32[]{:S(2)}) collective-permute-start(bf16[96,2048]{1,0:T(8,128)(2,1)S(1)} %get-tuple-element.28.refs_12_), channel_id=1, source_target_pairs={{0,4},{1,5},{2,6},{3,7},{4,0},{5,1},{6,2},{7,3},{8,12},{9,13},{10,... | collective-permute-start | bytes 1179656 | tf_op jit(solution)/shard_map/ppermute | solution.py:588
  7.3 12.4 %shard_map.212 = (bf16[16,128]{1,0:T(8,128)(2,1)}, bf16[16,128]{1,0:T(8,128)(2,1)}, f32[16,2048]{1,0:T(8,128)}, bf16[16,2048]{1,0:T(8,128)(2,1)}, bf16[512,256]{...) custom-call(s32[16]{0:T(128)} %lengths_hbm.1, f32[8]{0:T(128)} %bias_hbm.1, ...), custom_call_target="tpu_custom_call" | custom-call | tf_op jit(solution)/shard_map/pallas_call | solution.py:251
  19.7 4.0 %all-to-all-start = ((bf16[32,16,256]{2,1,0:T(8,128)(2,1)}), bf16[32,16,256]{2,1,0:T(8,128)(2,1)S(1)}, u32[]{:S(2)}, u32[]{:S(2)}) async-start(bf16[32,16,256]{2,1,0:T(8,128)(2,1)} %bitcast.18), calls=%async_computation | async-start | bytes 524288 | tf_op jit(solution)/shard_map/all_to_all | solution.py:648
  23.7 1.8 %collective-permute-start = (bf16[16,2048]{1,0:T(8,128)(2,1)}, bf16[16,2048]{1,0:T(8,128)(2,1)}, u32[]{:S(2)}, u32[]{:S(2)}) collective-permute-start(bf16[16,2048]{1,0:T(8,128)(2,1)} %get-tuple-element.26.refs_0_), channel_id=1, source_target_pairs={{0,8},{1,9},{2,10},{3,11},{4,12},{5,13},{6,14},{7,15},{8,16},{9,17... | collective-permute-start | bytes 196616 | tf_op jit(solution)/shard_map/ppermute | solution.py:591
  25.5 2.4 %collective-permute-start.1 = (bf16[16,2048]{1,0:T(8,128)(2,1)}, bf16[16,2048]{1,0:T(8,128)(2,1)S(1)}, u32[]{:S(2)}, u32[]{:S(2)}) collective-permute-start(bf16[16,2048]{1,0:T(8,128)(2,1)} %get-tuple-element.26.refs_0_), channel_id=1, source_target_pairs={{0,16},{1,17},{2,18},{3,19},{4,20},{5,21},{6,22},{7,23},{8,24},{9,... | collective-permute-start | bytes 196616 | tf_op jit(solution)/shard_map/ppermute | solution.py:591
  27.9 1.5 %collective-permute-start.8 = (bf16[96,2048]{1,0:T(8,128)(2,1)S(1)}, bf16[96,2048]{1,0:T(8,128)(2,1)}, u32[]{:S(2)}, u32[]{:S(2)}) collective-permute-start(bf16[96,2048]{1,0:T(8,128)(2,1)S(1)} %get-tuple-element.27.refs_8_), channel_id=1, source_target_pairs={{0,4},{1,5},{2,6},{3,7},{4,0},{5,1},{6,2},{7,3},{8,12},{9,13},{10,... | collective-permute-start | bytes 1179656 | tf_op jit(solution)/shard_map/ppermute | solution.py:588
  29.4 5.2 %collective-permute-done.refs_1_ = bf16[16,2048]{1,0:T(8,128)(2,1)} collective-permute-done((bf16[16,2048]{1,0:T(8,128)(2,1)}, bf16[16,2048]{1,0:T(8,128)(2,1)}, u32[]{:S(2)}, u32[]{:S(2)}) %collective-permute-start) | collective-permute-done | bytes 65568 | tf_op jit(solution)/shard_map/ppermute | solution.py:591
  34.7 1.5 %collective-permute-start.10 = (bf16[96,2048]{1,0:T(8,128)(2,1)S(1)}, bf16[96,2048]{1,0:T(8,128)(2,1)}, u32[]{:S(2)}, u32[]{:S(2)}) collective-permute-start(bf16[96,2048]{1,0:T(8,128)(2,1)S(1)} %get-tuple-element.28.refs_12_), channel_id=1, source_target_pairs={{0,2},{1,3},{2,0},{3,1},{4,6},{5,7},{6,4},{7,5},{8,10},{9,11},{10,... | collective-permute-start | bytes 1179656 | tf_op jit(solution)/shard_map/ppermute | solution.py:588
  36.2 1.5 %collective-permute-start.9 = (bf16[96,2048]{1,0:T(8,128)(2,1)S(1)}, bf16[96,2048]{1,0:T(8,128)(2,1)}, u32[]{:S(2)}, u32[]{:S(2)}) collective-permute-start(bf16[96,2048]{1,0:T(8,128)(2,1)S(1)} %collective-permute-done.7.refs_9_), channel_id=1, source_target_pairs={{0,4},{1,5},{2,6},{3,7},{4,0},{5,1},{6,2},{7,3},{8,12},{9,13},{10,... | collective-permute-start | bytes 1179656 | tf_op jit(solution)/shard_map/ppermute | solution.py:588
  38.6 4.1 %collective-permute-done.2.refs_3_ = bf16[16,2048]{1,0:T(8,128)(2,1)S(1)} collective-permute-done((bf16[16,2048]{1,0:T(8,128)(2,1)}, bf16[16,2048]{1,0:T(8,128)(2,1)S(1)}, u32[]{:S(2)}, u32[]{:S(2)}) %collective-permute-start.2) | collective-permute-done | bytes 65568 | tf_op jit(solution)/shard_map/ppermute | solution.py:591
  42.7 1.5 %collective-permute-done.3.refs_4_ = bf16[16,2048]{1,0:T(8,128)(2,1)S(1)} collective-permute-done((bf16[16,2048]{1,0:T(8,128)(2,1)}, bf16[16,2048]{1,0:T(8,128)(2,1)S(1)}, u32[]{:S(2)}, u32[]{:S(2)}) %collective-permute-start.3) | collective-permute-done | bytes 65568 | tf_op jit(solution)/shard_map/ppermute | solution.py:588
  45.0 4.1 %shard_map.213 = bf16[32,16,256]{2,1,0:T(8,128)(2,1)} custom-call(bf16[32,16,256]{2,1,0:T(8,128)(2,1)S(1)} %all-to-all-done.rows, bf16[2048,512]{1,0:T(8,128)(2,1)S(1)} %get-tuple-element.25.gate, bf16[2048,512]{1,0:T(8,128)(2,1)} %bitcast.13, bf16[512,2048]{1,0:T(8,128)(2,1)} %bitcast.14), custom_call_target="tpu_custom_call" | custom-call | tf_op jit(solution)/shard_map/pallas_call | solution.py:251
  49.1 4.5 %all-to-all-start.1 = ((bf16[32,16,256]{2,1,0:T(8,128)(2,1)}), bf16[32,16,256]{2,1,0:T(8,128)(2,1)S(1)}, u32[]{:S(2)}, u32[]{:S(2)}) async-start(bf16[32,16,256]{2,1,0:T(8,128)(2,1)} %shard_map.213), calls=%async_computation.1 | async-start | bytes 524288 | tf_op jit(solution)/shard_map/all_to_all | solution.py:661
  53.9 1.2 %collective-permute-done.5.refs_6_ = bf16[16,2048]{1,0:T(8,128)(2,1)S(1)} collective-permute-done((bf16[16,2048]{1,0:T(8,128)(2,1)}, bf16[16,2048]{1,0:T(8,128)(2,1)S(1)}, u32[]{:S(2)}, u32[]{:S(2)}) %collective-permute-start.5) | collective-permute-done | bytes 65568 | tf_op jit(solution)/shard_map/ppermute | solution.py:588
  55.4 1.2 %collective-permute-done.6.refs_7_ = bf16[16,2048]{1,0:T(8,128)(2,1)S(1)} collective-permute-done((bf16[16,2048]{1,0:T(8,128)(2,1)}, bf16[16,2048]{1,0:T(8,128)(2,1)S(1)}, u32[]{:S(2)}, u32[]{:S(2)}) %collective-permute-start.6) | collective-permute-done | bytes 65568 | tf_op jit(solution)/shard_map/ppermute | solution.py:588
  60.0 3.9 %shard_map.214 = (f32[64,2048]{1,0:T(8,128)S(1)}, bf16[64,2048]{1,0:T(8,128)(2,1)S(1)}) custom-call(bf16[16,2048]{1,0:T(8,128)(2,1)S(1)} %copy-done.2, bf16[16,2048]{1,0:T(8,128)(2,1)} %collective-permute-done.refs_1_, bf16[16,2048]{1,0:T(8,128)(2,1)S(1)} %copy-done.4, bf16[16,2048]{1,0:T(8,128)(2,1)S(1)} %copy-done.6, bf16[16,2048]{1,0:T(8,128)(2,1)S(1)} %copy-done.8, ...), custom_call_target="tpu_custom_call" | custom-call | tf_op jit(solution)/shard_map/pallas_call | solution.py:251
  64.2 1.3 %collective-permute-done.13.right = bf16[64,2048]{1,0:T(8,128)(2,1)S(1)} collective-permute-done((bf16[64,2048]{1,0:T(8,128)(2,1)S(1)}, bf16[64,2048]{1,0:T(8,128)(2,1)S(1)}, u32[]{:S(2)}, u32[]{:S(2)}) %collective-permute-start.13) | collective-permute-done | bytes 262176 | tf_op jit(solution)/shard_map/ppermute | solution.py:588
  65.5 3.7 %collective-permute-start.14 = (bf16[16,2048]{1,0:T(8,128)(2,1)S(1)}, bf16[16,2048]{1,0:T(8,128)(2,1)S(1)}, u32[]{:S(2)}, u32[]{:S(2)}) collective-permute-start(bf16[16,2048]{1,0:T(8,128)(2,1)S(1)} %get-tuple-element.32), channel_id=1, source_target_pairs={{0,24},{1,25},{2,26},{3,27},{4,28},{5,29},{6,30},{7,31},{8,0},{9,1... | collective-permute-start | bytes 196616 | tf_op jit(solution)/shard_map/ppermute | solution.py:591
  69.2 1.1 %collective-permute-start.16 = (bf16[16,2048]{1,0:T(8,128)(2,1)S(1)}, bf16[16,2048]{1,0:T(8,128)(2,1)S(1)}, u32[]{:S(2)}, u32[]{:S(2)}) collective-permute-start(bf16[16,2048]{1,0:T(8,128)(2,1)S(1)} %get-tuple-element.34), channel_id=1, source_target_pairs={{0,8},{1,9},{2,10},{3,11},{4,12},{5,13},{6,14},{7,15},{8,16},{9,17... | collective-permute-start | bytes 196616 | tf_op jit(solution)/shard_map/ppermute | solution.py:591
  70.3 1.4 %collective-permute-done.14.refs_1_ = bf16[16,2048]{1,0:T(8,128)(2,1)S(1)} collective-permute-done((bf16[16,2048]{1,0:T(8,128)(2,1)S(1)}, bf16[16,2048]{1,0:T(8,128)(2,1)S(1)}, u32[]{:S(2)}, u32[]{:S(2)}) %collective-permute-start.14) | collective-permute-done | bytes 65568 | tf_op jit(solution)/shard_map/ppermute | solution.py:591
  71.7 4.3 %collective-permute-done.15.refs_2_ = bf16[16,2048]{1,0:T(8,128)(2,1)S(1)} collective-permute-done((bf16[16,2048]{1,0:T(8,128)(2,1)S(1)}, bf16[16,2048]{1,0:T(8,128)(2,1)S(1)}, u32[]{:S(2)}, u32[]{:S(2)}) %collective-permute-start.15) | collective-permute-done | bytes 65568 | tf_op jit(solution)/shard_map/ppermute | solution.py:591
  76.1 0.9 %shard_map.216 = bf16[16,2048]{1,0:T(8,128)(2,1)} custom-call(f32[16,2048]{1,0:T(8,128)S(1)} %copy-done.1, f32[16,128]{1,0:T(8,128)S(1)} %get-tuple-element.22.gate, bf16[512,384]{1,0:T(8,128)(2,1)S(1)} %copy-done, bf16[32,16,256]{2,1,0:T(8,128)(2,1)S(1)} %all-to-all-done.1.rows, f32[16,2048]{1,0:T(8,128)S(1)} %get-tuple-element.31.refs_0_, ...), custom_call_target="tpu_custom_call" | custom-call | tf_op jit(solution)/shard_map/pallas_call | solution.py:251
  (38 shorter events, 6.1 us)
Async XLA Ops:
  2.8 33.4 %collective-permute-start.7 = (bf16[96,2048]{1,0:T(8,128)(2,1)S(1)}, bf16[96,2048]{1,0:T(8,128)(2,1)S(1)}, u32[]{:S(2)}, u32[]{:S(2)}) collective-permute-start(bf16[96,2048]{1,0:T(8,128)(2,1)S(1)} %get-tuple-element.27.refs_8_), channel_id=1, source_target_pairs={{0,2},{1,3},{2,0},{3,1},{4,6},{5,7},{6,4},{7,5},{8,10},{9,11},{10,... | collective-permute-start | bytes 1179656 | tf_op jit(solution)/shard_map/ppermute | solution.py:588
  5.8 31.9 %collective-permute-start.11 = (bf16[96,2048]{1,0:T(8,128)(2,1)S(1)}, bf16[96,2048]{1,0:T(8,128)(2,1)}, u32[]{:S(2)}, u32[]{:S(2)}) collective-permute-start(bf16[96,2048]{1,0:T(8,128)(2,1)S(1)} %get-tuple-element.28.refs_12_), channel_id=1, source_target_pairs={{0,4},{1,5},{2,6},{3,7},{4,0},{5,1},{6,2},{7,3},{8,12},{9,13},{10,... | collective-permute-start | bytes 1179656 | tf_op jit(solution)/shard_map/ppermute | solution.py:588
  19.7 25.2 %all-to-all-start = ((bf16[32,16,256]{2,1,0:T(8,128)(2,1)}), bf16[32,16,256]{2,1,0:T(8,128)(2,1)S(1)}, u32[]{:S(2)}, u32[]{:S(2)}) async-start(bf16[32,16,256]{2,1,0:T(8,128)(2,1)} %bitcast.18), calls=%async_computation | async-start | bytes 524288 | tf_op jit(solution)/shard_map/all_to_all | solution.py:648
  23.7 11.0 %collective-permute-start = (bf16[16,2048]{1,0:T(8,128)(2,1)}, bf16[16,2048]{1,0:T(8,128)(2,1)}, u32[]{:S(2)}, u32[]{:S(2)}) collective-permute-start(bf16[16,2048]{1,0:T(8,128)(2,1)} %get-tuple-element.26.refs_0_), channel_id=1, source_target_pairs={{0,8},{1,9},{2,10},{3,11},{4,12},{5,13},{6,14},{7,15},{8,16},{9,17... | collective-permute-start | bytes 196616 | tf_op jit(solution)/shard_map/ppermute | solution.py:591
  25.5 12.7 %collective-permute-start.1 = (bf16[16,2048]{1,0:T(8,128)(2,1)}, bf16[16,2048]{1,0:T(8,128)(2,1)S(1)}, u32[]{:S(2)}, u32[]{:S(2)}) collective-permute-start(bf16[16,2048]{1,0:T(8,128)(2,1)} %get-tuple-element.26.refs_0_), channel_id=1, source_target_pairs={{0,16},{1,17},{2,18},{3,19},{4,20},{5,21},{6,22},{7,23},{8,24},{9,... | collective-permute-start | bytes 196616 | tf_op jit(solution)/shard_map/ppermute | solution.py:591
  27.9 28.6 %collective-permute-start.8 = (bf16[96,2048]{1,0:T(8,128)(2,1)S(1)}, bf16[96,2048]{1,0:T(8,128)(2,1)}, u32[]{:S(2)}, u32[]{:S(2)}) collective-permute-start(bf16[96,2048]{1,0:T(8,128)(2,1)S(1)} %get-tuple-element.27.refs_8_), channel_id=1, source_target_pairs={{0,4},{1,5},{2,6},{3,7},{4,0},{5,1},{6,2},{7,3},{8,12},{9,13},{10,... | collective-permute-start | bytes 1179656 | tf_op jit(solution)/shard_map/ppermute | solution.py:588
  34.7 21.9 %collective-permute-start.10 = (bf16[96,2048]{1,0:T(8,128)(2,1)S(1)}, bf16[96,2048]{1,0:T(8,128)(2,1)}, u32[]{:S(2)}, u32[]{:S(2)}) collective-permute-start(bf16[96,2048]{1,0:T(8,128)(2,1)S(1)} %get-tuple-element.28.refs_12_), channel_id=1, source_target_pairs={{0,2},{1,3},{2,0},{3,1},{4,6},{5,7},{6,4},{7,5},{8,10},{9,11},{10,... | collective-permute-start | bytes 1179656 | tf_op jit(solution)/shard_map/ppermute | solution.py:588
  36.2 20.4 %collective-permute-start.9 = (bf16[96,2048]{1,0:T(8,128)(2,1)S(1)}, bf16[96,2048]{1,0:T(8,128)(2,1)}, u32[]{:S(2)}, u32[]{:S(2)}) collective-permute-start(bf16[96,2048]{1,0:T(8,128)(2,1)S(1)} %collective-permute-done.7.refs_9_), channel_id=1, source_target_pairs={{0,4},{1,5},{2,6},{3,7},{4,0},{5,1},{6,2},{7,3},{8,12},{9,13},{10,... | collective-permute-start | bytes 1179656 | tf_op jit(solution)/shard_map/ppermute | solution.py:588
  37.7 18.9 %collective-permute-start.12 = (bf16[96,2048]{1,0:T(8,128)(2,1)}, bf16[96,2048]{1,0:T(8,128)(2,1)}, u32[]{:S(2)}, u32[]{:S(2)}) collective-permute-start(bf16[96,2048]{1,0:T(8,128)(2,1)} %collective-permute-done.11.refs_14_), channel_id=1, source_target_pairs={{0,2},{1,3},{2,0},{3,1},{4,6},{5,7},{6,4},{7,5},{8,10},{9,11},{10,... | collective-permute-start | bytes 1179656 | tf_op jit(solution)/shard_map/ppermute | solution.py:588
  38.2 5.9 %copy-start.3 = (bf16[16,2048]{1,0:T(8,128)(2,1)}, bf16[16,2048]{1,0:T(8,128)(2,1)S(1)}, u32[]{:S(2)}) copy-start(bf16[16,2048]{1,0:T(8,128)(2,1)S(1)} %collective-permute-done.1.refs_2_) | copy-start | bytes 196612
  38.2 4.5 %collective-permute-start.2 = (bf16[16,2048]{1,0:T(8,128)(2,1)}, bf16[16,2048]{1,0:T(8,128)(2,1)S(1)}, u32[]{:S(2)}, u32[]{:S(2)}) collective-permute-start(bf16[16,2048]{1,0:T(8,128)(2,1)} %get-tuple-element.26.refs_0_), channel_id=1, source_target_pairs={{0,24},{1,25},{2,26},{3,27},{4,28},{5,29},{6,30},{7,31},{8,0},{9,1... | collective-permute-start | bytes 196616 | tf_op jit(solution)/shard_map/ppermute | solution.py:591
  42.7 1.5 %copy-start.5 = (bf16[16,2048]{1,0:T(8,128)(2,1)}, bf16[16,2048]{1,0:T(8,128)(2,1)S(1)}, u32[]{:S(2)}) copy-start(bf16[16,2048]{1,0:T(8,128)(2,1)S(1)} %collective-permute-done.2.refs_3_) | copy-start | bytes 196612
  42.7 1.5 %collective-permute-start.3 = (bf16[16,2048]{1,0:T(8,128)(2,1)}, bf16[16,2048]{1,0:T(8,128)(2,1)S(1)}, u32[]{:S(2)}, u32[]{:S(2)}) collective-permute-start(bf16[16,2048]{1,0:T(8,128)(2,1)} %get-tuple-element.26.refs_0_), channel_id=1, source_target_pairs={{0,1},{1,0},{2,3},{3,2},{4,5},{5,4},{6,7},{7,6},{8,9},{9,8},{10,11... | collective-permute-start | bytes 196616 | tf_op jit(solution)/shard_map/ppermute | solution.py:588
  44.8 8.8 %collective-permute-start.4 = (bf16[16,2048]{1,0:T(8,128)(2,1)}, bf16[16,2048]{1,0:T(8,128)(2,1)}, u32[]{:S(2)}, u32[]{:S(2)}) collective-permute-start(bf16[16,2048]{1,0:T(8,128)(2,1)} %collective-permute-done.refs_1_), channel_id=1, source_target_pairs={{0,1},{1,0},{2,3},{3,2},{4,5},{5,4},{6,7},{7,6},{8,9},{9,8},{10,11... | collective-permute-start | bytes 196616 | tf_op jit(solution)/shard_map/ppermute | solution.py:588
  49.1 21.2 %all-to-all-start.1 = ((bf16[32,16,256]{2,1,0:T(8,128)(2,1)}), bf16[32,16,256]{2,1,0:T(8,128)(2,1)S(1)}, u32[]{:S(2)}, u32[]{:S(2)}) async-start(bf16[32,16,256]{2,1,0:T(8,128)(2,1)} %shard_map.213), calls=%async_computation.1 | async-start | bytes 524288 | tf_op jit(solution)/shard_map/all_to_all | solution.py:661
  53.6 22.5 %copy-start = (bf16[512,384]{1,0:T(8,128)(2,1)S(1)}, bf16[512,384]{1,0:T(8,128)(2,1)}, u32[]{:S(2)}) copy-start(bf16[512,384]{1,0:T(8,128)(2,1)} %get-tuple-element.23.mix) | copy-start | bytes 1179652
  53.6 22.5 %copy-start.1 = (f32[16,2048]{1,0:T(8,128)S(1)}, f32[16,2048]{1,0:T(8,128)}, u32[]{:S(2)}) copy-start(f32[16,2048]{1,0:T(8,128)} %get-tuple-element.21.base) | copy-start | bytes 393220
  53.6 1.5 %collective-permute-start.5 = (bf16[16,2048]{1,0:T(8,128)(2,1)}, bf16[16,2048]{1,0:T(8,128)(2,1)S(1)}, u32[]{:S(2)}, u32[]{:S(2)}) collective-permute-start(bf16[16,2048]{1,0:T(8,128)(2,1)} %copy-done.3), channel_id=1, source_target_pairs={{0,1},{1,0},{2,3},{3,2},{4,5},{5,4},{6,7},{7,6},{8,9},{9,8},{10,11... | collective-permute-start | bytes 196616 | tf_op jit(solution)/shard_map/ppermute | solution.py:588
  55.1 1.5 %collective-permute-start.6 = (bf16[16,2048]{1,0:T(8,128)(2,1)}, bf16[16,2048]{1,0:T(8,128)(2,1)S(1)}, u32[]{:S(2)}, u32[]{:S(2)}) collective-permute-start(bf16[16,2048]{1,0:T(8,128)(2,1)} %copy-done.5), channel_id=1, source_target_pairs={{0,1},{1,0},{2,3},{3,2},{4,5},{5,4},{6,7},{7,6},{8,9},{9,8},{10,11... | collective-permute-start | bytes 196616 | tf_op jit(solution)/shard_map/ppermute | solution.py:588
  56.6 0.8 %copy-start.2 = (bf16[16,2048]{1,0:T(8,128)(2,1)S(1)}, bf16[16,2048]{1,0:T(8,128)(2,1)}, u32[]{:S(2)}) copy-start(bf16[16,2048]{1,0:T(8,128)(2,1)} %get-tuple-element.26.refs_0_) | copy-start | bytes 196612
  63.9 1.6 %collective-permute-start.13 = (bf16[64,2048]{1,0:T(8,128)(2,1)S(1)}, bf16[64,2048]{1,0:T(8,128)(2,1)S(1)}, u32[]{:S(2)}, u32[]{:S(2)}) collective-permute-start(bf16[64,2048]{1,0:T(8,128)(2,1)S(1)} %get-tuple-element.30), channel_id=1, source_target_pairs={{0,1},{1,0},{2,3},{3,2},{4,5},{5,4},{6,7},{7,6},{8,9},{9,8},{10,11... | collective-permute-start | bytes 786440 | tf_op jit(solution)/shard_map/ppermute | solution.py:588
  65.5 6.2 %collective-permute-start.14 = (bf16[16,2048]{1,0:T(8,128)(2,1)S(1)}, bf16[16,2048]{1,0:T(8,128)(2,1)S(1)}, u32[]{:S(2)}, u32[]{:S(2)}) collective-permute-start(bf16[16,2048]{1,0:T(8,128)(2,1)S(1)} %get-tuple-element.32), channel_id=1, source_target_pairs={{0,24},{1,25},{2,26},{3,27},{4,28},{5,29},{6,30},{7,31},{8,0},{9,1... | collective-permute-start | bytes 196616 | tf_op jit(solution)/shard_map/ppermute | solution.py:591
  69.2 6.9 %collective-permute-start.15 = (bf16[16,2048]{1,0:T(8,128)(2,1)S(1)}, bf16[16,2048]{1,0:T(8,128)(2,1)S(1)}, u32[]{:S(2)}, u32[]{:S(2)}) collective-permute-start(bf16[16,2048]{1,0:T(8,128)(2,1)S(1)} %get-tuple-element.33), channel_id=1, source_target_pairs={{0,16},{1,17},{2,18},{3,19},{4,20},{5,21},{6,22},{7,23},{8,24},{9,... | collective-permute-start | bytes 196616 | tf_op jit(solution)/shard_map/ppermute | solution.py:591
  69.2 6.9 %collective-permute-start.16 = (bf16[16,2048]{1,0:T(8,128)(2,1)S(1)}, bf16[16,2048]{1,0:T(8,128)(2,1)S(1)}, u32[]{:S(2)}, u32[]{:S(2)}) collective-permute-start(bf16[16,2048]{1,0:T(8,128)(2,1)S(1)} %get-tuple-element.34), channel_id=1, source_target_pairs={{0,8},{1,9},{2,10},{3,11},{4,12},{5,13},{6,14},{7,15},{8,16},{9,17... | collective-permute-start | bytes 196616 | tf_op jit(solution)/shard_map/ppermute | solution.py:591
  (4 other events, 3.1 us)

commit v3 on v2

--- a/solution.py
+++ b/solution.py
@@ -57,14 +57,10 @@
     branch_hbm,
     dispatch,
     query_hbm,
-    key_hbm,
-    value_hbm,
     keys_hbm,
     values_hbm,
     out_hbm,
     expert_gate_hbm,
-    new_keys,
-    new_values,
     middle_hbm,
     ffn_hbm,
     outgoing_hbm,
@@ -77,8 +73,6 @@
     ffn_gain,
     branch_gate,
     query_w,
-    key_w,
-    value_w,
     keys,
     values,
     out_w,
@@ -88,7 +82,7 @@
     blocked,
     weights_t,
     small_sems,
-    weight_sems,
+    query_sem,
     key_sems,
     value_sems,
     out_sem,
@@ -115,35 +109,29 @@
         )
     ]
     expert_copy = pltpu.make_async_copy(expert_gate_hbm, expert_gate, expert_sem)
-    first = [
-        pltpu.make_async_copy(query_hbm, query_w, weight_sems.at[0]),
-        pltpu.make_async_copy(key_hbm, key_w, weight_sems.at[1]),
-        pltpu.make_async_copy(value_hbm, value_w, weight_sems.at[2]),
-    ]
+    query_copy = pltpu.make_async_copy(query_hbm, query_w, query_sem)
+    batches = key_sems.shape[0]
+    batch = seqs // batches
     key_copies = [
         pltpu.make_async_copy(
-            keys_hbm.at[:, pl.ds(c * CHUNK, CHUNK), :],
-            keys.at[:, pl.ds(c * CHUNK, CHUNK), :],
-            key_sems.at[c],
+            keys_hbm.at[pl.ds(b * batch, batch)], keys.at[pl.ds(b * batch, batch)], key_sems.at[b]
         )
-        for c in range(chunks)
+        for b in range(batches)
     ]
     value_copies = [
         pltpu.make_async_copy(
-            values_hbm.at[pl.ds(p * 2, 2)], values.at[pl.ds(p * 2, 2)], value_sems.at[p]
+            values_hbm.at[pl.ds(b * batch, batch)],
+            values.at[pl.ds(b * batch, batch)],
+            value_sems.at[b],
         )
-        for p in range(pairs)
+        for b in range(batches)
     ]
     out_copy = pltpu.make_async_copy(out_hbm, out_w, out_sem)
     for copy in small:
         copy.start()
-    for copy in first:
+    query_copy.start()
+    for copy in key_copies:
         copy.start()
-    for copy in reversed(key_copies):
-        copy.start()
-    for copy in value_copies:
-        copy.start()
-    out_copy.start()
 
     for copy in small:
         copy.wait()
@@ -169,11 +157,12 @@
     ).astype(bf16)
     later = (iota((CHUNK, CHUNK), 1) > iota((CHUNK, CHUNK), 0)).astype(bf16)
 
-    for copy in first:
-        copy.wait()
+    query_copy.wait()
+    for copy in value_copies:
+        copy.start()
+    out_copy.start()
+    expert_copy.start()
     queries = matmul(normed, query_w[...]).astype(bf16)
-    new_keys[...] = matmul(normed, key_w[...]).astype(bf16)
-    new_values[...] = matmul(normed, value_w[...]).astype(bf16)
 
     spread_q = jnp.where(own_head, matmul(spread, queries), 0.0).astype(bf16)
     by_head = jnp.transpose(matmul(spread_q, fold))
@@ -184,9 +173,10 @@
             bf16
         )
 
+    for copy in key_copies:
+        copy.wait()
     carry = jnp.zeros((1, lanes), f32)
     for c in reversed(range(chunks)):
-        key_copies[c].wait()
         rows = slice(c * CHUNK, (c + 1) * CHUNK)
         key_rows = jnp.concatenate([keys[n, rows, :] for n in range(seqs)], axis=1)
         scores = matmul(key_rows, blocked[...]) * HEAD ** (-0.5) + lane_bias
@@ -200,10 +190,10 @@
         taken = jnp.where(live, jnp.exp(log_take + after), 0.0)
         weights_t[:, rows] = jnp.transpose(taken).astype(bf16)
 
-    expert_copy.start()
     pieces = []
     for p in range(pairs):
-        value_copies[p].wait()
+        if 2 * p % batch == 0:
+            value_copies[2 * p // batch].wait()
         value_rows = jnp.concatenate([values[2 * p], values[2 * p + 1]], axis=1)
         mixed = matmul(weights_t[2 * p * HEADS : 2 * (p + 1) * HEADS, :], value_rows)
         pieces.append(mixed[:HEADS, :KV_WIDTH])
@@ -264,29 +254,27 @@
 
 def attend(args, out_rows, out_cut):
     hidden = args[2]
-    keys = args[10]
+    keys = args[8]
     seqs, width = hidden.shape
     cache_len = keys.shape[1]
     return call(
         attend_kernel,
         (
-            shaped((seqs, KV_WIDTH), bf16),
-            shaped((seqs, KV_WIDTH), bf16),
             pltpu.HBM((seqs, width), f32),
             pltpu.HBM((seqs, width), bf16),
             pltpu.HBM((out_rows, out_cut), bf16),
             shaped((seqs, 128), f32),
         )
-        + tuple(pltpu.VMEM(a.shape, a.dtype) for a in args[13:]),
+        + tuple(pltpu.VMEM(a.shape, a.dtype) for a in args[11:]),
         tuple(arg if i == 6 else in_hbm(arg) for i, arg in enumerate(args)),
-        [HBM] * 6 + [VMEM] + [HBM] * 7,
-        [VMEM] * 2 + [HBM] * 3 + [VMEM] * 2,
+        [HBM] * 6 + [VMEM] + [HBM] * 5,
+        [HBM] * 3 + [VMEM] * 2,
         [
             pltpu.SMEM(args[0].shape, jnp.int32),
             pltpu.SMEM(args[1].shape, f32),
         ]
         + [pltpu.VMEM(a.shape, a.dtype) for a in args[2:6]]
-        + [pltpu.VMEM(a.shape, a.dtype) for a in args[7:13]]
+        + [pltpu.VMEM(a.shape, a.dtype) for a in args[7:11]]
         + [
             pltpu.VMEM((seqs, width), f32),
             pltpu.VMEM((seqs, width), bf16),
@@ -294,9 +282,9 @@
             pltpu.VMEM((seqs * KV_WIDTH, seqs * HEADS), bf16),
             pltpu.VMEM((seqs * HEADS, cache_len), bf16),
             pltpu.SemaphoreType.DMA((6,)),
-            pltpu.SemaphoreType.DMA((3,)),
-            pltpu.SemaphoreType.DMA((cache_len // CHUNK,)),
-            pltpu.SemaphoreType.DMA((seqs // 2,)),
+            pltpu.SemaphoreType.DMA,
+            pltpu.SemaphoreType.DMA((4,)),
+            pltpu.SemaphoreType.DMA((4,)),
             pltpu.SemaphoreType.DMA,
             pltpu.SemaphoreType.DMA,
             pltpu.SemaphoreType.DMA((3,)),
@@ -305,12 +293,26 @@
     )
 
 
+def project(hidden, gain, key_w, value_w):
+    def kernel(rows, gains, left, right, left_out, right_out):
+        normed = rms_rows(rows[...].astype(f32), gains[...])
+        left_out[...] = matmul(normed, left[...]).astype(bf16)
+        right_out[...] = matmul(normed, right[...]).astype(bf16)
+
+    return call(
+        kernel,
+        (shaped((hidden.shape[0], KV_WIDTH), bf16),) * 2,
+        (hidden, gain, key_w, value_w),
+        [VMEM] * 4,
+        [VMEM] * 2,
+    )
+
+
 def prepare(gate_t, up_t, down_t, routes_t, route_weights_t, capacity, cuts, experts):
     units, width = gate_t.shape
     seqs = routes_t.shape[1]
     rows = experts * capacity * cuts
     lanes = cuts * seqs
-    half = units // 2
 
     def kernel(
         gate,
@@ -318,8 +320,7 @@
         down,
         picks_hbm,
         pick_weights_hbm,
-        low,
-        high,
+        own,
         dispatch,
         combine_hbm,
         combine,
@@ -334,14 +335,8 @@
         for copy in small:
             copy.start()
         copies = [
-            pltpu.make_async_copy(gate, low.at[pl.ds(0, units)], sems.at[0]),
-            pltpu.make_async_copy(
-                up.at[pl.ds(0, half)], low.at[pl.ds(units, half)], sems.at[1]
-            ),
-            pltpu.make_async_copy(
-                up.at[pl.ds(half, half)], high.at[pl.ds(0, half)], sems.at[2]
-            ),
-            pltpu.make_async_copy(down, high.at[pl.ds(half, units)], sems.at[3]),
+            pltpu.make_async_copy(source, own.at[pl.ds(i * units, units)], sems.at[i])
+            for i, source in enumerate((gate, up, down))
         ]
         for copy in copies:
             copy.start()
@@ -377,14 +372,13 @@
     return call(
         kernel,
         (
-            shaped((units + half, width), bf16),
-            shaped((units + half, width), bf16),
+            shaped((3 * units, width), bf16),
             shaped((rows, lanes), bf16),
             pltpu.HBM((rows, 3 * lanes), bf16),
         ),
         (gate_t, up_t, down_t, routes_t, route_weights_t),
         [HBM] * 5,
-        [HBM] * 2 + [VMEM] + [HBM],
+        [HBM] + [VMEM] + [HBM],
         [
             pltpu.VMEM((rows, 3 * lanes), bf16),
             pltpu.VMEM(routes_t.shape, jnp.int32),
@@ -460,47 +454,51 @@
     )
 
 
-def run_dense(tokens, lows, highs):
+def run_dense(tokens, pieces):
     seqs, width = tokens[0].shape
-    count = len(lows)
-    held = lows[0].shape[0]
-    half = held // 3
-    units = 2 * half
+    count = len(pieces)
+    units = pieces[0].shape[0] // 3
     total = len(tokens)
     kept = total // 2 * seqs
 
     def kernel(*refs):
         token_refs = refs[:total]
-        sources = refs[total : total + 2 * count]
-        keep, give = refs[total + 2 * count : total + 2 * count + 2]
-        weights, sems = refs[total + 2 * count + 2 :]
+        sources = refs[total : total + count]
+        keep, give, gates, ups, downs, sems = refs[total + count :]
         copies = [
-            pltpu.make_async_copy(source, weights.at[i], sems.at[i])
-            for i, source in enumerate(sources)
+            [
+                pltpu.make_async_copy(
+                    source.at[pl.ds(kind * units, units)],
+                    target.at[pl.ds(i * units, units)],
+                    sems.at[kind, i],
+                )
+                for i, source in enumerate(sources)
+            ]
+            for kind, target in enumerate((gates, ups, downs))
         ]
-        for copy in copies:
-            copy.start()
+        for group in copies:
+            for copy in group:
+                copy.start()
         rows = jnp.concatenate([ref[...] for ref in token_refs], axis=0)
-        for copy in copies:
+        for copy in copies[0]:
             copy.wait()
-        gates = [weights[j, :units] for j in range(count)]
-        ups = []
-        for j in range(count):
-            ups += [weights[j, units:], weights[count + j, :half]]
-        downs = [weights[count + j, half:] for j in range(count)]
-        hidden = jax.nn.silu(matmul_bt(rows, jnp.concatenate(gates, axis=0)))
-        hidden = hidden * matmul_bt(rows, jnp.concatenate(ups, axis=0))
-        partial = matmul(hidden.astype(bf16), jnp.concatenate(downs, axis=0))
+        hidden = jax.nn.silu(matmul_bt(rows, gates[...]))
+        for copy in copies[1]:
+            copy.wait()
+        hidden = hidden * matmul_bt(rows, ups[...])
+        for copy in copies[2]:
+            copy.wait()
+        partial = matmul(hidden.astype(bf16), downs[...])
         keep[...] = partial[:kept]
         give[...] = partial[kept:].astype(bf16)
 
     return call(
         kernel,
         (shaped((kept, width), f32), shaped((total * seqs - kept, width), bf16)),
-        (*tokens, *lows, *highs),
-        [VMEM] * total + [HBM] * (2 * count),
+        (*tokens, *pieces),
+        [VMEM] * total + [HBM] * count,
         [VMEM] * 2,
-        [pltpu.VMEM((2 * count, held, width), bf16), pltpu.SemaphoreType.DMA((2 * count,))],
+        [pltpu.VMEM((count * units, width), bf16)] * 3 + [pltpu.SemaphoreType.DMA((3, count))],
         32,
     )
 
@@ -592,7 +590,7 @@
             values, "ep", [(i, (i + steps * plane) % devices) for i in range(devices)]
         )
 
-    low, high, dispatch, combine = prepare(
+    own, dispatch, combine = prepare(
         in_hbm(dense_gate.T),
         in_hbm(dense_up.T),
         in_hbm(dense_down.T),
@@ -602,30 +600,11 @@
         cuts,
         experts_all,
     )
-    lows = [low]
-    highs = [high]
-    bits = 2
-    while bits < plane:
-        more_lows = [swap(low, bits)]
-        more_highs = [swap(high, bits)]
-        bits = 2 * bits
-        lows += more_lows
-        highs += more_highs
-    bits = 2
-    direct = {1 << (k + 1): k + 1 for k in range(len(lows) - 1)}
+    pieces = [own]
     for other in range(2, plane, 2):
-        if other in direct:
-            continue
-        first = other & -other
-        last = other ^ first
-        if last in direct:
-            lows.append(swap(lows[direct[first]], last))
-            highs.append(swap(highs[direct[last]], first))
-        else:
-            lows.append(swap(low, other))
-            highs.append(swap(high, other))
-
-    new_keys, new_values, middle, ffn_in, outgoing, gate_value, gate_w = attend(
+        pieces.append(swap(own, other))
+
+    middle, ffn_in, outgoing, gate_value, gate_w = attend(
         (
             lengths,
             score_bias,
@@ -635,8 +614,6 @@
             branch_gate.reshape(1, width),
             dispatch,
             query_weight,
-            key_weight,
-            value_weight,
             key_cache,
             value_cache,
             out_weight,
@@ -661,12 +638,18 @@
     returned = lax.all_to_all(
         expert_rows, "ep", split_axis=0, concat_axis=0, tiled=True
     )
-    kept, given = run_dense(chain, lows, highs)
+    kept, given = run_dense(chain, pieces)
     taken = swap(given, 1)
     own, *rest = merge(kept, taken, seqs)
     parts = [own]
     for k in range(1, layers):
         parts.append(climb(rest[k - 1], -k))
+    new_keys, new_values = project(
+        in_hbm(hidden_in),
+        in_hbm(attn_gain.reshape(1, width)),
+        in_hbm(key_weight),
+        in_hbm(value_weight),
+    )
     hidden_out = finish(middle, gate_value, combine, returned, parts)
     return (hidden_out, new_keys, new_values)
 

time: 77.5 us -> 72.9 us (0.941)
  waiting for transfers between devices: 20.3 us -> 24.5 us
  local copies, waits for them, and re-layouts: 3.99 us -> 0.01 us
  starting transfers between devices: 28.5 us -> 26.1 us
  Pallas kernels: 23.5 us -> 21.2 us
    all_to_all x1, waiting for transfers between devices: 0.01 us -> 11.1 us  [per_device(): lax.all_to_all(outgoing.reshape(devices, chunk, width // cuts), 'ep', spl...]
    ppermute x6, waiting for transfers between devices: 15.1 us -> 10.4 us  [climb(): lax.ppermute(values, 'ep', [(i, (i + steps * plane) % devices) for i in r...]
    ppermute x11 -> x8, starting transfers between devices: 10.6 us -> 5.98 us  [swap(): return lax.ppermute(values, 'ep', [(i, i ^ bits) for i in range(devices)])]
    unnamed x18 -> x6, local copies, waits for them, and re-layouts: 3.99 us -> 0.01 us
    all_to_all x1, starting transfers between devices: 3.97 us -> 6.32 us  [per_device(): lax.all_to_all(outgoing.reshape(devices, chunk, width // cuts), 'ep', spl...]
    pallas_call x6 -> x7, Pallas kernels: 23.5 us -> 21.2 us  [call(): pl.pallas_call(kernel, out_shape=out_shape, in_specs=in_specs, out_specs=...]
    ppermute x11 -> x8, waiting for transfers between devices: 5.19 us -> 3.02 us  [swap(): return lax.ppermute(values, 'ep', [(i, i ^ bits) for i in range(devices)])]
  transfers between devices with their start and end apart: 19 -> 16, of which waited for: 8 -> 7; matrix products, arithmetic and copies ran while one was open for 0% -> 0% of each run, Pallas kernels for 27% -> 25%
where the time goes in v3:
time: 72.9 us; the launch traced here: 72.5 us
  starting transfers between devices  26.1 us (36%)
  waiting for transfers between devices  24.5 us (34%)
  Pallas kernels  21.2 us (29%)
  between operations  0.74 us (1%)
    pallas_call x7, Pallas kernels, call(): pl.pallas_call(kernel, out_shape=out_shape, in_specs=in_specs, out_specs=...  21.2 us
    all_to_all x1, waiting for transfers between devices, per_device(): lax.all_to_all(outgoing.reshape(devices, chunk, width // cuts), 'ep', spl...  11.1 us
    ppermute x6, waiting for transfers between devices, climb(): lax.ppermute(values, 'ep', [(i, (i + steps * plane) % devices) for i in r...  10.4 us
    ppermute x6, starting transfers between devices, climb(): lax.ppermute(values, 'ep', [(i, (i + steps * plane) % devices) for i in r...  8.89 us
    all_to_all x1, starting transfers between devices, per_device(): lax.all_to_all(outgoing.reshape(devices, chunk, width // cuts), 'ep', spl...  6.32 us
    ppermute x8, starting transfers between devices, swap(): return lax.ppermute(values, 'ep', [(i, i ^ bits) for i in range(devices)])  5.98 us
    all_to_all x1, starting transfers between devices, per_device(): lax.all_to_all(expert_rows, 'ep', split_axis=0, concat_axis=0, tiled=True)  4.86 us
    ppermute x8, waiting for transfers between devices, swap(): return lax.ppermute(values, 'ep', [(i, i ^ bits) for i in range(devices)])  3.02 us
  transfers between devices with their start and end apart: 16, of which 7 were waited for; matrix products, arithmetic and copies ran while one was open for 0% of the time, Pallas kernels for 25%

profile of v3, /device:TPU:0, one launch (start us, length us, event | category | flops | bytes accessed | tf_op | source)
XLA Modules:
  0.0 72.5 jit_solution(9748527218669984514)
XLA Ops:
  0.6 2.1 %shard_map.211 = (bf16[192,2048]{1,0:T(8,128)(2,1)S(1)}, bf16[512,128]{1,0:T(8,128)(2,1)S(1)}, bf16[512,384]{1,0:T(8,128)(2,1)}) custom-call(bf16[64,2048]{1,0:T(8,128)(2,1)} %bitcast.15, bf16[64,2048]{1,0:T(8,128)(2,1)} %bitcast.16, bf16[64,2048]{1,0:T(8,128)(2,1)} %bitcast.17, s32[4,16]{1,0:T(4,128)} %bitcast.23, f32[4,16]{1,0:T(4,128)} %bitcast.24), custom_call_target="tpu_custom_call" | custom-call | tf_op jit(solution)/shard_map/pallas_call | solution.py:241
  2.8 3.0 %collective-permute-start.7 = (bf16[192,2048]{1,0:T(8,128)(2,1)S(1)}, bf16[192,2048]{1,0:T(8,128)(2,1)}, u32[]{:S(2)}, u32[]{:S(2)}) collective-permute-start(bf16[192,2048]{1,0:T(8,128)(2,1)S(1)} %get-tuple-element.26.refs_8_), channel_id=1, source_target_pairs={{0,2},{1,3},{2,0},{3,1},{4,6},{5,7},{6,4},{7,5},{8,10},{9,11},{10,... | collective-permute-start | bytes 2359304 | tf_op jit(solution)/shard_map/ppermute | solution.py:586
  5.8 1.5 %collective-permute-start.8 = (bf16[192,2048]{1,0:T(8,128)(2,1)S(1)}, bf16[192,2048]{1,0:T(8,128)(2,1)}, u32[]{:S(2)}, u32[]{:S(2)}) collective-permute-start(bf16[192,2048]{1,0:T(8,128)(2,1)S(1)} %get-tuple-element.26.refs_8_), channel_id=1, source_target_pairs={{0,4},{1,5},{2,6},{3,7},{4,0},{5,1},{6,2},{7,3},{8,12},{9,13},{10,... | collective-permute-start | bytes 2359304 | tf_op jit(solution)/shard_map/ppermute | solution.py:586
  7.3 8.8 %shard_map.212 = (f32[16,2048]{1,0:T(8,128)}, bf16[16,2048]{1,0:T(8,128)(2,1)}, bf16[512,256]{1,0:T(8,128)(2,1)}, f32[16,128]{1,0:T(8,128)S(1)}, bf16[2048,512]{1,0:T(8,128)(2,1)S(1)}) custom-call(s32[16]{0:T(128)} %lengths_hbm.1, f32[8]{0:T(128)} %bias_hbm.1, bf16[16,2048]{1,0:T(8,128)(2,1)} %rows.1, f32[1,2048]{1,0:T(1,128)} %bitcast.19, ...), custom_call_target="tpu_custom_call" | custom-call | tf_op jit(solution)/shard_map/pallas_call | solution.py:241
  16.2 6.3 %all-to-all-start = ((bf16[32,16,256]{2,1,0:T(8,128)(2,1)}), bf16[32,16,256]{2,1,0:T(8,128)(2,1)S(1)}, u32[]{:S(2)}, u32[]{:S(2)}) async-start(bf16[32,16,256]{2,1,0:T(8,128)(2,1)} %bitcast.18), calls=%async_computation | async-start | bytes 524288 | tf_op jit(solution)/shard_map/all_to_all | solution.py:625
  22.5 1.8 %collective-permute-start = (bf16[16,2048]{1,0:T(8,128)(2,1)}, bf16[16,2048]{1,0:T(8,128)(2,1)S(1)}, u32[]{:S(2)}, u32[]{:S(2)}) collective-permute-start(bf16[16,2048]{1,0:T(8,128)(2,1)} %get-tuple-element.25.refs_0_), channel_id=1, source_target_pairs={{0,8},{1,9},{2,10},{3,11},{4,12},{5,13},{6,14},{7,15},{8,16},{9,17... | collective-permute-start | bytes 196616 | tf_op jit(solution)/shard_map/ppermute | solution.py:589
  24.3 2.4 %collective-permute-start.1 = (bf16[16,2048]{1,0:T(8,128)(2,1)}, bf16[16,2048]{1,0:T(8,128)(2,1)S(1)}, u32[]{:S(2)}, u32[]{:S(2)}) collective-permute-start(bf16[16,2048]{1,0:T(8,128)(2,1)} %get-tuple-element.25.refs_0_), channel_id=1, source_target_pairs={{0,16},{1,17},{2,18},{3,19},{4,20},{5,21},{6,22},{7,23},{8,24},{9,... | collective-permute-start | bytes 196616 | tf_op jit(solution)/shard_map/ppermute | solution.py:589
  26.7 6.6 %collective-permute-done.refs_1_ = bf16[16,2048]{1,0:T(8,128)(2,1)S(1)} collective-permute-done((bf16[16,2048]{1,0:T(8,128)(2,1)}, bf16[16,2048]{1,0:T(8,128)(2,1)S(1)}, u32[]{:S(2)}, u32[]{:S(2)}) %collective-permute-start) | collective-permute-done | bytes 65568 | tf_op jit(solution)/shard_map/ppermute | solution.py:589
  33.4 11.1 %all-to-all-done.rows = bf16[32,16,256]{2,1,0:T(8,128)(2,1)S(1)} async-done(((bf16[32,16,256]{2,1,0:T(8,128)(2,1)}), bf16[32,16,256]{2,1,0:T(8,128)(2,1)S(1)}, u32[]{:S(2)}, u32[]{:S(2)}) %all-to-all-start) | async-done | bytes 262176 | tf_op jit(solution)/shard_map/all_to_all | solution.py:625
  44.5 4.1 %shard_map.213 = bf16[32,16,256]{2,1,0:T(8,128)(2,1)} custom-call(bf16[32,16,256]{2,1,0:T(8,128)(2,1)S(1)} %all-to-all-done.rows, bf16[2048,512]{1,0:T(8,128)(2,1)S(1)} %get-tuple-element.24.gate, bf16[2048,512]{1,0:T(8,128)(2,1)} %bitcast.12, bf16[512,2048]{1,0:T(8,128)(2,1)} %bitcast.13), custom_call_target="tpu_custom_call" | custom-call | tf_op jit(solution)/shard_map/pallas_call | solution.py:241
  48.6 4.9 %all-to-all-start.1 = ((bf16[32,16,256]{2,1,0:T(8,128)(2,1)}), bf16[32,16,256]{2,1,0:T(8,128)(2,1)S(1)}, u32[]{:S(2)}, u32[]{:S(2)}) async-start(bf16[32,16,256]{2,1,0:T(8,128)(2,1)} %shard_map.213), calls=%async_computation.1 | async-start | bytes 524288 | tf_op jit(solution)/shard_map/all_to_all | solution.py:638
  53.5 0.3 collective-permute-start.3
  53.8 0.3 collective-permute-start.4
  54.1 0.7 %collective-permute-done.3.refs_4_ = bf16[16,2048]{1,0:T(8,128)(2,1)S(1)} collective-permute-done((bf16[16,2048]{1,0:T(8,128)(2,1)S(1)}, bf16[16,2048]{1,0:T(8,128)(2,1)S(1)}, u32[]{:S(2)}, u32[]{:S(2)}) %collective-permute-start.3) | collective-permute-done | bytes 65568 | tf_op jit(solution)/shard_map/ppermute | solution.py:586
  55.1 0.3 collective-permute-start.6
  55.3 0.7 %collective-permute-done.5.refs_6_ = bf16[16,2048]{1,0:T(8,128)(2,1)S(1)} collective-permute-done((bf16[16,2048]{1,0:T(8,128)(2,1)S(1)}, bf16[16,2048]{1,0:T(8,128)(2,1)S(1)}, u32[]{:S(2)}, u32[]{:S(2)}) %collective-permute-start.5) | collective-permute-done | bytes 65568 | tf_op jit(solution)/shard_map/ppermute | solution.py:586
  56.3 3.0 %shard_map.214 = (f32[64,2048]{1,0:T(8,128)S(1)}, bf16[64,2048]{1,0:T(8,128)(2,1)S(1)}) custom-call(bf16[16,2048]{1,0:T(8,128)(2,1)S(1)} %copy-done.2, bf16[16,2048]{1,0:T(8,128)(2,1)S(1)} %collective-permute-done.refs_1_, bf16[16,2048]{1,0:T(8,128)(2,1)S(1)} %collective-permute-done.1.refs_2_, bf16[16,2048]{1,0:T(8,128)(2,1)S(1)} %collective-permute-done.2.refs_3_, ...), custom_call_target="tpu_custom_call" | custom-call | tf_op jit(solution)/shard_map/pallas_call | solution.py:241
  59.3 0.3 collective-permute-start.10
  59.6 1.3 %collective-permute-done.10.right = bf16[64,2048]{1,0:T(8,128)(2,1)S(1)} collective-permute-done((bf16[64,2048]{1,0:T(8,128)(2,1)S(1)}, bf16[64,2048]{1,0:T(8,128)(2,1)S(1)}, u32[]{:S(2)}, u32[]{:S(2)}) %collective-permute-start.10) | collective-permute-done | bytes 262176 | tf_op jit(solution)/shard_map/ppermute | solution.py:586
  61.0 3.6 %collective-permute-start.11 = (bf16[16,2048]{1,0:T(8,128)(2,1)S(1)}, bf16[16,2048]{1,0:T(8,128)(2,1)S(1)}, u32[]{:S(2)}, u32[]{:S(2)}) collective-permute-start(bf16[16,2048]{1,0:T(8,128)(2,1)S(1)} %get-tuple-element.30), channel_id=1, source_target_pairs={{0,24},{1,25},{2,26},{3,27},{4,28},{5,29},{6,30},{7,31},{8,0},{9,1... | collective-permute-start | bytes 196616 | tf_op jit(solution)/shard_map/ppermute | solution.py:589
  64.5 1.1 %collective-permute-start.13 = (bf16[16,2048]{1,0:T(8,128)(2,1)S(1)}, bf16[16,2048]{1,0:T(8,128)(2,1)S(1)}, u32[]{:S(2)}, u32[]{:S(2)}) collective-permute-start(bf16[16,2048]{1,0:T(8,128)(2,1)S(1)} %get-tuple-element.32), channel_id=1, source_target_pairs={{0,8},{1,9},{2,10},{3,11},{4,12},{5,13},{6,14},{7,15},{8,16},{9,17... | collective-permute-start | bytes 196616 | tf_op jit(solution)/shard_map/ppermute | solution.py:589
  65.6 2.2 %shard_map.217 = (bf16[16,128]{1,0:T(8,128)(2,1)}, bf16[16,128]{1,0:T(8,128)(2,1)}) custom-call(bf16[16,2048]{1,0:T(8,128)(2,1)} %rows.1, f32[1,2048]{1,0:T(1,128)} %bitcast.20, bf16[2048,128]{1,0:T(8,128)(2,1)} %left.1, bf16[2048,128]{1,0:T(8,128)(2,1)} %right.1), custom_call_target="tpu_custom_call" | custom-call | tf_op jit(solution)/shard_map/pallas_call | solution.py:241
  67.8 3.8 %collective-permute-done.12.refs_2_ = bf16[16,2048]{1,0:T(8,128)(2,1)S(1)} collective-permute-done((bf16[16,2048]{1,0:T(8,128)(2,1)S(1)}, bf16[16,2048]{1,0:T(8,128)(2,1)S(1)}, u32[]{:S(2)}, u32[]{:S(2)}) %collective-permute-start.12) | collective-permute-done | bytes 65568 | tf_op jit(solution)/shard_map/ppermute | solution.py:589
  71.6 0.9 %shard_map.216 = bf16[16,2048]{1,0:T(8,128)(2,1)} custom-call(f32[16,2048]{1,0:T(8,128)S(1)} %copy-done.1, f32[16,128]{1,0:T(8,128)S(1)} %get-tuple-element.21.gate, bf16[512,384]{1,0:T(8,128)(2,1)S(1)} %copy-done, bf16[32,16,256]{2,1,0:T(8,128)(2,1)S(1)} %all-to-all-done.1.rows, f32[16,2048]{1,0:T(8,128)S(1)} %get-tuple-element.29.refs_0_, ...), custom_call_target="tpu_custom_call" | custom-call | tf_op jit(solution)/shard_map/pallas_call | solution.py:241
  (21 shorter events, 0.6 us)
Async XLA Ops:
  2.8 53.5 %collective-permute-start.7 = (bf16[192,2048]{1,0:T(8,128)(2,1)S(1)}, bf16[192,2048]{1,0:T(8,128)(2,1)}, u32[]{:S(2)}, u32[]{:S(2)}) collective-permute-start(bf16[192,2048]{1,0:T(8,128)(2,1)S(1)} %get-tuple-element.26.refs_8_), channel_id=1, source_target_pairs={{0,2},{1,3},{2,0},{3,1},{4,6},{5,7},{6,4},{7,5},{8,10},{9,11},{10,... | collective-permute-start | bytes 2359304 | tf_op jit(solution)/shard_map/ppermute | solution.py:586
  5.8 50.5 %collective-permute-start.8 = (bf16[192,2048]{1,0:T(8,128)(2,1)S(1)}, bf16[192,2048]{1,0:T(8,128)(2,1)}, u32[]{:S(2)}, u32[]{:S(2)}) collective-permute-start(bf16[192,2048]{1,0:T(8,128)(2,1)S(1)} %get-tuple-element.26.refs_8_), channel_id=1, source_target_pairs={{0,4},{1,5},{2,6},{3,7},{4,0},{5,1},{6,2},{7,3},{8,12},{9,13},{10,... | collective-permute-start | bytes 2359304 | tf_op jit(solution)/shard_map/ppermute | solution.py:586
  7.3 49.0 %collective-permute-start.9 = (bf16[192,2048]{1,0:T(8,128)(2,1)S(1)}, bf16[192,2048]{1,0:T(8,128)(2,1)}, u32[]{:S(2)}, u32[]{:S(2)}) collective-permute-start(bf16[192,2048]{1,0:T(8,128)(2,1)S(1)} %get-tuple-element.26.refs_8_), channel_id=1, source_target_pairs={{0,6},{1,7},{2,4},{3,5},{4,2},{5,3},{6,0},{7,1},{8,14},{9,15},{10,... | collective-permute-start | bytes 2359304 | tf_op jit(solution)/shard_map/ppermute | solution.py:586
  16.2 28.3 %all-to-all-start = ((bf16[32,16,256]{2,1,0:T(8,128)(2,1)}), bf16[32,16,256]{2,1,0:T(8,128)(2,1)S(1)}, u32[]{:S(2)}, u32[]{:S(2)}) async-start(bf16[32,16,256]{2,1,0:T(8,128)(2,1)} %bitcast.18), calls=%async_computation | async-start | bytes 524288 | tf_op jit(solution)/shard_map/all_to_all | solution.py:625
  22.5 10.9 %collective-permute-start = (bf16[16,2048]{1,0:T(8,128)(2,1)}, bf16[16,2048]{1,0:T(8,128)(2,1)S(1)}, u32[]{:S(2)}, u32[]{:S(2)}) collective-permute-start(bf16[16,2048]{1,0:T(8,128)(2,1)} %get-tuple-element.25.refs_0_), channel_id=1, source_target_pairs={{0,8},{1,9},{2,10},{3,11},{4,12},{5,13},{6,14},{7,15},{8,16},{9,17... | collective-permute-start | bytes 196616 | tf_op jit(solution)/shard_map/ppermute | solution.py:589
  24.3 29.1 %collective-permute-start.1 = (bf16[16,2048]{1,0:T(8,128)(2,1)}, bf16[16,2048]{1,0:T(8,128)(2,1)S(1)}, u32[]{:S(2)}, u32[]{:S(2)}) collective-permute-start(bf16[16,2048]{1,0:T(8,128)(2,1)} %get-tuple-element.25.refs_0_), channel_id=1, source_target_pairs={{0,16},{1,17},{2,18},{3,19},{4,20},{5,21},{6,22},{7,23},{8,24},{9,... | collective-permute-start | bytes 196616 | tf_op jit(solution)/shard_map/ppermute | solution.py:589
  33.4 20.4 %collective-permute-start.2 = (bf16[16,2048]{1,0:T(8,128)(2,1)}, bf16[16,2048]{1,0:T(8,128)(2,1)S(1)}, u32[]{:S(2)}, u32[]{:S(2)}) collective-permute-start(bf16[16,2048]{1,0:T(8,128)(2,1)} %get-tuple-element.25.refs_0_), channel_id=1, source_target_pairs={{0,24},{1,25},{2,26},{3,27},{4,28},{5,29},{6,30},{7,31},{8,0},{9,1... | collective-permute-start | bytes 196616 | tf_op jit(solution)/shard_map/ppermute | solution.py:589
  44.5 9.0 %copy-start.2 = (bf16[16,2048]{1,0:T(8,128)(2,1)S(1)}, bf16[16,2048]{1,0:T(8,128)(2,1)}, u32[]{:S(2)}) copy-start(bf16[16,2048]{1,0:T(8,128)(2,1)} %get-tuple-element.25.refs_0_) | copy-start | bytes 196612
  48.6 19.2 %all-to-all-start.1 = ((bf16[32,16,256]{2,1,0:T(8,128)(2,1)}), bf16[32,16,256]{2,1,0:T(8,128)(2,1)S(1)}, u32[]{:S(2)}, u32[]{:S(2)}) async-start(bf16[32,16,256]{2,1,0:T(8,128)(2,1)} %shard_map.213), calls=%async_computation.1 | async-start | bytes 524288 | tf_op jit(solution)/shard_map/all_to_all | solution.py:638
  53.4 18.2 %copy-start = (bf16[512,384]{1,0:T(8,128)(2,1)S(1)}, bf16[512,384]{1,0:T(8,128)(2,1)}, u32[]{:S(2)}) copy-start(bf16[512,384]{1,0:T(8,128)(2,1)} %get-tuple-element.22.mix) | copy-start | bytes 1179652
  53.4 18.2 %copy-start.1 = (f32[16,2048]{1,0:T(8,128)S(1)}, f32[16,2048]{1,0:T(8,128)}, u32[]{:S(2)}) copy-start(f32[16,2048]{1,0:T(8,128)} %get-tuple-element.20.base) | copy-start | bytes 393220
  53.5 1.3 %collective-permute-start.3 = (bf16[16,2048]{1,0:T(8,128)(2,1)S(1)}, bf16[16,2048]{1,0:T(8,128)(2,1)S(1)}, u32[]{:S(2)}, u32[]{:S(2)}) collective-permute-start(bf16[16,2048]{1,0:T(8,128)(2,1)S(1)} %copy-done.2), channel_id=1, source_target_pairs={{0,1},{1,0},{2,3},{3,2},{4,5},{5,4},{6,7},{7,6},{8,9},{9,8},{10,11... | collective-permute-start | bytes 196616 | tf_op jit(solution)/shard_map/ppermute | solution.py:586
  53.8 1.3 %collective-permute-start.4 = (bf16[16,2048]{1,0:T(8,128)(2,1)S(1)}, bf16[16,2048]{1,0:T(8,128)(2,1)S(1)}, u32[]{:S(2)}, u32[]{:S(2)}) collective-permute-start(bf16[16,2048]{1,0:T(8,128)(2,1)S(1)} %collective-permute-done.refs_1_), channel_id=1, source_target_pairs={{0,1},{1,0},{2,3},{3,2},{4,5},{5,4},{6,7},{7,6},{8,9},{9,8},{10,11... | collective-permute-start | bytes 196616 | tf_op jit(solution)/shard_map/ppermute | solution.py:586
  54.8 1.3 %collective-permute-start.5 = (bf16[16,2048]{1,0:T(8,128)(2,1)S(1)}, bf16[16,2048]{1,0:T(8,128)(2,1)S(1)}, u32[]{:S(2)}, u32[]{:S(2)}) collective-permute-start(bf16[16,2048]{1,0:T(8,128)(2,1)S(1)} %collective-permute-done.1.refs_2_), channel_id=1, source_target_pairs={{0,1},{1,0},{2,3},{3,2},{4,5},{5,4},{6,7},{7,6},{8,9},{9,8},{10,11... | collective-permute-start | bytes 196616 | tf_op jit(solution)/shard_map/ppermute | solution.py:586
  55.1 1.3 %collective-permute-start.6 = (bf16[16,2048]{1,0:T(8,128)(2,1)S(1)}, bf16[16,2048]{1,0:T(8,128)(2,1)S(1)}, u32[]{:S(2)}, u32[]{:S(2)}) collective-permute-start(bf16[16,2048]{1,0:T(8,128)(2,1)S(1)} %collective-permute-done.2.refs_3_), channel_id=1, source_target_pairs={{0,1},{1,0},{2,3},{3,2},{4,5},{5,4},{6,7},{7,6},{8,9},{9,8},{10,11... | collective-permute-start | bytes 196616 | tf_op jit(solution)/shard_map/ppermute | solution.py:586
  59.3 1.6 %collective-permute-start.10 = (bf16[64,2048]{1,0:T(8,128)(2,1)S(1)}, bf16[64,2048]{1,0:T(8,128)(2,1)S(1)}, u32[]{:S(2)}, u32[]{:S(2)}) collective-permute-start(bf16[64,2048]{1,0:T(8,128)(2,1)S(1)} %get-tuple-element.28), channel_id=1, source_target_pairs={{0,1},{1,0},{2,3},{3,2},{4,5},{5,4},{6,7},{7,6},{8,9},{9,8},{10,11... | collective-permute-start | bytes 786440 | tf_op jit(solution)/shard_map/ppermute | solution.py:586
  61.0 6.9 %collective-permute-start.11 = (bf16[16,2048]{1,0:T(8,128)(2,1)S(1)}, bf16[16,2048]{1,0:T(8,128)(2,1)S(1)}, u32[]{:S(2)}, u32[]{:S(2)}) collective-permute-start(bf16[16,2048]{1,0:T(8,128)(2,1)S(1)} %get-tuple-element.30), channel_id=1, source_target_pairs={{0,24},{1,25},{2,26},{3,27},{4,28},{5,29},{6,30},{7,31},{8,0},{9,1... | collective-permute-start | bytes 196616 | tf_op jit(solution)/shard_map/ppermute | solution.py:589
  64.5 7.1 %collective-permute-start.12 = (bf16[16,2048]{1,0:T(8,128)(2,1)S(1)}, bf16[16,2048]{1,0:T(8,128)(2,1)S(1)}, u32[]{:S(2)}, u32[]{:S(2)}) collective-permute-start(bf16[16,2048]{1,0:T(8,128)(2,1)S(1)} %get-tuple-element.31), channel_id=1, source_target_pairs={{0,16},{1,17},{2,18},{3,19},{4,20},{5,21},{6,22},{7,23},{8,24},{9,... | collective-permute-start | bytes 196616 | tf_op jit(solution)/shard_map/ppermute | solution.py:589
  64.5 7.1 %collective-permute-start.13 = (bf16[16,2048]{1,0:T(8,128)(2,1)S(1)}, bf16[16,2048]{1,0:T(8,128)(2,1)S(1)}, u32[]{:S(2)}, u32[]{:S(2)}) collective-permute-start(bf16[16,2048]{1,0:T(8,128)(2,1)S(1)} %get-tuple-element.32), channel_id=1, source_target_pairs={{0,8},{1,9},{2,10},{3,11},{4,12},{5,13},{6,14},{7,15},{8,16},{9,17... | collective-permute-start | bytes 196616 | tf_op jit(solution)/shard_map/ppermute | solution.py:589

commit v4 on v3

--- a/solution.py
+++ b/solution.py
@@ -49,13 +49,15 @@
 
 
 def attend_kernel(
+    capacity,
     lengths_hbm,
     bias_hbm,
     hidden_hbm,
     attn_gain_hbm,
     ffn_gain_hbm,
     branch_hbm,
-    dispatch,
+    picks_hbm,
+    pick_weights_hbm,
     query_hbm,
     keys_hbm,
     values_hbm,
@@ -64,6 +66,7 @@
     middle_hbm,
     ffn_hbm,
     outgoing_hbm,
+    combine_hbm,
     gate_value,
     expert_gate,
     lengths,
@@ -72,6 +75,8 @@
     attn_gain,
     ffn_gain,
     branch_gate,
+    picks,
+    pick_weights,
     query_w,
     keys,
     values,
@@ -79,6 +84,8 @@
     middle,
     ffn_in,
     outgoing,
+    combine,
+    dispatch,
     blocked,
     weights_t,
     small_sems,
@@ -105,6 +112,8 @@
                 (bias_hbm, score_bias),
                 (ffn_gain_hbm, ffn_gain),
                 (branch_hbm, branch_gate),
+                (picks_hbm, picks),
+                (pick_weights_hbm, pick_weights),
             )
         )
     ]
@@ -138,6 +147,33 @@
     hidden_f = hidden[...].astype(f32)
     normed = rms_rows(hidden_f, attn_gain[...])
 
+    rows = outgoing.shape[0]
+    cuts = hidden.shape[1] // outgoing.shape[1]
+    shape = (rows, seqs)
+    expert = iota(shape, 0) // (capacity * cuts)
+    named = jnp.zeros(shape, f32)
+    weighted = jnp.zeros(shape, f32)
+    for k in range(TOP):
+        hit = expert == picks[k : k + 1, :]
+        named = named + jnp.where(hit, 1.0, 0.0)
+        weighted = weighted + jnp.where(hit, pick_weights[k : k + 1, :], 0.0)
+    earlier = (iota((seqs, seqs), 0) < iota((seqs, seqs), 1)).astype(bf16)
+    rank = matmul(named.astype(bf16), earlier)
+    mine = rank == (iota(shape, 0) % capacity).astype(f32)
+    wide = (rows, cuts * seqs)
+    repeat = (iota((seqs, wide[1]), 1) % seqs == iota((seqs, wide[1]), 0)).astype(bf16)
+    own_cut = (iota(wide, 0) // capacity) % cuts == iota(wide, 1) // seqs
+
+    def spread_cuts(values):
+        return jnp.where(own_cut, matmul(values, repeat), 0.0).astype(bf16)
+
+    dispatch[...] = spread_cuts(jnp.where(mine, named, 0.0).astype(bf16))
+    parts = three_parts(jnp.where(mine, weighted, 0.0))
+    for part in range(3):
+        combine[:, part * wide[1] : (part + 1) * wide[1]] = spread_cuts(parts[part])
+    send_combine = pltpu.make_async_copy(combine, combine_hbm, send_sems.at[3])
+    send_combine.start()
+
     lane = iota((1, lanes), 1)
     lane_len = jnp.zeros((1, lanes), jnp.int32)
     for n in range(seqs):
@@ -226,6 +262,7 @@
     send_middle.wait()
     send_ffn.wait()
     send_out.wait()
+    send_combine.wait()
 
 
 SMEM = pl.BlockSpec(memory_space=pltpu.SMEM)
@@ -252,44 +289,47 @@
     return jax.ShapeDtypeStruct(shape, dtype)
 
 
-def attend(args, out_rows, out_cut):
+def attend(args, capacity, out_rows, out_cut):
     hidden = args[2]
-    keys = args[8]
+    keys = args[9]
     seqs, width = hidden.shape
     cache_len = keys.shape[1]
+    lanes = width // out_cut * seqs
     return call(
-        attend_kernel,
+        lambda *refs: attend_kernel(capacity, *refs),
         (
             pltpu.HBM((seqs, width), f32),
             pltpu.HBM((seqs, width), bf16),
             pltpu.HBM((out_rows, out_cut), bf16),
+            pltpu.HBM((out_rows, 3 * lanes), bf16),
             shaped((seqs, 128), f32),
-        )
-        + tuple(pltpu.VMEM(a.shape, a.dtype) for a in args[11:]),
-        tuple(arg if i == 6 else in_hbm(arg) for i, arg in enumerate(args)),
-        [HBM] * 6 + [VMEM] + [HBM] * 5,
-        [HBM] * 3 + [VMEM] * 2,
+            pltpu.VMEM(args[12].shape, bf16),
+        ),
+        tuple(in_hbm(arg) for arg in args),
+        [HBM] * 13,
+        [HBM] * 4 + [VMEM] * 2,
         [
             pltpu.SMEM(args[0].shape, jnp.int32),
             pltpu.SMEM(args[1].shape, f32),
         ]
-        + [pltpu.VMEM(a.shape, a.dtype) for a in args[2:6]]
-        + [pltpu.VMEM(a.shape, a.dtype) for a in args[7:11]]
+        + [pltpu.VMEM(a.shape, a.dtype) for a in args[2:12]]
         + [
             pltpu.VMEM((seqs, width), f32),
             pltpu.VMEM((seqs, width), bf16),
             pltpu.VMEM((out_rows, out_cut), bf16),
+            pltpu.VMEM((out_rows, 3 * lanes), bf16),
+            pltpu.VMEM((out_rows, lanes), bf16),
             pltpu.VMEM((seqs * KV_WIDTH, seqs * HEADS), bf16),
             pltpu.VMEM((seqs * HEADS, cache_len), bf16),
-            pltpu.SemaphoreType.DMA((6,)),
+            pltpu.SemaphoreType.DMA((8,)),
             pltpu.SemaphoreType.DMA,
             pltpu.SemaphoreType.DMA((4,)),
             pltpu.SemaphoreType.DMA((4,)),
             pltpu.SemaphoreType.DMA,
             pltpu.SemaphoreType.DMA,
-            pltpu.SemaphoreType.DMA((3,)),
+            pltpu.SemaphoreType.DMA((4,)),
         ],
-        32,
+        40,
     )
 
 
@@ -305,87 +345,6 @@
         (hidden, gain, key_w, value_w),
         [VMEM] * 4,
         [VMEM] * 2,
-    )
-
-
-def prepare(gate_t, up_t, down_t, routes_t, route_weights_t, capacity, cuts, experts):
-    units, width = gate_t.shape
-    seqs = routes_t.shape[1]
-    rows = experts * capacity * cuts
-    lanes = cuts * seqs
-
-    def kernel(
-        gate,
-        up,
-        down,
-        picks_hbm,
-        pick_weights_hbm,
-        own,
-        dispatch,
-        combine_hbm,
-        combine,
-        picks,
-        pick_weights,
-        sems,
-    ):
-        small = [
-            pltpu.make_async_copy(picks_hbm, picks, sems.at[4]),
-            pltpu.make_async_copy(pick_weights_hbm, pick_weights, sems.at[5]),
-        ]
-        for copy in small:
-            copy.start()
-        copies = [
-            pltpu.make_async_copy(source, own.at[pl.ds(i * units, units)], sems.at[i])
-            for i, source in enumerate((gate, up, down))
-        ]
-        for copy in copies:
-            copy.start()
-        for copy in small:
-            copy.wait()
-        shape = (rows, seqs)
-        expert = iota(shape, 0) // (capacity * cuts)
-        named = jnp.zeros(shape, f32)
-        weighted = jnp.zeros(shape, f32)
-        for k in range(TOP):
-            hit = expert == picks[k : k + 1, :]
-            named = named + jnp.where(hit, 1.0, 0.0)
-            weighted = weighted + jnp.where(hit, pick_weights[k : k + 1, :], 0.0)
-        earlier = (iota((seqs, seqs), 0) < iota((seqs, seqs), 1)).astype(bf16)
-        rank = matmul(named.astype(bf16), earlier)
-        mine = rank == (iota(shape, 0) % capacity).astype(f32)
-        repeat = (iota((seqs, lanes), 1) % seqs == iota((seqs, lanes), 0)).astype(bf16)
-        own_cut = (iota((rows, lanes), 0) // capacity) % cuts == iota((rows, lanes), 1) // seqs
-
-        def spread(values):
-            return jnp.where(own_cut, matmul(values, repeat), 0.0).astype(bf16)
-
-        dispatch[...] = spread(jnp.where(mine, named, 0.0).astype(bf16))
-        parts = three_parts(jnp.where(mine, weighted, 0.0))
-        for part in range(3):
-            combine[:, part * lanes : (part + 1) * lanes] = spread(parts[part])
-        send = pltpu.make_async_copy(combine, combine_hbm, sems.at[6])
-        send.start()
-        send.wait()
-        for copy in copies:
-            copy.wait()
-
-    return call(
-        kernel,
-        (
-            shaped((3 * units, width), bf16),
-            shaped((rows, lanes), bf16),
-            pltpu.HBM((rows, 3 * lanes), bf16),
-        ),
-        (gate_t, up_t, down_t, routes_t, route_weights_t),
-        [HBM] * 5,
-        [HBM] + [VMEM] + [HBM],
-        [
-            pltpu.VMEM((rows, 3 * lanes), bf16),
-            pltpu.VMEM(routes_t.shape, jnp.int32),
-            pltpu.VMEM(route_weights_t.shape, f32),
-            pltpu.SemaphoreType.DMA((7,)),
-        ],
-        32,
     )
 
 
@@ -456,39 +415,33 @@
 
 def run_dense(tokens, pieces):
     seqs, width = tokens[0].shape
-    count = len(pieces)
-    units = pieces[0].shape[0] // 3
+    count = len(pieces) // 3
+    units = pieces[0].shape[0]
     total = len(tokens)
     kept = total // 2 * seqs
 
     def kernel(*refs):
         token_refs = refs[:total]
-        sources = refs[total : total + count]
-        keep, give, gates, ups, downs, sems = refs[total + count :]
+        sources = refs[total : total + 3 * count]
+        keep, give, weights, sems = refs[total + 3 * count :]
         copies = [
-            [
-                pltpu.make_async_copy(
-                    source.at[pl.ds(kind * units, units)],
-                    target.at[pl.ds(i * units, units)],
-                    sems.at[kind, i],
-                )
-                for i, source in enumerate(sources)
-            ]
-            for kind, target in enumerate((gates, ups, downs))
+            pltpu.make_async_copy(
+                source, weights.at[i // count, pl.ds(i % count * units, units)], sems.at[i]
+            )
+            for i, source in enumerate(sources)
         ]
-        for group in copies:
-            for copy in group:
-                copy.start()
+        for copy in copies:
+            copy.start()
         rows = jnp.concatenate([ref[...] for ref in token_refs], axis=0)
-        for copy in copies[0]:
+        for copy in copies[:count]:
             copy.wait()
-        hidden = jax.nn.silu(matmul_bt(rows, gates[...]))
-        for copy in copies[1]:
+        hidden = jax.nn.silu(matmul_bt(rows, weights[0]))
+        for copy in copies[count : 2 * count]:
             copy.wait()
-        hidden = hidden * matmul_bt(rows, ups[...])
-        for copy in copies[2]:
+        hidden = hidden * matmul_bt(rows, weights[1])
+        for copy in copies[2 * count :]:
             copy.wait()
-        partial = matmul(hidden.astype(bf16), downs[...])
+        partial = matmul(hidden.astype(bf16), weights[2])
         keep[...] = partial[:kept]
         give[...] = partial[kept:].astype(bf16)
 
@@ -496,9 +449,12 @@
         kernel,
         (shaped((kept, width), f32), shaped((total * seqs - kept, width), bf16)),
         (*tokens, *pieces),
-        [VMEM] * total + [HBM] * count,
+        [VMEM] * total + [HBM] * (3 * count),
         [VMEM] * 2,
-        [pltpu.VMEM((count * units, width), bf16)] * 3 + [pltpu.SemaphoreType.DMA((3, count))],
+        [
+            pltpu.VMEM((3, count * units, width), bf16),
+            pltpu.SemaphoreType.DMA((3 * count,)),
+        ],
         32,
     )
 
@@ -590,21 +546,21 @@
             values, "ep", [(i, (i + steps * plane) % devices) for i in range(devices)]
         )
 
-    own, dispatch, combine = prepare(
-        in_hbm(dense_gate.T),
-        in_hbm(dense_up.T),
-        in_hbm(dense_down.T),
-        in_hbm(routes.T),
-        in_hbm(route_weights.T),
-        capacity,
-        cuts,
-        experts_all,
-    )
-    pieces = [own]
+    own = {"gate": dense_gate.T, "up": dense_up.T, "down": dense_down.T}
+    held = {0: own}
     for other in range(2, plane, 2):
-        pieces.append(swap(own, other))
-
-    middle, ffn_in, outgoing, gate_value, gate_w = attend(
+        first, last = other & -other, other & (other - 1)
+        held[other] = {}
+        for kind, values in own.items():
+            if last == 0 or last & (last - 1):
+                held[other][kind] = swap(values, other)
+            elif kind == "gate":
+                held[other][kind] = swap(held[first][kind], last)
+            else:
+                held[other][kind] = swap(held[last][kind], first)
+    pieces = [held[other][kind] for kind in own for other in held]
+
+    middle, ffn_in, outgoing, combine, gate_value, gate_w = attend(
         (
             lengths,
             score_bias,
@@ -612,13 +568,15 @@
             attn_gain.reshape(1, width),
             ffn_gain.reshape(1, width),
             branch_gate.reshape(1, width),
-            dispatch,
+            routes.T,
+            route_weights.T,
             query_weight,
             key_cache,
             value_cache,
             out_weight,
             expert_gate[0],
         ),
+        capacity,
         devices * chunk,
         width // cuts,
     )

time: 72.9 us -> 88.1 us (1.21)
  local copies, waits for them, and re-layouts: 0.01 us -> 10.4 us
  starting transfers between devices: 26.1 us -> 33 us
  Pallas kernels: 21.2 us -> 19 us
    ppermute x8 -> x14, waiting for transfers between devices: 3.02 us -> 15.1 us  [swap(): return lax.ppermute(values, 'ep', [(i, i ^ bits) for i in range(devices)])]
    all_to_all x1, waiting for transfers between devices: 11.1 us -> 0.01 us  [per_device(): lax.all_to_all(outgoing.reshape(devices, chunk, width // cuts), 'ep', spl...]
    unnamed x6 -> x40, local copies, waits for them, and re-layouts: 0.01 us -> 10.4 us
    ppermute x8 -> x14, starting transfers between devices: 5.98 us -> 11.9 us  [swap(): return lax.ppermute(values, 'ep', [(i, i ^ bits) for i in range(devices)])]
    pallas_call x7 -> x6, Pallas kernels: 21.2 us -> 19 us  [call(): pl.pallas_call(kernel, out_shape=out_shape, in_specs=in_specs, out_specs=...]
    ppermute x6, waiting for transfers between devices: 10.4 us -> 9.21 us  [climb(): lax.ppermute(values, 'ep', [(i, (i + steps * plane) % devices) for i in r...]
    all_to_all x1, starting transfers between devices: 6.32 us -> 7.33 us  [per_device(): lax.all_to_all(outgoing.reshape(devices, chunk, width // cuts), 'ep', spl...]
  transfers between devices with their start and end apart: 16 -> 22, of which waited for: 7 -> 10; matrix products, arithmetic and copies ran while one was open for 0% -> 0% of each run, Pallas kernels for 25% -> 10%
where the time goes in v4:
time: 88.1 us; the launch traced here: 87.6 us
  starting transfers between devices  33 us (37%)
  waiting for transfers between devices  24.3 us (28%)
  Pallas kernels  19 us (22%)
  local copies, waits for them, and re-layouts  10.4 us (12%)
    pallas_call x6, Pallas kernels, call(): pl.pallas_call(kernel, out_shape=out_shape, in_specs=in_specs, out_specs=...  19 us
    ppermute x14, waiting for transfers between devices, swap(): return lax.ppermute(values, 'ep', [(i, i ^ bits) for i in range(devices)])  15.1 us
    ppermute x14, starting transfers between devices, swap(): return lax.ppermute(values, 'ep', [(i, i ^ bits) for i in range(devices)])  11.9 us
    unnamed x40, local copies, waits for them, and re-layouts  10.4 us
    ppermute x6, waiting for transfers between devices, climb(): lax.ppermute(values, 'ep', [(i, (i + steps * plane) % devices) for i in r...  9.21 us
    ppermute x6, starting transfers between devices, climb(): lax.ppermute(values, 'ep', [(i, (i + steps * plane) % devices) for i in r...  9.18 us
    all_to_all x1, starting transfers between devices, per_device(): lax.all_to_all(outgoing.reshape(devices, chunk, width // cuts), 'ep', spl...  7.33 us
    all_to_all x1, starting transfers between devices, per_device(): lax.all_to_all(expert_rows, 'ep', split_axis=0, concat_axis=0, tiled=True)  4.67 us
  transfers between devices with their start and end apart: 22, of which 10 were waited for; matrix products, arithmetic and copies ran while one was open for 0% of the time, Pallas kernels for 10%

profile of v4, /device:TPU:0, one launch (start us, length us, event | category | flops | bytes accessed | tf_op | source)
XLA Modules:
  0.0 87.6 jit_solution(1328393557609529181)
XLA Ops:
  0.7 8.9 %shard_map.211 = (f32[16,2048]{1,0:T(8,128)}, bf16[16,2048]{1,0:T(8,128)(2,1)}, bf16[512,256]{1,0:T(8,128)(2,1)}, bf16[512,384]{1,0:T(8,128)(2,1)}, f32[16,128]{...) custom-call(s32[16]{0:T(128)} %refs_0_.1, f32[8]{0:T(128)} %refs_1_.1, bf16[16,2048]{1,0:T(8,128)(2,1)} %rows.1, ...), custom_call_target="tpu_custom_call" | custom-call | tf_op jit(solution)/shard_map/pallas_call | solution.py:278
  9.6 7.3 %all-to-all-start = ((bf16[32,16,256]{2,1,0:T(8,128)(2,1)}), bf16[32,16,256]{2,1,0:T(8,128)(2,1)S(1)}, u32[]{:S(2)}, u32[]{:S(2)}) async-start(bf16[32,16,256]{2,1,0:T(8,128)(2,1)} %bitcast.24), calls=%async_computation | async-start | bytes 524288 | tf_op jit(solution)/shard_map/all_to_all | solution.py:583
  16.9 1.8 %collective-permute-start = (bf16[16,2048]{1,0:T(8,128)(2,1)}, bf16[16,2048]{1,0:T(8,128)(2,1)S(1)}, u32[]{:S(2)}, u32[]{:S(2)}) collective-permute-start(bf16[16,2048]{1,0:T(8,128)(2,1)} %get-tuple-element.22.refs_0_), channel_id=1, source_target_pairs={{0,8},{1,9},{2,10},{3,11},{4,12},{5,13},{6,14},{7,15},{8,16},{9,17... | collective-permute-start | bytes 196616 | tf_op jit(solution)/shard_map/ppermute | solution.py:545
  18.7 2.4 %collective-permute-start.1 = (bf16[16,2048]{1,0:T(8,128)(2,1)}, bf16[16,2048]{1,0:T(8,128)(2,1)S(1)}, u32[]{:S(2)}, u32[]{:S(2)}) collective-permute-start(bf16[16,2048]{1,0:T(8,128)(2,1)} %get-tuple-element.22.refs_0_), channel_id=1, source_target_pairs={{0,16},{1,17},{2,18},{3,19},{4,20},{5,21},{6,22},{7,23},{8,24},{9,... | collective-permute-start | bytes 196616 | tf_op jit(solution)/shard_map/ppermute | solution.py:545
  21.1 1.4 %collective-permute-start.2 = (bf16[16,2048]{1,0:T(8,128)(2,1)}, bf16[16,2048]{1,0:T(8,128)(2,1)S(1)}, u32[]{:S(2)}, u32[]{:S(2)}) collective-permute-start(bf16[16,2048]{1,0:T(8,128)(2,1)} %get-tuple-element.22.refs_0_), channel_id=1, source_target_pairs={{0,24},{1,25},{2,26},{3,27},{4,28},{5,29},{6,30},{7,31},{8,0},{9,1... | collective-permute-start | bytes 196616 | tf_op jit(solution)/shard_map/ppermute | solution.py:545
  22.6 1.5 %collective-permute-start.7 = (bf16[64,2048]{1,0:T(8,128)(2,1)S(1)}, bf16[64,2048]{1,0:T(8,128)(2,1)S(1)}, u32[]{:S(2)}, u32[]{:S(2)}) collective-permute-start(bf16[64,2048]{1,0:T(8,128)(2,1)S(1)} %bitcast.12), channel_id=1, source_target_pairs={{0,2},{1,3},{2,0},{3,1},{4,6},{5,7},{6,4},{7,5},{8,10},{9,11},{10,... | collective-permute-start | bytes 786440 | tf_op jit(solution)/shard_map/ppermute | solution.py:542
  24.0 3.7 %collective-permute-done.refs_1_ = bf16[16,2048]{1,0:T(8,128)(2,1)S(1)} collective-permute-done((bf16[16,2048]{1,0:T(8,128)(2,1)}, bf16[16,2048]{1,0:T(8,128)(2,1)S(1)}, u32[]{:S(2)}, u32[]{:S(2)}) %collective-permute-start) | collective-permute-done | bytes 65568 | tf_op jit(solution)/shard_map/ppermute | solution.py:545
  27.8 1.5 %collective-permute-start.8 = (bf16[64,2048]{1,0:T(8,128)(2,1)S(1)}, bf16[64,2048]{1,0:T(8,128)(2,1)S(1)}, u32[]{:S(2)}, u32[]{:S(2)}) collective-permute-start(bf16[64,2048]{1,0:T(8,128)(2,1)S(1)} %bitcast.13), channel_id=1, source_target_pairs={{0,4},{1,5},{2,6},{3,7},{4,0},{5,1},{6,2},{7,3},{8,12},{9,13},{10,... | collective-permute-start | bytes 786440 | tf_op jit(solution)/shard_map/ppermute | solution.py:542
  29.3 1.8 %collective-permute-done.1.refs_2_ = bf16[16,2048]{1,0:T(8,128)(2,1)S(1)} collective-permute-done((bf16[16,2048]{1,0:T(8,128)(2,1)}, bf16[16,2048]{1,0:T(8,128)(2,1)S(1)}, u32[]{:S(2)}, u32[]{:S(2)}) %collective-permute-start.1) | collective-permute-done | bytes 65568 | tf_op jit(solution)/shard_map/ppermute | solution.py:545
  31.0 1.5 %collective-permute-start.11 = (bf16[64,2048]{1,0:T(8,128)(2,1)S(1)}, bf16[64,2048]{1,0:T(8,128)(2,1)}, u32[]{:S(2)}, u32[]{:S(2)}) collective-permute-start(bf16[64,2048]{1,0:T(8,128)(2,1)S(1)} %bitcast.15), channel_id=1, source_target_pairs={{0,4},{1,5},{2,6},{3,7},{4,0},{5,1},{6,2},{7,3},{8,12},{9,13},{10,... | collective-permute-start | bytes 786440 | tf_op jit(solution)/shard_map/ppermute | solution.py:542
  33.7 1.3 %collective-permute-done.4.refs_5_ = bf16[16,2048]{1,0:T(8,128)(2,1)S(1)} collective-permute-done((bf16[16,2048]{1,0:T(8,128)(2,1)S(1)}, bf16[16,2048]{1,0:T(8,128)(2,1)S(1)}, u32[]{:S(2)}, u32[]{:S(2)}) %collective-permute-start.4) | collective-permute-done | bytes 65568 | tf_op jit(solution)/shard_map/ppermute | solution.py:542
  39.3 1.5 %collective-permute-start.10 = (bf16[64,2048]{1,0:T(8,128)(2,1)S(1)}, bf16[64,2048]{1,0:T(8,128)(2,1)}, u32[]{:S(2)}, u32[]{:S(2)}) collective-permute-start(bf16[64,2048]{1,0:T(8,128)(2,1)S(1)} %bitcast.16), channel_id=1, source_target_pairs={{0,2},{1,3},{2,0},{3,1},{4,6},{5,7},{6,4},{7,5},{8,10},{9,11},{10,... | collective-permute-start | bytes 786440 | tf_op jit(solution)/shard_map/ppermute | solution.py:542
  42.0 1.5 %collective-permute-start.9 = (bf16[64,2048]{1,0:T(8,128)(2,1)S(1)}, bf16[64,2048]{1,0:T(8,128)(2,1)}, u32[]{:S(2)}, u32[]{:S(2)}) collective-permute-start(bf16[64,2048]{1,0:T(8,128)(2,1)S(1)} %collective-permute-done.7.refs_9_), channel_id=1, source_target_pairs={{0,4},{1,5},{2,6},{3,7},{4,0},{5,1},{6,2},{7,3},{8,12},{9,13},{10,... | collective-permute-start | bytes 786440 | tf_op jit(solution)/shard_map/ppermute | solution.py:542
  43.5 1.5 %collective-permute-start.12 = (bf16[64,2048]{1,0:T(8,128)(2,1)}, bf16[64,2048]{1,0:T(8,128)(2,1)}, u32[]{:S(2)}, u32[]{:S(2)}) collective-permute-start(bf16[64,2048]{1,0:T(8,128)(2,1)} %collective-permute-done.11.refs_14_), channel_id=1, source_target_pairs={{0,2},{1,3},{2,0},{3,1},{4,6},{5,7},{6,4},{7,5},{8,10},{9,11},{10,... | collective-permute-start | bytes 786440 | tf_op jit(solution)/shard_map/ppermute | solution.py:542
  45.0 3.3 %collective-permute-done.14.refs_18_ = bf16[64,2048]{1,0:T(8,128)(2,1)} collective-permute-done((bf16[64,2048]{1,0:T(8,128)(2,1)S(1)}, bf16[64,2048]{1,0:T(8,128)(2,1)}, u32[]{:S(2)}, u32[]{:S(2)}) %collective-permute-start.14) | collective-permute-done | bytes 262176 | tf_op jit(solution)/shard_map/ppermute | solution.py:542
  48.3 1.5 %collective-permute-start.15 = (bf16[64,2048]{1,0:T(8,128)(2,1)}, bf16[64,2048]{1,0:T(8,128)(2,1)}, u32[]{:S(2)}, u32[]{:S(2)}) collective-permute-start(bf16[64,2048]{1,0:T(8,128)(2,1)} %collective-permute-done.14.refs_18_), channel_id=1, source_target_pairs={{0,2},{1,3},{2,0},{3,1},{4,6},{5,7},{6,4},{7,5},{8,10},{9,11},{10,... | collective-permute-start | bytes 786440 | tf_op jit(solution)/shard_map/ppermute | solution.py:542
  49.8 4.1 %shard_map.212 = bf16[32,16,256]{2,1,0:T(8,128)(2,1)} custom-call(bf16[32,16,256]{2,1,0:T(8,128)(2,1)S(1)} %all-to-all-done.rows, bf16[2048,512]{1,0:T(8,128)(2,1)S(1)} %get-tuple-element.21.gate, bf16[2048,512]{1,0:T(8,128)(2,1)} %bitcast.22, bf16[512,2048]{1,0:T(8,128)(2,1)} %bitcast.23), custom_call_target="tpu_custom_call" | custom-call | tf_op jit(solution)/shard_map/pallas_call | solution.py:278
  53.9 4.7 %all-to-all-start.1 = ((bf16[32,16,256]{2,1,0:T(8,128)(2,1)}), bf16[32,16,256]{2,1,0:T(8,128)(2,1)S(1)}, u32[]{:S(2)}, u32[]{:S(2)}) async-start(bf16[32,16,256]{2,1,0:T(8,128)(2,1)} %shard_map.212), calls=%async_computation.1 | async-start | bytes 524288 | tf_op jit(solution)/shard_map/all_to_all | solution.py:596
  59.8 6.8 %collective-permute-done.15.refs_19_ = bf16[64,2048]{1,0:T(8,128)(2,1)} collective-permute-done((bf16[64,2048]{1,0:T(8,128)(2,1)}, bf16[64,2048]{1,0:T(8,128)(2,1)}, u32[]{:S(2)}, u32[]{:S(2)}) %collective-permute-start.15) | collective-permute-done | bytes 262176 | tf_op jit(solution)/shard_map/ppermute | solution.py:542
  72.7 2.8 %shard_map.213 = (f32[64,2048]{1,0:T(8,128)S(1)}, bf16[64,2048]{1,0:T(8,128)(2,1)S(1)}) custom-call(bf16[16,2048]{1,0:T(8,128)(2,1)S(1)} %copy-done.7, bf16[16,2048]{1,0:T(8,128)(2,1)S(1)} %collective-permute-done.refs_1_, bf16[16,2048]{1,0:T(8,128)(2,1)S(1)} %copy-done.9, bf16[16,2048]{1,0:T(8,128)(2,1)S(1)} %copy-done.11, bf16[16,2048]{1,0:T(8,128)(2,1)S(1)} %copy-done.13, ...), custom_call_target="tpu_custom_call" | custom-call | tf_op jit(solution)/shard_map/pallas_call | solution.py:278
  75.6 1.5 %collective-permute-done.16.right = bf16[64,2048]{1,0:T(8,128)(2,1)S(1)} collective-permute-done((bf16[64,2048]{1,0:T(8,128)(2,1)S(1)}, bf16[64,2048]{1,0:T(8,128)(2,1)S(1)}, u32[]{:S(2)}, u32[]{:S(2)}) %collective-permute-start.16) | collective-permute-done | bytes 262176 | tf_op jit(solution)/shard_map/ppermute | solution.py:542
  77.2 2.3 %collective-permute-start.17 = (bf16[16,2048]{1,0:T(8,128)(2,1)S(1)}, bf16[16,2048]{1,0:T(8,128)(2,1)S(1)}, u32[]{:S(2)}, u32[]{:S(2)}) collective-permute-start(bf16[16,2048]{1,0:T(8,128)(2,1)S(1)} %get-tuple-element.26), channel_id=1, source_target_pairs={{0,24},{1,25},{2,26},{3,27},{4,28},{5,29},{6,30},{7,31},{8,0},{9,1... | collective-permute-start | bytes 196616 | tf_op jit(solution)/shard_map/ppermute | solution.py:545
  80.7 2.2 %shard_map.216 = (bf16[16,128]{1,0:T(8,128)(2,1)}, bf16[16,128]{1,0:T(8,128)(2,1)}) custom-call(bf16[16,2048]{1,0:T(8,128)(2,1)} %rows.1, f32[1,2048]{1,0:T(1,128)} %bitcast.26, bf16[2048,128]{1,0:T(8,128)(2,1)} %left.1, bf16[2048,128]{1,0:T(8,128)(2,1)} %right.1), custom_call_target="tpu_custom_call" | custom-call | tf_op jit(solution)/shard_map/pallas_call | solution.py:278
  82.9 3.7 %collective-permute-done.18.refs_2_ = bf16[16,2048]{1,0:T(8,128)(2,1)S(1)} collective-permute-done((bf16[16,2048]{1,0:T(8,128)(2,1)S(1)}, bf16[16,2048]{1,0:T(8,128)(2,1)S(1)}, u32[]{:S(2)}, u32[]{:S(2)}) %collective-permute-start.18) | collective-permute-done | bytes 65568 | tf_op jit(solution)/shard_map/ppermute | solution.py:545
  (66 shorter events, 16.3 us)
Async XLA Ops:
  0.7 31.9 %copy-start.3 = (bf16[2048,64]{0,1:T(8,128)(2,1)S(1)}, bf16[2048,64]{0,1:T(8,128)(2,1)}, u32[]{:S(2)}) copy-start(bf16[2048,64]{0,1:T(8,128)(2,1)} %param.38) | copy-start | bytes 786436
  9.6 40.2 %all-to-all-start = ((bf16[32,16,256]{2,1,0:T(8,128)(2,1)}), bf16[32,16,256]{2,1,0:T(8,128)(2,1)S(1)}, u32[]{:S(2)}, u32[]{:S(2)}) async-start(bf16[32,16,256]{2,1,0:T(8,128)(2,1)} %bitcast.24), calls=%async_computation | async-start | bytes 524288 | tf_op jit(solution)/shard_map/all_to_all | solution.py:583
  16.9 10.9 %collective-permute-start = (bf16[16,2048]{1,0:T(8,128)(2,1)}, bf16[16,2048]{1,0:T(8,128)(2,1)S(1)}, u32[]{:S(2)}, u32[]{:S(2)}) collective-permute-start(bf16[16,2048]{1,0:T(8,128)(2,1)} %get-tuple-element.22.refs_0_), channel_id=1, source_target_pairs={{0,8},{1,9},{2,10},{3,11},{4,12},{5,13},{6,14},{7,15},{8,16},{9,17... | collective-permute-start | bytes 196616 | tf_op jit(solution)/shard_map/ppermute | solution.py:545
  18.7 12.3 %collective-permute-start.1 = (bf16[16,2048]{1,0:T(8,128)(2,1)}, bf16[16,2048]{1,0:T(8,128)(2,1)S(1)}, u32[]{:S(2)}, u32[]{:S(2)}) collective-permute-start(bf16[16,2048]{1,0:T(8,128)(2,1)} %get-tuple-element.22.refs_0_), channel_id=1, source_target_pairs={{0,16},{1,17},{2,18},{3,19},{4,20},{5,21},{6,22},{7,23},{8,24},{9,... | collective-permute-start | bytes 196616 | tf_op jit(solution)/shard_map/ppermute | solution.py:545
  21.1 11.4 %collective-permute-start.2 = (bf16[16,2048]{1,0:T(8,128)(2,1)}, bf16[16,2048]{1,0:T(8,128)(2,1)S(1)}, u32[]{:S(2)}, u32[]{:S(2)}) collective-permute-start(bf16[16,2048]{1,0:T(8,128)(2,1)} %get-tuple-element.22.refs_0_), channel_id=1, source_target_pairs={{0,24},{1,25},{2,26},{3,27},{4,28},{5,29},{6,30},{7,31},{8,0},{9,1... | collective-permute-start | bytes 196616 | tf_op jit(solution)/shard_map/ppermute | solution.py:545
  22.6 10.5 %collective-permute-start.3 = (bf16[16,2048]{1,0:T(8,128)(2,1)}, bf16[16,2048]{1,0:T(8,128)(2,1)S(1)}, u32[]{:S(2)}, u32[]{:S(2)}) collective-permute-start(bf16[16,2048]{1,0:T(8,128)(2,1)} %get-tuple-element.22.refs_0_), channel_id=1, source_target_pairs={{0,1},{1,0},{2,3},{3,2},{4,5},{5,4},{6,7},{7,6},{8,9},{9,8},{10,11... | collective-permute-start | bytes 196616 | tf_op jit(solution)/shard_map/ppermute | solution.py:542
  22.6 18.2 %collective-permute-start.7 = (bf16[64,2048]{1,0:T(8,128)(2,1)S(1)}, bf16[64,2048]{1,0:T(8,128)(2,1)S(1)}, u32[]{:S(2)}, u32[]{:S(2)}) collective-permute-start(bf16[64,2048]{1,0:T(8,128)(2,1)S(1)} %bitcast.12), channel_id=1, source_target_pairs={{0,2},{1,3},{2,0},{3,1},{4,6},{5,7},{6,4},{7,5},{8,10},{9,11},{10,... | collective-permute-start | bytes 786440 | tf_op jit(solution)/shard_map/ppermute | solution.py:542
  27.8 13.6 %collective-permute-start.8 = (bf16[64,2048]{1,0:T(8,128)(2,1)S(1)}, bf16[64,2048]{1,0:T(8,128)(2,1)S(1)}, u32[]{:S(2)}, u32[]{:S(2)}) collective-permute-start(bf16[64,2048]{1,0:T(8,128)(2,1)S(1)} %bitcast.13), channel_id=1, source_target_pairs={{0,4},{1,5},{2,6},{3,7},{4,0},{5,1},{6,2},{7,3},{8,12},{9,13},{10,... | collective-permute-start | bytes 786440 | tf_op jit(solution)/shard_map/ppermute | solution.py:542
  31.0 12.5 %collective-permute-start.11 = (bf16[64,2048]{1,0:T(8,128)(2,1)S(1)}, bf16[64,2048]{1,0:T(8,128)(2,1)}, u32[]{:S(2)}, u32[]{:S(2)}) collective-permute-start(bf16[64,2048]{1,0:T(8,128)(2,1)S(1)} %bitcast.15), channel_id=1, source_target_pairs={{0,4},{1,5},{2,6},{3,7},{4,0},{5,1},{6,2},{7,3},{8,12},{9,13},{10,... | collective-permute-start | bytes 786440 | tf_op jit(solution)/shard_map/ppermute | solution.py:542
  32.5 15.8 %collective-permute-start.14 = (bf16[64,2048]{1,0:T(8,128)(2,1)S(1)}, bf16[64,2048]{1,0:T(8,128)(2,1)}, u32[]{:S(2)}, u32[]{:S(2)}) collective-permute-start(bf16[64,2048]{1,0:T(8,128)(2,1)S(1)} %bitcast.18), channel_id=1, source_target_pairs={{0,4},{1,5},{2,6},{3,7},{4,0},{5,1},{6,2},{7,3},{8,12},{9,13},{10,... | collective-permute-start | bytes 786440 | tf_op jit(solution)/shard_map/ppermute | solution.py:542
  33.7 1.3 %collective-permute-start.4 = (bf16[16,2048]{1,0:T(8,128)(2,1)S(1)}, bf16[16,2048]{1,0:T(8,128)(2,1)S(1)}, u32[]{:S(2)}, u32[]{:S(2)}) collective-permute-start(bf16[16,2048]{1,0:T(8,128)(2,1)S(1)} %collective-permute-done.refs_1_), channel_id=1, source_target_pairs={{0,1},{1,0},{2,3},{3,2},{4,5},{5,4},{6,7},{7,6},{8,9},{9,8},{10,11... | collective-permute-start | bytes 196616 | tf_op jit(solution)/shard_map/ppermute | solution.py:542
  35.6 1.3 %collective-permute-start.5 = (bf16[16,2048]{1,0:T(8,128)(2,1)S(1)}, bf16[16,2048]{1,0:T(8,128)(2,1)S(1)}, u32[]{:S(2)}, u32[]{:S(2)}) collective-permute-start(bf16[16,2048]{1,0:T(8,128)(2,1)S(1)} %collective-permute-done.1.refs_2_), channel_id=1, source_target_pairs={{0,1},{1,0},{2,3},{3,2},{4,5},{5,4},{6,7},{7,6},{8,9},{9,8},{10,11... | collective-permute-start | bytes 196616 | tf_op jit(solution)/shard_map/ppermute | solution.py:542
  37.4 1.3 %collective-permute-start.6 = (bf16[16,2048]{1,0:T(8,128)(2,1)S(1)}, bf16[16,2048]{1,0:T(8,128)(2,1)S(1)}, u32[]{:S(2)}, u32[]{:S(2)}) collective-permute-start(bf16[16,2048]{1,0:T(8,128)(2,1)S(1)} %collective-permute-done.2.refs_3_), channel_id=1, source_target_pairs={{0,1},{1,0},{2,3},{3,2},{4,5},{5,4},{6,7},{7,6},{8,9},{9,8},{10,11... | collective-permute-start | bytes 196616 | tf_op jit(solution)/shard_map/ppermute | solution.py:542
  39.3 19.3 %collective-permute-start.10 = (bf16[64,2048]{1,0:T(8,128)(2,1)S(1)}, bf16[64,2048]{1,0:T(8,128)(2,1)}, u32[]{:S(2)}, u32[]{:S(2)}) collective-permute-start(bf16[64,2048]{1,0:T(8,128)(2,1)S(1)} %bitcast.16), channel_id=1, source_target_pairs={{0,2},{1,3},{2,0},{3,1},{4,6},{5,7},{6,4},{7,5},{8,10},{9,11},{10,... | collective-permute-start | bytes 786440 | tf_op jit(solution)/shard_map/ppermute | solution.py:542
  40.8 17.8 %collective-permute-start.13 = (bf16[64,2048]{1,0:T(8,128)(2,1)S(1)}, bf16[64,2048]{1,0:T(8,128)(2,1)}, u32[]{:S(2)}, u32[]{:S(2)}) collective-permute-start(bf16[64,2048]{1,0:T(8,128)(2,1)S(1)} %bitcast.19), channel_id=1, source_target_pairs={{0,2},{1,3},{2,0},{3,1},{4,6},{5,7},{6,4},{7,5},{8,10},{9,11},{10,... | collective-permute-start | bytes 786440 | tf_op jit(solution)/shard_map/ppermute | solution.py:542
  42.0 16.5 %collective-permute-start.9 = (bf16[64,2048]{1,0:T(8,128)(2,1)S(1)}, bf16[64,2048]{1,0:T(8,128)(2,1)}, u32[]{:S(2)}, u32[]{:S(2)}) collective-permute-start(bf16[64,2048]{1,0:T(8,128)(2,1)S(1)} %collective-permute-done.7.refs_9_), channel_id=1, source_target_pairs={{0,4},{1,5},{2,6},{3,7},{4,0},{5,1},{6,2},{7,3},{8,12},{9,13},{10,... | collective-permute-start | bytes 786440 | tf_op jit(solution)/shard_map/ppermute | solution.py:542
  43.5 16.3 %collective-permute-start.12 = (bf16[64,2048]{1,0:T(8,128)(2,1)}, bf16[64,2048]{1,0:T(8,128)(2,1)}, u32[]{:S(2)}, u32[]{:S(2)}) collective-permute-start(bf16[64,2048]{1,0:T(8,128)(2,1)} %collective-permute-done.11.refs_14_), channel_id=1, source_target_pairs={{0,2},{1,3},{2,0},{3,1},{4,6},{5,7},{6,4},{7,5},{8,10},{9,11},{10,... | collective-permute-start | bytes 786440 | tf_op jit(solution)/shard_map/ppermute | solution.py:542
  48.3 18.4 %collective-permute-start.15 = (bf16[64,2048]{1,0:T(8,128)(2,1)}, bf16[64,2048]{1,0:T(8,128)(2,1)}, u32[]{:S(2)}, u32[]{:S(2)}) collective-permute-start(bf16[64,2048]{1,0:T(8,128)(2,1)} %collective-permute-done.14.refs_18_), channel_id=1, source_target_pairs={{0,2},{1,3},{2,0},{3,1},{4,6},{5,7},{6,4},{7,5},{8,10},{9,11},{10,... | collective-permute-start | bytes 786440 | tf_op jit(solution)/shard_map/ppermute | solution.py:542
  53.9 32.7 %copy-start.6 = (f32[16,2048]{1,0:T(8,128)S(1)}, f32[16,2048]{1,0:T(8,128)}, u32[]{:S(2)}) copy-start(f32[16,2048]{1,0:T(8,128)} %get-tuple-element.17.base) | copy-start | bytes 393220
  53.9 32.7 %all-to-all-start.1 = ((bf16[32,16,256]{2,1,0:T(8,128)(2,1)}), bf16[32,16,256]{2,1,0:T(8,128)(2,1)S(1)}, u32[]{:S(2)}, u32[]{:S(2)}) async-start(bf16[32,16,256]{2,1,0:T(8,128)(2,1)} %shard_map.212), calls=%async_computation.1 | async-start | bytes 524288 | tf_op jit(solution)/shard_map/all_to_all | solution.py:596
  75.5 1.6 %collective-permute-start.16 = (bf16[64,2048]{1,0:T(8,128)(2,1)S(1)}, bf16[64,2048]{1,0:T(8,128)(2,1)S(1)}, u32[]{:S(2)}, u32[]{:S(2)}) collective-permute-start(bf16[64,2048]{1,0:T(8,128)(2,1)S(1)} %get-tuple-element.24), channel_id=1, source_target_pairs={{0,1},{1,0},{2,3},{3,2},{4,5},{5,4},{6,7},{7,6},{8,9},{9,8},{10,11... | collective-permute-start | bytes 786440 | tf_op jit(solution)/shard_map/ppermute | solution.py:542
  77.2 5.7 %collective-permute-start.17 = (bf16[16,2048]{1,0:T(8,128)(2,1)S(1)}, bf16[16,2048]{1,0:T(8,128)(2,1)S(1)}, u32[]{:S(2)}, u32[]{:S(2)}) collective-permute-start(bf16[16,2048]{1,0:T(8,128)(2,1)S(1)} %get-tuple-element.26), channel_id=1, source_target_pairs={{0,24},{1,25},{2,26},{3,27},{4,28},{5,29},{6,30},{7,31},{8,0},{9,1... | collective-permute-start | bytes 196616 | tf_op jit(solution)/shard_map/ppermute | solution.py:545
  79.5 7.1 %collective-permute-start.18 = (bf16[16,2048]{1,0:T(8,128)(2,1)S(1)}, bf16[16,2048]{1,0:T(8,128)(2,1)S(1)}, u32[]{:S(2)}, u32[]{:S(2)}) collective-permute-start(bf16[16,2048]{1,0:T(8,128)(2,1)S(1)} %get-tuple-element.27), channel_id=1, source_target_pairs={{0,16},{1,17},{2,18},{3,19},{4,20},{5,21},{6,22},{7,23},{8,24},{9,... | collective-permute-start | bytes 196616 | tf_op jit(solution)/shard_map/ppermute | solution.py:545
  79.5 7.1 %collective-permute-start.19 = (bf16[16,2048]{1,0:T(8,128)(2,1)S(1)}, bf16[16,2048]{1,0:T(8,128)(2,1)S(1)}, u32[]{:S(2)}, u32[]{:S(2)}) collective-permute-start(bf16[16,2048]{1,0:T(8,128)(2,1)S(1)} %get-tuple-element.28), channel_id=1, source_target_pairs={{0,8},{1,9},{2,10},{3,11},{4,12},{5,13},{6,14},{7,15},{8,16},{9,17... | collective-permute-start | bytes 196616 | tf_op jit(solution)/shard_map/ppermute | solution.py:545
  (18 other events, 107.6 us)
